TPU v7x, 768 devices: a whole 4x8x12 slice. The times are simulated.
768 devices in a mesh: sp: 96 (over z, y), tp: 8 (over x, core).
Axes of the slice: x: 4, y: 8, z: 12, core: 2. Of those that a mesh axis runs over, the one named last changes fastest.
Arguments:
- target: bfloat16 [12288, 2048], P('sp'), may hold values from -160 to 160
- source: bfloat16 [24576, 2048], P(('sp', 'tp')), may hold values from -160 to 160
- query_gain: float32 [2048], replicated, may hold values from 0.1 to 1.9
- source_gain: float32 [2048], replicated, may hold values from 0.1 to 1.9
- query_weight: bfloat16 [2048, 2048], P(None, 'tp'), may hold values from -4 to 4
- key_weight: bfloat16 [2048, 512], replicated, may hold values from -4 to 4
- value_weight: bfloat16 [2048, 512], replicated, may hold values from -1 to 1
- out_weight: bfloat16 [2048, 2048], P('tp'), may hold values from -0.125 to 0.125
- mixer_gain: float32 [2048], replicated, may hold values from 0.1 to 1.9
- gate_weight: bfloat16 [2048, 3072], P(None, 'tp'), may hold values from -0.125 to 0.125
- up_weight: bfloat16 [2048, 3072], P(None, 'tp'), may hold values from -0.125 to 0.125
- gate_taps: bfloat16 [3, 3072], P(None, 'tp'), may hold values from -3.5 to 3.5
- up_taps: bfloat16 [3, 3072], P(None, 'tp'), may hold values from -3.5 to 3.5
- down_weight: bfloat16 [3072, 2048], P('tp'), may hold values from -0.109375 to 0.109375
- final_gain: float32 [2048], replicated, may hold values from 0.1 to 1.9
Outputs:
- layer_out: bfloat16 [12288, 2048], P(('sp', 'tp'))
All inputs are finite; a program needn't handle non-finite values.
Results may differ from a plain program's by a relative error of at most 0.012.
Values may be sent and summed in bfloat16 or wider, within the bound.
No kernel may reach another device: no remote copies, remote signals or barrier semaphores. Data moves between devices by JAX's collectives and lax.ppermute only.
A program may use at most 64 MiB of HBM per device.

v0:
```python
import math

import jax
import jax.numpy as jnp
from jax import lax
from jax.sharding import Mesh
from jax.sharding import PartitionSpec as P

D = 2048
HEADS = 8
HEAD = 256
KV_HEADS = 2
CONV = 3
TGT_DEV = 128
TP = ("tp_0", "tp_1")
SP_TP = ("sp", "tp_0", "tp_1")


EPS = 1e-06


def sent_to_all(shard, axis):
    copies = jnp.broadcast_to(shard, (lax.axis_size(axis), *shard.shape))
    return lax.all_to_all(copies, axis, split_axis=0, concat_axis=0, tiled=True)


def laid_out(tiles, dim):
    tiles = jnp.moveaxis(tiles, 0, dim)
    lengths = tiles.shape
    return tiles.reshape(*lengths[:dim], lengths[dim] * lengths[dim + 1], *lengths[dim + 2 :])


def gather_directly(shard, axis, dim):
    tiles = sent_to_all(shard, axis)
    return laid_out(tiles, dim)


def in_one_piece(arrays, axis, dim, along):
    both = jnp.concatenate(arrays, axis=along)
    result, at, done = (lax.all_gather(both, axis, axis=dim, tiled=True), 0, [])
    for a in arrays:
        done.append(lax.slice_in_dim(result, at, at + a.shape[along], axis=along))
        at += a.shape[along]
    return tuple(done)


def in_one_piece_2(arrays, axis, split_dim, concat_dim, along):
    columns = [a.reshape(*a.shape[:along], -1) for a in arrays]
    both = jnp.concatenate(columns, axis=along)
    result, at, done = (
        lax.all_to_all(both, axis, split_axis=split_dim, concat_axis=concat_dim, tiled=True),
        0,
        [],
    )
    for a, column in zip(arrays, columns):
        share = result[..., at : at + column.shape[along]]
        done.append(share.reshape(*share.shape[:along], *a.shape[along:]))
        at += column.shape[along]
    return tuple(done)


def cut_along(shard, dim, peers):
    lengths = shard.shape
    tiles = shard.reshape(*lengths[:dim], peers, lengths[dim] // peers, *lengths[dim + 1 :])
    return jnp.moveaxis(tiles, dim, 0)


def summed_on_arrival(shard, axis, dim):
    peers = lax.axis_size(axis)
    tiles = lax.all_to_all(cut_along(shard, dim, peers), axis, 0, 0, tiled=True)
    return jnp.sum(tiles, axis=0)


def all_blocks(shard, axes, turns):
    tiles = shard[None]
    for k in turns:
        tiles = lax.all_gather(tiles, axes[k], axis=0, tiled=True)
    carried = [lax.axis_size(axes[k]) for k in reversed(turns)]
    tiles = tiles.reshape(*carried, *shard.shape)
    turned = sorted(range(len(turns)), key=lambda place: turns[len(turns) - 1 - place])
    return tiles.transpose(*turned, *range(len(turns), tiles.ndim)).reshape(-1, *shard.shape)


def gather_axes(shard, axes, turns, dim):
    return laid_out(all_blocks(shard, axes, turns), dim)


def passed_along(shard, axis, by):
    peers = lax.axis_size(axis)
    pairs = [(i, i + by) for i in range(peers) if 0 <= i + by < peers]
    return lax.ppermute(shard, axis, pairs)


def normalize(values, gain):
    widened = values.astype(jnp.float32)
    scaled = widened * lax.rsqrt(jnp.mean(widened * widened, axis=-1, keepdims=True) + EPS)
    return (scaled * gain).astype(jnp.bfloat16)


def shards(
    target,
    source,
    query_gain,
    source_gain,
    query_weight,
    key_weight,
    value_weight,
    out_weight,
    mixer_gain,
    gate_weight,
    up_weight,
    gate_taps,
    up_taps,
    down_weight,
    final_gain,
):
    tp_count = lax.axis_size(TP)
    heads_here = HEADS // tp_count
    group_size = HEADS // KV_HEADS
    row_share = TGT_DEV // tp_count
    first_mine = lax.axis_index(TP) * row_share
    score_scale = HEAD ** (-0.5)
    normed = normalize(target, query_gain)
    own_query = jnp.dot(normed, query_weight, preferred_element_type=jnp.float32).astype(
        jnp.bfloat16
    )
    own_query = own_query.reshape(TGT_DEV, heads_here, HEAD).transpose(1, 0, 2)
    queries = gather_directly(own_query, TP, 0)
    grouped = queries.reshape(KV_HEADS, group_size * TGT_DEV, HEAD)
    source_normed = normalize(source, source_gain)
    key_rows = jnp.dot(source_normed, key_weight, preferred_element_type=jnp.float32).astype(
        jnp.bfloat16
    )
    value_rows = jnp.dot(source_normed, value_weight, preferred_element_type=jnp.float32).astype(
        jnp.bfloat16
    )
    keys_all, values_all = in_one_piece((key_rows, value_rows), "sp", 0, 1)
    total_keys = keys_all.shape[0]
    block_rows = math.gcd(total_keys, 512)
    block_count = total_keys // block_rows

    def absorb(block_index, state_now):
        running_max, running_sum, weighted = state_now
        first_row = block_index * block_rows
        key_heads = lax.dynamic_slice_in_dim(keys_all, first_row, block_rows, 0).reshape(
            block_rows, KV_HEADS, HEAD
        )
        value_heads = lax.dynamic_slice_in_dim(values_all, first_row, block_rows, 0).reshape(
            block_rows, KV_HEADS, HEAD
        )
        scores = (
            jnp.einsum("gqd,ngd->gqn", grouped, key_heads, preferred_element_type=jnp.float32)
            * score_scale
        )
        new_max = jnp.maximum(running_max, jnp.max(scores, axis=-1))
        shrink = jnp.exp(running_max - new_max)
        probabilities = jnp.exp(scores - new_max[..., None])
        running_sum = running_sum * shrink + jnp.sum(probabilities, axis=-1)
        weighted = weighted * shrink[..., None] + jnp.einsum(
            "gqn,ngd->gqd",
            probabilities.astype(jnp.bfloat16),
            value_heads,
            preferred_element_type=jnp.float32,
        )
        return (new_max, running_sum, weighted)

    start_state = (
        jnp.full((KV_HEADS, group_size * TGT_DEV), -1e30, jnp.float32),
        jnp.zeros((KV_HEADS, group_size * TGT_DEV), jnp.float32),
        jnp.zeros((KV_HEADS, group_size * TGT_DEV, HEAD), jnp.float32),
    )
    running_max, running_sum, weighted = lax.fori_loop(0, block_count, absorb, start_state)
    running_max = running_max.reshape(1, HEADS, TGT_DEV)
    running_sum = running_sum.reshape(1, HEADS, TGT_DEV)
    weighted = weighted.reshape(1, HEADS, TGT_DEV, HEAD)
    maxima, totals, partial_sums = in_one_piece_2((running_max, running_sum, weighted), TP, 1, 0, 3)
    highest = jnp.max(maxima, axis=0)
    factor = jnp.exp(maxima - highest)
    denominator = jnp.sum(factor * totals, axis=0)
    merged = (jnp.sum(factor[..., None] * partial_sums, axis=0) / denominator[..., None]).astype(
        jnp.bfloat16
    )
    out_heads = out_weight.reshape(heads_here, HEAD, D)
    row_block = merged
    projected = summed_on_arrival(
        jnp.einsum("hrd,hdc->rc", row_block, out_heads, preferred_element_type=jnp.float32), TP, 0
    )
    target_rows = lax.dynamic_slice_in_dim(target, first_mine, row_share, 0)
    residual_rows = (target_rows.astype(jnp.float32) + projected).astype(jnp.bfloat16)
    arrived = gather_axes(normalize(residual_rows, mixer_gain), ("tp_0", "tp_1"), (0, 1), 0)
    gate_up = jnp.stack(
        [
            jnp.dot(arrived, gate_weight, preferred_element_type=jnp.float32).astype(jnp.bfloat16),
            jnp.dot(arrived, up_weight, preferred_element_type=jnp.float32).astype(jnp.bfloat16),
        ]
    )
    tail_rows = gate_up[:, TGT_DEV - (CONV - 1) :, :]
    earlier = passed_along(tail_rows, "sp", 1)
    padded = jnp.concatenate([earlier, gate_up], axis=1).astype(jnp.float32)
    conv_taps = jnp.stack([gate_taps, up_taps]).astype(jnp.float32)
    mixed = conv_taps[:, 0:1, :] * padded[:, 0:TGT_DEV, :]
    for index_tap in range(1, CONV):
        mixed = (
            mixed
            + conv_taps[:, index_tap : index_tap + 1, :]
            * padded[:, index_tap : index_tap + TGT_DEV, :]
        )
    hidden = (jax.nn.silu(mixed[0]) * mixed[1]).astype(jnp.bfloat16)
    row_block = hidden
    mixer = summed_on_arrival(
        jnp.dot(row_block, down_weight, preferred_element_type=jnp.float32), TP, 0
    )
    return normalize(residual_rows.astype(jnp.float32) + mixer, final_gain)


def solution(mesh):
    split = Mesh(mesh.devices.reshape(mesh.shape["sp"], 4, 2), ("sp", "tp_0", "tp_1"))
    return jax.shard_map(
        shards,
        mesh=split,
        in_specs=(
            P("sp", None),
            P(SP_TP, None),
            P(),
            P(),
            P(None, TP),
            P(),
            P(),
            P(TP, None),
            P(),
            P(None, TP),
            P(None, TP),
            P(None, TP),
            P(None, TP),
            P(TP, None),
            P(),
        ),
        out_specs=P(SP_TP, None),
        check_vma=False,
    )
```

profile of v0, /device:TPU:64, one launch (start us, length us, event | category | flops | bytes accessed | tf_op | source)
XLA Modules:
  0.0 323.5 jit_solution(3041654211035776364)
XLA Ops:
  13.5 4.3 %all-to-all-start = ((bf16[8,1,128,256]{3,2,1,0:T(8,128)(2,1)}), bf16[8,1,128,256]{3,2,1,0:T(8,128)(2,1)S(1)}, u32[]{:S(2)}, u32[]{:S(2)}) async-start(bf16[8,1,128,256]{3,2,1,0:T(8,128)(2,1)} %broadcast_in_dim.19), calls=%async_computation | async-start | bytes 1048576 | tf_op jit(solution)/shard_map/all_to_all | solution.py:24
  17.8 127.8 %all-gather.3.cloned.1.call-done = bf16[3072,1024]{1,0:T(8,128)(2,1)} async-done(((bf16[32,1024]{1,0:T(8,128)(2,1)}), bf16[3072,1024]{1,0:T(8,128)(2,1)}) %all-gather.3.cloned.1.call-update) | async-done | bytes 6291472 | tf_op jit(solution)/shard_map/all_gather | solution.py:40
  145.6 5.9 %fusion.39 = (bf16[3072,512]{1,0:T(8,128)(2,1)}, bf16[3072,512]{1,0:T(8,128)(2,1)}) fusion(bf16[3072,1024]{1,0:T(8,128)(2,1)} %all-gather.3.cloned.1.call-done), kind=kLoop, calls=%fused_computation.84 | loop fusion | bytes 12582912 | tf_op jit(solution)/shard_map/slice | solution.py:42
  151.5 71.7 %while.18 = (s32[]{:T(128)}, f32[2,512]{1,0:T(2,128)S(1)}, f32[2,512]{1,0:T(2,128)S(1)}, f32[2,512,256]{2,1,0:T(8,128)}, bf16[3072,512]{1,0:T(8,128)(2,1)}, /*in...) while((s32[]{:T(128)}, f32[2,512]{1,0:T(2,128)S(1)}, ...), condition=%wide.region_5.0_spmd.clone, body=%wide.region_2.0_spmd.clone.sunk | while | flops 541856768 | bytes 18415844 | solution.py:172
  154.6 3.1 bitcast_reduce_fusion.2
  157.7 2.0 fusion.63
  159.9 3.3 %convolution_add_fusion.2 = f32[2,512,256]{2,1,0:T(8,128)} fusion(bf16[512,2,256]{0,2,1:T(8,128)(2,1)S(1)} %bitcast.84, f32[2,512,512]{2,1,0:T(8,128)} %get-tuple-element.282, f32[2,512,256]{2,1,0:T(8,128)} %get-tuple-element.300, f32[2,512]{1,0:T(2,128)S(1)} %fusion.62, f32[2,512]{1,0:T(2,128)S(1)} %get-tuple-element.285, pred[]{:T(512)S(6)} %compare.3), kind=kOutput, calls=%fused_computation.5.clone.1 | convolution fusion | flops 270794752 | bytes 4726785 | tf_op jit(solution)/shard_map/while/body/eval_jaxpr/gqn,ngd->gqd/dot_general | solution.py:159
  166.3 3.1 bitcast_reduce_fusion.2
  169.4 2.0 fusion.63
  171.6 3.6 %convolution_add_fusion.2 = f32[2,512,256]{2,1,0:T(8,128)} fusion(bf16[512,2,256]{0,2,1:T(8,128)(2,1)S(1)} %bitcast.84, f32[2,512,512]{2,1,0:T(8,128)} %get-tuple-element.282, f32[2,512,256]{2,1,0:T(8,128)} %get-tuple-element.300, f32[2,512]{1,0:T(2,128)S(1)} %fusion.62, f32[2,512]{1,0:T(2,128)S(1)} %get-tuple-element.285, pred[]{:T(512)S(6)} %compare.3), kind=kOutput, calls=%fused_computation.5.clone.1 | convolution fusion | flops 270794752 | bytes 4726785 | tf_op jit(solution)/shard_map/while/body/eval_jaxpr/gqn,ngd->gqd/dot_general | solution.py:159
  178.3 3.1 bitcast_reduce_fusion.2
  181.4 2.0 fusion.63
  183.6 3.6 %convolution_add_fusion.2 = f32[2,512,256]{2,1,0:T(8,128)} fusion(bf16[512,2,256]{0,2,1:T(8,128)(2,1)S(1)} %bitcast.84, f32[2,512,512]{2,1,0:T(8,128)} %get-tuple-element.282, f32[2,512,256]{2,1,0:T(8,128)} %get-tuple-element.300, f32[2,512]{1,0:T(2,128)S(1)} %fusion.62, f32[2,512]{1,0:T(2,128)S(1)} %get-tuple-element.285, pred[]{:T(512)S(6)} %compare.3), kind=kOutput, calls=%fused_computation.5.clone.1 | convolution fusion | flops 270794752 | bytes 4726785 | tf_op jit(solution)/shard_map/while/body/eval_jaxpr/gqn,ngd->gqd/dot_general | solution.py:159
  190.3 3.1 bitcast_reduce_fusion.2
  193.4 2.0 fusion.63
  195.6 3.6 %convolution_add_fusion.2 = f32[2,512,256]{2,1,0:T(8,128)} fusion(bf16[512,2,256]{0,2,1:T(8,128)(2,1)S(1)} %bitcast.84, f32[2,512,512]{2,1,0:T(8,128)} %get-tuple-element.282, f32[2,512,256]{2,1,0:T(8,128)} %get-tuple-element.300, f32[2,512]{1,0:T(2,128)S(1)} %fusion.62, f32[2,512]{1,0:T(2,128)S(1)} %get-tuple-element.285, pred[]{:T(512)S(6)} %compare.3), kind=kOutput, calls=%fused_computation.5.clone.1 | convolution fusion | flops 270794752 | bytes 4726785 | tf_op jit(solution)/shard_map/while/body/eval_jaxpr/gqn,ngd->gqd/dot_general | solution.py:159
  202.3 3.1 bitcast_reduce_fusion.2
  205.4 2.0 fusion.63
  207.6 3.6 %convolution_add_fusion.2 = f32[2,512,256]{2,1,0:T(8,128)} fusion(bf16[512,2,256]{0,2,1:T(8,128)(2,1)S(1)} %bitcast.84, f32[2,512,512]{2,1,0:T(8,128)} %get-tuple-element.282, f32[2,512,256]{2,1,0:T(8,128)} %get-tuple-element.300, f32[2,512]{1,0:T(2,128)S(1)} %fusion.62, f32[2,512]{1,0:T(2,128)S(1)} %get-tuple-element.285, pred[]{:T(512)S(6)} %compare.3), kind=kOutput, calls=%fused_computation.5.clone.1 | convolution fusion | flops 270794752 | bytes 4726785 | tf_op jit(solution)/shard_map/while/body/eval_jaxpr/gqn,ngd->gqd/dot_general | solution.py:159
  214.3 3.1 bitcast_reduce_fusion.2
  217.4 2.0 fusion.63
  219.6 3.6 %convolution_add_fusion.2 = f32[2,512,256]{2,1,0:T(8,128)} fusion(bf16[512,2,256]{0,2,1:T(8,128)(2,1)S(1)} %bitcast.84, f32[2,512,512]{2,1,0:T(8,128)} %get-tuple-element.282, f32[2,512,256]{2,1,0:T(8,128)} %get-tuple-element.300, f32[2,512]{1,0:T(2,128)S(1)} %fusion.62, f32[2,512]{1,0:T(2,128)S(1)} %get-tuple-element.285, pred[]{:T(512)S(6)} %compare.3), kind=kOutput, calls=%fused_computation.5.clone.1 | convolution fusion | flops 270794752 | bytes 4726785 | tf_op jit(solution)/shard_map/while/body/eval_jaxpr/gqn,ngd->gqd/dot_general | solution.py:159
  223.9 3.1 pad_maximum_fusion
  227.1 2.6 copy.68
  229.7 20.1 %all_to_all.27 = f32[1,8,128,258]{2,0,3,1:T(1,128)S(1)} all-to-all(f32[1,8,128,258]{2,0,3,1:T(1,128)S(1)} %copy.68), channel_id=1, replica_groups=mesh['sp'=96,'tp_0'=4,'tp_1'=2] {'tp_0','tp_1'}, dimensions={1} | all-to-all | bytes 2113536 | tf_op jit(solution)/shard_map/all_to_all | solution.py:51
  252.4 3.7 %all-to-all-start.2 = ((f32[8,16,2048]{2,1,0:T(8,128)}), f32[8,16,2048]{2,1,0:T(8,128)S(1)}, u32[]{:S(2)}, u32[]{:S(2)}) async-start(f32[8,16,2048]{2,1,0:T(8,128)} %fusion.17), calls=%async_computation.2 | async-start | bytes 2097152 | tf_op jit(solution)/shard_map/all_to_all | solution.py:70
  256.1 15.8 %all-to-all-done.2 = f32[8,16,2048]{2,1,0:T(8,128)S(1)} async-done(((f32[8,16,2048]{2,1,0:T(8,128)}), f32[8,16,2048]{2,1,0:T(8,128)S(1)}, u32[]{:S(2)}, u32[]{:S(2)}) %all-to-all-start.2) | async-done | bytes 1048608 | tf_op jit(solution)/shard_map/all_to_all | solution.py:70
  273.2 12.3 %all-gather = bf16[64,2048]{1,0:T(8,128)(2,1)S(1)} all-gather(bf16[16,2048]{1,0:T(8,128)(2,1)S(1)} %fusion.29), channel_id=2, replica_groups=mesh['sp'=96,'tp_0'=4,'tp_1'=2] {'tp_0'}, dimensions={0}, use_global_device_ids=true | all-gather | bytes 327680 | tf_op jit(solution)/shard_map/all_gather | solution.py:77
  285.5 2.3 all_gather.11
  288.8 2.4 collective-permute-start
  291.2 5.3 %collective-permute-done = bf16[2,2,384]{2,1,0:T(2,128)(2,1)S(1)} collective-permute-done((bf16[2,2,384]{2,1,0:T(2,128)(2,1)S(1)}, bf16[2,2,384]{2,1,0:T(2,128)(2,1)S(1)}, u32[]{:S(2)}, u32[]{:S(2)}) %collective-permute-start) | collective-permute-done | bytes 3104 | tf_op jit(solution)/shard_map/ppermute | solution.py:91
  297.2 18.5 %all_to_all.28 = f32[8,16,2048]{2,1,0:T(8,128)S(1)} all-to-all(f32[8,16,2048]{2,1,0:T(8,128)S(1)} %fusion.9), channel_id=1, replica_groups=mesh['sp'=96,'tp_0'=4,'tp_1'=2] {'tp_0','tp_1'}, dimensions={0} | all-to-all | bytes 2097152 | tf_op jit(solution)/shard_map/all_to_all | solution.py:70
  (132 shorter events, 33.9 us)
Async XLA Ops:
  6.5 1.7 copy-start
  6.5 3.1 copy-start.7
  6.5 3.1 copy-start.10
  6.5 139.1 %all-gather.3.cloned.1.call-start = ((), (), s32[]{:S(2)}) async-start(), calls=%async_computation.4 | async-start | bytes 6356992 | tf_op jit(solution)/shard_map/all_gather | solution.py:40
  6.5 3.1 copy-start.3
  8.2 2.7 copy-start.9
  8.2 2.9 copy-start.15
  13.5 138.0 %all-to-all-start = ((bf16[8,1,128,256]{3,2,1,0:T(8,128)(2,1)}), bf16[8,1,128,256]{3,2,1,0:T(8,128)(2,1)S(1)}, u32[]{:S(2)}, u32[]{:S(2)}) async-start(bf16[8,1,128,256]{3,2,1,0:T(8,128)(2,1)} %broadcast_in_dim.19), calls=%async_computation | async-start | bytes 1048576 | tf_op jit(solution)/shard_map/all_to_all | solution.py:24
  151.5 0.8 copy-start.1
  159.9 3.4 %copy-start.2 = (bf16[2,512,256]{2,1,0:T(8,128)(2,1)S(1)}, bf16[2,512,256]{2,1,0:T(8,128)(2,1)}, u32[]{:S(2)}) copy-start(bf16[2,512,256]{2,1,0:T(8,128)(2,1)} %copy-done.1) | copy-start | bytes 1572868 | tf_op jit(solution)/shard_map/while
  163.3 0.8 copy-start.1
  171.6 3.6 %copy-start.2 = (bf16[2,512,256]{2,1,0:T(8,128)(2,1)S(1)}, bf16[2,512,256]{2,1,0:T(8,128)(2,1)}, u32[]{:S(2)}) copy-start(bf16[2,512,256]{2,1,0:T(8,128)(2,1)} %copy-done.1) | copy-start | bytes 1572868 | tf_op jit(solution)/shard_map/while
  175.3 0.8 copy-start.1
  183.6 3.6 %copy-start.2 = (bf16[2,512,256]{2,1,0:T(8,128)(2,1)S(1)}, bf16[2,512,256]{2,1,0:T(8,128)(2,1)}, u32[]{:S(2)}) copy-start(bf16[2,512,256]{2,1,0:T(8,128)(2,1)} %copy-done.1) | copy-start | bytes 1572868 | tf_op jit(solution)/shard_map/while
  187.2 0.8 copy-start.1
  195.6 3.6 %copy-start.2 = (bf16[2,512,256]{2,1,0:T(8,128)(2,1)S(1)}, bf16[2,512,256]{2,1,0:T(8,128)(2,1)}, u32[]{:S(2)}) copy-start(bf16[2,512,256]{2,1,0:T(8,128)(2,1)} %copy-done.1) | copy-start | bytes 1572868 | tf_op jit(solution)/shard_map/while
  199.2 0.8 copy-start.1
  207.6 3.6 %copy-start.2 = (bf16[2,512,256]{2,1,0:T(8,128)(2,1)S(1)}, bf16[2,512,256]{2,1,0:T(8,128)(2,1)}, u32[]{:S(2)}) copy-start(bf16[2,512,256]{2,1,0:T(8,128)(2,1)} %copy-done.1) | copy-start | bytes 1572868 | tf_op jit(solution)/shard_map/while
  211.2 0.8 copy-start.1
  219.6 3.6 %copy-start.2 = (bf16[2,512,256]{2,1,0:T(8,128)(2,1)S(1)}, bf16[2,512,256]{2,1,0:T(8,128)(2,1)}, u32[]{:S(2)}) copy-start(bf16[2,512,256]{2,1,0:T(8,128)(2,1)} %copy-done.1) | copy-start | bytes 1572868 | tf_op jit(solution)/shard_map/while
  249.8 1.2 copy-start.8
  251.0 5.1 %copy-start.13 = (bf16[3,384]{1,0:T(4,128)(2,1)S(1)}, bf16[3,384]{1,0:T(4,128)(2,1)}, u32[]{:S(2)}) copy-start(bf16[3,384]{1,0:T(4,128)(2,1)} %param.29) | copy-start | bytes 6916
  251.0 5.1 %copy-start.14 = (bf16[3,384]{1,0:T(4,128)(2,1)S(1)}, bf16[3,384]{1,0:T(4,128)(2,1)}, u32[]{:S(2)}) copy-start(bf16[3,384]{1,0:T(4,128)(2,1)} %param.28) | copy-start | bytes 6916
  252.4 20.7 %copy-start.11 = (f32[2048]{0:T(1024)S(1)}, f32[2048]{0:T(1024)}, u32[]{:S(2)}) copy-start(f32[2048]{0:T(1024)} %param.25) | copy-start | bytes 24580
  252.4 19.6 %all-to-all-start.2 = ((f32[8,16,2048]{2,1,0:T(8,128)}), f32[8,16,2048]{2,1,0:T(8,128)S(1)}, u32[]{:S(2)}, u32[]{:S(2)}) async-start(f32[8,16,2048]{2,1,0:T(8,128)} %fusion.17), calls=%async_computation.2 | async-start | bytes 2097152 | tf_op jit(solution)/shard_map/all_to_all | solution.py:70
  272.0 15.9 %copy-start.5 = (bf16[2048,384]{1,0:T(8,128)(2,1)S(1)}, bf16[2048,384]{1,0:T(8,128)(2,1)}, u32[]{:S(2)}) copy-start(bf16[2048,384]{1,0:T(8,128)(2,1)} %param.26) | copy-start | bytes 4718596
  285.5 2.8 copy-start.6
  288.7 8.0 %copy-start.4 = (bf16[384,2048]{1,0:T(8,128)(2,1)S(1)}, bf16[384,2048]{1,0:T(8,128)(2,1)}, u32[]{:S(2)}) copy-start(bf16[384,2048]{1,0:T(8,128)(2,1)} %param.30) | copy-start | bytes 4718596
  288.8 7.7 %collective-permute-start = (bf16[2,2,384]{2,1,0:T(2,128)(2,1)S(1)}, bf16[2,2,384]{2,1,0:T(2,128)(2,1)S(1)}, u32[]{:S(2)}, u32[]{:S(2)}) collective-permute-start(bf16[2,2,384]{2,1,0:T(2,128)(2,1)S(1)} %pad_maximum_fusion.3), channel_id=1, source_target_pairs={{0,8},{8,16},{16,24},{24,32},{32,40},{40,48},{48,56},{56,64},{64,7... | collective-permute-start | bytes 9224 | tf_op jit(solution)/shard_map/ppermute | solution.py:91
  297.2 18.7 %copy-start.12 = (f32[2048]{0:T(1024)S(1)}, f32[2048]{0:T(1024)}, u32[]{:S(2)}) copy-start(f32[2048]{0:T(1024)} %param.31) | copy-start | bytes 24580
Sparse Core Ops, SparseCore 0:
  11.1 134.4 all-gather.2
where the time goes:
time: 325 us; the launch traced here: 323 us
  waiting for transfers between devices  149 us (46%)
  blocking collectives  53.2 us (16%)
  matrix products  46.1 us (14%)
  local copies, waits for them, and re-layouts  31.3 us (10%)
  other arithmetic  19.7 us (6%)
  between operations  13.7 us (4%)
  starting transfers between devices  10.4 us (3%)
    all_gather x1, waiting for transfers between devices, in_one_piece(): result, at, done = (lax.all_gather(both, axis, axis=dim, tiled=True), 0, [])  128 us
    dot_general x6, matrix products, absorb(): jnp.einsum('gqn,ngd->gqd', probabilities.astype(jnp.bfloat16), value_head...  21.4 us
    all_to_all x1, blocking collectives, in_one_piece_2(): lax.all_to_all(both, axis, split_axis=split_dim, concat_axis=concat_dim,...  20.1 us
    all_to_all x1, blocking collectives, summed_on_arrival(): tiles = lax.all_to_all(cut_along(shard, dim, peers), axis, 0, 0, tiled=True)  18.5 us
    dot_general x6, matrix products, absorb(): jnp.einsum('gqd,ngd->gqn', grouped, key_heads, preferred_element_type=jnp...  18.5 us
    all_to_all x1, waiting for transfers between devices, summed_on_arrival(): tiles = lax.all_to_all(cut_along(shard, dim, peers), axis, 0, 0, tiled=True)  15.8 us
    all_gather x2, blocking collectives, all_blocks(): tiles = lax.all_gather(tiles, axes[k], axis=0, tiled=True)  14.6 us
    reduce_sum x6, other arithmetic, absorb(): running_sum = running_sum * shrink + jnp.sum(probabilities, axis=-1)  11.7 us
  transfers between devices with their start and end apart: 4, of which 3 were waited for; matrix products, arithmetic and copies ran while one was open for 3% of the time, Pallas kernels for 0%

commit v1 on v0

v1 whole, which is shorter than its diff:
```python
import functools

import jax
import jax.numpy as jnp
from jax import lax
from jax.experimental import pallas as pl
from jax.experimental.pallas import tpu as pltpu
from jax.sharding import Mesh
from jax.sharding import PartitionSpec as P

D = 2048
HEADS = 8
HEAD = 256
KV_HEADS = 2
CONV = 3
TGT_DEV = 128
PAD = 16
EPS = 1e-06

M = 2
SP = ("z", "q", "m")
TP = ("g", "xp", "c")
CHIPS = ("g", "xp")
SLICES = ("m", "xp", "c")
BLOCK = 16
HALF = TGT_DEV // 2
bf16 = jnp.bfloat16
f32 = jnp.float32


def normalize(values, gain):
    widened = values.astype(f32)
    scaled = widened * lax.rsqrt(jnp.mean(widened * widened, axis=-1, keepdims=True) + EPS)
    return (scaled * gain).astype(bf16)


def attend_body(q_ref, kv_ref, o_ref):
    k = kv_ref[:, :HEAD]
    v = kv_ref[:, HEAD:]
    row = lax.broadcasted_iota(jnp.int32, (PAD, HEAD), 0)
    for pair in range(0, q_ref.shape[0], 2):
        q = q_ref[pair : pair + 2].reshape(2 * TGT_DEV, HEAD)
        s = lax.dot_general(q, k, (((1,), (1,)), ((), ())), preferred_element_type=f32)
        top = jnp.max(s, axis=1, keepdims=True)
        p = jnp.exp(s - top)
        total = jnp.sum(p, axis=1, keepdims=True)
        o = jnp.dot(p.astype(bf16), v, preferred_element_type=f32) / total
        o = o.astype(bf16)
        lse = top + jnp.log(total)
        for core in range(2):
            starts = [
                head * TGT_DEV + (2 * x + core) * BLOCK
                for head in (core, 1 - core)
                for x in range(4)
            ]
            for at, start in enumerate(starts):
                o_ref[pair + core, at * BLOCK : (at + 1) * BLOCK, :] = o[start : start + BLOCK]
            column = jnp.concatenate([lse[start : start + BLOCK] for start in starts], axis=0)
            line = jnp.broadcast_to(column, (TGT_DEV, TGT_DEV)).T[:1]
            hi = line.astype(bf16).astype(f32)
            mid = (line - hi).astype(bf16).astype(f32)
            lo = line - hi - mid
            first = jnp.concatenate([hi, mid], axis=1)
            second = jnp.concatenate([lo, jnp.zeros_like(lo)], axis=1)
            tile = jnp.where(row == 0, first, jnp.where(row == 1, second, 0.0))
            o_ref[pair + core, TGT_DEV:, :] = tile.astype(bf16)


def attend(queries, kv, step=4):
    blocks = queries.shape[0]
    return pl.pallas_call(
        attend_body,
        grid=(blocks // step,),
        in_specs=[
            pl.BlockSpec((step, TGT_DEV, HEAD), lambda i: (i, 0, 0)),
            pl.BlockSpec(kv.shape, lambda i: (0, 0)),
        ],
        out_specs=pl.BlockSpec((step, TGT_DEV + PAD, HEAD), lambda i: (i, 0, 0)),
        out_shape=jax.ShapeDtypeStruct((blocks, TGT_DEV + PAD, HEAD), bf16),
    )(queries, kv)


def merge_body(parts_ref, own_ref, other_ref, o_ref):
    count = parts_ref.shape[0]
    tail = parts_ref[:, TGT_DEV:, :].astype(f32)
    lse = tail[:, 0, :TGT_DEV] + tail[:, 0, TGT_DEV:] + tail[:, 1, :TGT_DEV]
    weight = jnp.exp(lse - jnp.max(lse, axis=0, keepdims=True))
    weight = (weight / jnp.sum(weight, axis=0, keepdims=True)).T
    merged = parts_ref[0, :TGT_DEV, :].astype(f32) * weight[:, :1]
    for t in range(1, count):
        merged = merged + parts_ref[t, :TGT_DEV, :].astype(f32) * weight[:, t : t + 1]
    merged = merged.astype(bf16)
    projected = jnp.dot(merged[:HALF], own_ref[...], preferred_element_type=f32)
    projected += jnp.dot(merged[HALF:], other_ref[...], preferred_element_type=f32)
    o_ref[...] = projected.astype(bf16)


def merge_project(parts, own, other):
    return pl.pallas_call(
        merge_body,
        out_shape=jax.ShapeDtypeStruct((HALF, D), bf16),
    )(parts, own, other)


def exchanged(array, axes):
    return lax.all_to_all(array, axes, 0, 0, tiled=True)


def sent_to_all(shard, axes):
    count = lax.axis_size(axes)
    return exchanged(jnp.broadcast_to(shard, (count, *shard.shape)), axes)


def summed_rows(partial):
    tiles = exchanged(partial.reshape(HALF // BLOCK, BLOCK, D), CHIPS)
    return jnp.sum(tiles.astype(f32), axis=0)


def other_core(array):
    return lax.ppermute(array, "c", [(0, 1), (1, 0)])


def from_last_line(array):
    lines = lax.axis_size(SP)
    axes = (*SP, "c")
    return lax.ppermute(array, axes, [(2 * i + 1, 2 * i + 2) for i in range(lines - 1)])


def shards(
    target,
    source,
    query_gain,
    source_gain,
    query_weight,
    key_weight,
    value_weight,
    out_weight,
    mixer_gain,
    gate_weight,
    up_weight,
    gate_taps,
    up_taps,
    down_weight,
    final_gain,
):
    first_mine = lax.axis_index(TP) * BLOCK
    source_normed = normalize(source, source_gain)
    key_rows = jnp.dot(source_normed, key_weight, preferred_element_type=f32).astype(bf16)
    value_rows = jnp.dot(source_normed, value_weight, preferred_element_type=f32).astype(bf16)
    rows = source.shape[0]
    by_head = jnp.stack(
        [
            jnp.concatenate([key_rows[:, :HEAD], value_rows[:, :HEAD]], axis=1),
            jnp.concatenate([key_rows[:, HEAD:], value_rows[:, HEAD:]], axis=1),
        ]
    )
    quads = lax.axis_size("q")
    to_send = jnp.broadcast_to(by_head[:, None], (KV_HEADS, quads, rows, 2 * HEAD))
    near = exchanged(to_send.reshape(KV_HEADS * quads, rows, 2 * HEAD), ("g", "q"))
    near = near.reshape(KV_HEADS * quads * rows, 2 * HEAD)
    near, target, out_weight, gate_weight, up_weight, gate_taps, up_taps, down_weight = (
        lax.optimization_barrier(
            (near, target, out_weight, gate_weight, up_weight, gate_taps, up_taps, down_weight)
        )
    )
    kv = lax.all_gather(near, "z", axis=0, tiled=True)

    normed = normalize(target, query_gain)
    own_query = jnp.dot(normed, query_weight, preferred_element_type=f32).astype(bf16)
    own_query = own_query * jnp.asarray(HEAD ** (-0.5), bf16)
    queries = sent_to_all(own_query, SLICES)
    out_other = other_core(out_weight)
    gate_other = other_core(gate_weight)
    up_other = other_core(up_weight)
    down_other = other_core(down_weight)
    taps = jnp.stack([gate_taps, up_taps])
    taps = jnp.concatenate([taps, other_core(taps)], axis=2).astype(f32)
    queries, out_other, gate_other, up_other, down_other, taps = lax.optimization_barrier(
        (queries, out_other, gate_other, up_other, down_other, taps)
    )

    parts = exchanged(attend(queries, kv), SLICES)
    projected = summed_rows(merge_project(parts, out_weight, out_other))
    target_rows = lax.dynamic_slice_in_dim(target, first_mine, BLOCK, 0)
    residual_rows = (target_rows.astype(f32) + projected).astype(bf16)
    arrived = sent_to_all(normalize(residual_rows, mixer_gain), CHIPS).reshape(HALF, D)
    gate_up = jnp.stack(
        [
            jnp.concatenate(
                [
                    jnp.dot(arrived, own, preferred_element_type=f32).astype(bf16),
                    jnp.dot(arrived, other, preferred_element_type=f32).astype(bf16),
                ],
                axis=1,
            )
            for own, other in ((gate_weight, gate_other), (up_weight, up_other))
        ]
    )
    width = gate_up.shape[2]
    blocks = gate_up.reshape(2, HALF // BLOCK, BLOCK, width)
    tails = blocks[:, :, BLOCK - (CONV - 1) :, :]
    across = other_core(tails)
    before = from_last_line(tails[:, -1:])
    shifted = jnp.concatenate([before, across[:, :-1]], axis=1)
    earlier = jnp.where(lax.axis_index("c") == 0, shifted, across)
    earlier = jnp.concatenate([earlier[..., width // 2 :], earlier[..., : width // 2]], axis=3)
    padded = jnp.concatenate([earlier, blocks], axis=2).astype(f32)
    mixed = taps[:, None, 0:1, :] * padded[:, :, 0:BLOCK, :]
    for tap in range(1, CONV):
        mixed = mixed + taps[:, None, tap : tap + 1, :] * padded[:, :, tap : tap + BLOCK, :]
    hidden = (jax.nn.silu(mixed[0]) * mixed[1]).astype(bf16).reshape(HALF, width)
    partial = jnp.dot(hidden[:, : width // 2], down_weight, preferred_element_type=f32)
    partial += jnp.dot(hidden[:, width // 2 :], down_other, preferred_element_type=f32)
    mixer = summed_rows(partial.astype(bf16))
    return normalize(residual_rows.astype(f32) + mixer, final_gain)


def solution(mesh):
    lines = mesh.shape["sp"]
    devices = mesh.devices.reshape(lines // 8, 8 // M, M, 2, 2, 2)
    split = Mesh(devices, SP + TP)
    whole = SP + TP
    return jax.shard_map(
        shards,
        mesh=split,
        in_specs=(
            P(SP, None),
            P(whole, None),
            P(),
            P(),
            P(None, TP),
            P(),
            P(),
            P(TP, None),
            P(),
            P(None, TP),
            P(None, TP),
            P(None, TP),
            P(None, TP),
            P(TP, None),
            P(),
        ),
        out_specs=P(whole, None),
        check_vma=False,
    )
```

time: 325 us -> 182 us (0.56)
  the two profiles are of different devices: /device:TPU:64 before, /device:TPU:24 now
where the time goes in v1:
time: 182 us; the launch traced here: 181 us
  waiting for transfers between devices  61.8 us (34%)
  blocking collectives  43.8 us (24%)
  starting transfers between devices  31.4 us (17%)
  between operations  13.8 us (8%)
  Pallas kernels  12.2 us (7%)
  matrix products  11.5 us (6%)
  local copies, waits for them, and re-layouts  3.34 us (2%)
  other arithmetic  2.97 us (2%)
    all_to_all x3, blocking collectives, exchanged(): return lax.all_to_all(array, axes, 0, 0, tiled=True)  43.8 us
    all_gather x1, waiting for transfers between devices, shards(): kv = lax.all_gather(near, 'z', axis=0, tiled=True)  41.3 us
    all_to_all x3, waiting for transfers between devices, exchanged(): return lax.all_to_all(array, axes, 0, 0, tiled=True)  18.7 us
    ppermute x6, starting transfers between devices, other_core(): return lax.ppermute(array, 'c', [(0, 1), (1, 0)])  16.8 us
    all_to_all x3, starting transfers between devices, exchanged(): return lax.all_to_all(array, axes, 0, 0, tiled=True)  13.3 us
    pallas_call x1, Pallas kernels, attend(): pl.pallas_call(attend_body, grid=(blocks // step,), in_specs=[pl.BlockSpe...  9.04 us
  transfers between devices with their start and end apart: 11, of which 6 were waited for; matrix products, arithmetic and copies ran while one was open for 1% of the time, Pallas kernels for 0%

profile of v1, /device:TPU:24, one launch (start us, length us, event | category | flops | bytes accessed | tf_op | source)
XLA Modules:
  0.0 180.8 jit_solution(13558431987997408716)
XLA Ops:
  6.6 1.2 fusion.10
  8.2 1.4 convolution_convert_fusion.6
  10.2 19.9 %all_to_all.30 = bf16[8,32,512]{2,1,0:T(8,128)(2,1)} all-to-all(bf16[8,32,512]{2,1,0:T(8,128)(2,1)S(1)} %bitcast.64), channel_id=1, replica_groups=mesh['z'=12,'q'=4,'m'=2,'g'=2,'xp'=2,'c'=2] {'g','q'}, dimensions={0} | all-to-all | bytes 524288 | tf_op jit(solution)/shard_map/all_to_all | solution.py:106
  30.2 1.9 %collective-permute-start.1 = (bf16[2048,384]{1,0:T(8,128)(2,1)}, bf16[2048,384]{1,0:T(8,128)(2,1)}, u32[]{:S(2)}, u32[]{:S(2)}) collective-permute-start(bf16[2048,384]{1,0:T(8,128)(2,1)} %param.24), channel_id=1, source_target_pairs={{0,1},{1,0},{2,3},{3,2},{4,5},{5,4},{6,7},{7,6},{8,9},{9,8},{10,11... | collective-permute-start | bytes 4718600 | tf_op jit(solution)/shard_map/ppermute | solution.py:120
  32.1 2.4 %collective-permute-start.2 = (bf16[2048,384]{1,0:T(8,128)(2,1)}, bf16[2048,384]{1,0:T(8,128)(2,1)}, u32[]{:S(2)}, u32[]{:S(2)}) collective-permute-start(bf16[2048,384]{1,0:T(8,128)(2,1)} %param.25), channel_id=1, source_target_pairs={{0,1},{1,0},{2,3},{3,2},{4,5},{5,4},{6,7},{7,6},{8,9},{9,8},{10,11... | collective-permute-start | bytes 4718600 | tf_op jit(solution)/shard_map/ppermute | solution.py:120
  34.5 1.9 %collective-permute-start.3 = (bf16[384,2048]{1,0:T(8,128)(2,1)}, bf16[384,2048]{1,0:T(8,128)(2,1)}, u32[]{:S(2)}, u32[]{:S(2)}) collective-permute-start(bf16[384,2048]{1,0:T(8,128)(2,1)} %param.28), channel_id=1, source_target_pairs={{0,1},{1,0},{2,3},{3,2},{4,5},{5,4},{6,7},{7,6},{8,9},{9,8},{10,11... | collective-permute-start | bytes 4718600 | tf_op jit(solution)/shard_map/ppermute | solution.py:120
  36.5 2.4 %collective-permute-start = (bf16[256,2048]{1,0:T(8,128)(2,1)}, bf16[256,2048]{1,0:T(8,128)(2,1)}, u32[]{:S(2)}, u32[]{:S(2)}) collective-permute-start(bf16[256,2048]{1,0:T(8,128)(2,1)} %own_ref), channel_id=1, source_target_pairs={{0,1},{1,0},{2,3},{3,2},{4,5},{5,4},{6,7},{7,6},{8,9},{9,8},{10,11... | collective-permute-start | bytes 3145736 | tf_op jit(solution)/shard_map/ppermute | solution.py:120
  39.1 1.6 fusion.1
  40.7 0.8 broadcast_in_dim.7
  41.6 5.7 %all-to-all-start.1 = ((bf16[8,128,256]{2,1,0:T(8,128)(2,1)}), bf16[8,128,256]{2,1,0:T(8,128)(2,1)S(1)}, u32[]{:S(2)}, u32[]{:S(2)}) async-start(bf16[8,128,256]{2,1,0:T(8,128)(2,1)} %broadcast_in_dim.7), calls=%async_computation.1 | async-start | bytes 1048576 | tf_op jit(solution)/shard_map/all_to_all | solution.py:106
  47.2 2.0 %collective-permute-start.4 = (bf16[2,3,384]{2,1,0:T(4,128)(2,1)S(1)}, bf16[2,3,384]{2,1,0:T(4,128)(2,1)S(1)}, u32[]{:S(2)}, u32[]{:S(2)}) collective-permute-start(bf16[2,3,384]{2,1,0:T(4,128)(2,1)S(1)} %pad_maximum_fusion.5), channel_id=1, source_target_pairs={{0,1},{1,0},{2,3},{3,2},{4,5},{5,4},{6,7},{7,6},{8,9},{9,8},{10,11... | collective-permute-start | bytes 13832 | tf_op jit(solution)/shard_map/ppermute | solution.py:120
  49.3 1.0 collective-permute-done.4
  50.3 5.2 %all-to-all-done.1.q_ref = bf16[8,128,256]{2,1,0:T(8,128)(2,1)S(1)} async-done(((bf16[8,128,256]{2,1,0:T(8,128)(2,1)}), bf16[8,128,256]{2,1,0:T(8,128)(2,1)S(1)}, u32[]{:S(2)}, u32[]{:S(2)}) %all-to-all-start.1) | async-done | bytes 524320 | tf_op jit(solution)/shard_map/all_to_all | solution.py:106
  55.5 41.3 %all-gather.2.cloned.1.call-done.kv_ref = bf16[3072,512]{1,0:T(8,128)(2,1)} async-done(((bf16[256,512]{1,0:T(8,128)(2,1)}), bf16[3072,512]{1,0:T(8,128)(2,1)}) %all-gather.2.cloned.1.call-update) | async-done | bytes 3145744 | tf_op jit(solution)/shard_map/all_gather | solution.py:166
  96.8 9.0 %shard_map.145 = bf16[8,144,256]{2,1,0:T(8,128)(2,1)} custom-call(bf16[8,128,256]{2,1,0:T(8,128)(2,1)} %copy-done.2, bf16[3072,512]{1,0:T(8,128)(2,1)} %all-gather.2.cloned.1.call-done.kv_ref), custom_call_target="tpu_custom_call" | custom-call | tf_op jit(solution)/shard_map/pallas_call | solution.py:71
  105.9 14.0 %all_to_all.31.parts_ref = bf16[8,144,256]{2,1,0:T(8,128)(2,1)} all-to-all(bf16[8,144,256]{2,1,0:T(8,128)(2,1)} %shard_map.145), channel_id=1, replica_groups=mesh['z'=12,'q'=4,'m'=2,'g'=2,'xp'=2,'c'=2] {'m','xp','c'}, dimensions={0} | all-to-all | bytes 1179648 | tf_op jit(solution)/shard_map/all_to_all | solution.py:106
  119.9 3.2 %shard_map.146 = bf16[64,2048]{1,0:T(8,128)(2,1)} custom-call(bf16[8,144,256]{2,1,0:T(8,128)(2,1)} %all_to_all.31.parts_ref, bf16[256,2048]{1,0:T(8,128)(2,1)} %own_ref, bf16[256,2048]{1,0:T(8,128)(2,1)} %collective-permute-done.other_ref), custom_call_target="tpu_custom_call" | custom-call | tf_op jit(solution)/shard_map/pallas_call | solution.py:99
  123.0 4.2 %all-to-all-start.3 = ((bf16[4,16,2048]{2,1,0:T(8,128)(2,1)}), bf16[4,16,2048]{2,1,0:T(8,128)(2,1)S(1)}, u32[]{:S(2)}, u32[]{:S(2)}) async-start(bf16[4,16,2048]{2,1,0:T(8,128)(2,1)} %bitcast.62), calls=%async_computation.3 | async-start | bytes 524288 | tf_op jit(solution)/shard_map/all_to_all | solution.py:106
  127.3 6.8 %all-to-all-done.3 = bf16[4,16,2048]{2,1,0:T(8,128)(2,1)S(1)} async-done(((bf16[4,16,2048]{2,1,0:T(8,128)(2,1)}), bf16[4,16,2048]{2,1,0:T(8,128)(2,1)S(1)}, u32[]{:S(2)}, u32[]{:S(2)}) %all-to-all-start.3) | async-done | bytes 262176 | tf_op jit(solution)/shard_map/all_to_all | solution.py:106
  134.4 0.7 broadcast_in_dim.8
  135.1 3.4 %all-to-all-start.4 = ((bf16[4,16,2048]{2,1,0:T(8,128)(2,1)}), bf16[4,16,2048]{2,1,0:T(8,128)(2,1)S(1)}, u32[]{:S(2)}, u32[]{:S(2)}) async-start(bf16[4,16,2048]{2,1,0:T(8,128)(2,1)} %broadcast_in_dim.8), calls=%async_computation.4 | async-start | bytes 524288 | tf_op jit(solution)/shard_map/all_to_all | solution.py:106
  138.6 6.6 %all-to-all-done.4 = bf16[4,16,2048]{2,1,0:T(8,128)(2,1)S(1)} async-done(((bf16[4,16,2048]{2,1,0:T(8,128)(2,1)}), bf16[4,16,2048]{2,1,0:T(8,128)(2,1)S(1)}, u32[]{:S(2)}, u32[]{:S(2)}) %all-to-all-start.4) | async-done | bytes 262176 | tf_op jit(solution)/shard_map/all_to_all | solution.py:106
  145.2 1.9 %convolution_convert_fusion.4 = bf16[64,384]{1,0:T(8,128)(2,1)S(1)} fusion(bf16[64,2048]{1,0:T(8,128)(2,1)S(1)} %bitcast.52, bf16[2048,384]{1,0:T(8,128)(2,1)} %param.24), kind=kOutput, calls=%fused_computation.8 | convolution fusion | flops 100687872 | bytes 1884160 | tf_op jit(solution)/shard_map/dot_general | solution.py:191
  147.5 1.8 convolution_convert_fusion.3
  149.2 1.8 convolution_convert_fusion.1
  151.1 1.3 collective-permute-start.5
  152.4 6.1 %collective-permute-start.6 = (bf16[2,4,2,768]{3,2,1,0:T(2,128)(2,1)S(1)}, bf16[2,4,2,768]{3,2,1,0:T(2,128)(2,1)S(1)}, u32[]{:S(2)}, u32[]{:S(2)}) collective-permute-start(bf16[2,4,2,768]{3,2,1,0:T(2,128)(2,1)S(1)} %pad_maximum_fusion.3), channel_id=1, source_target_pairs={{0,1},{1,0},{2,3},{3,2},{4,5},{5,4},{6,7},{7,6},{8,9},{9,8},{10,11... | collective-permute-start | bytes 73736 | tf_op jit(solution)/shard_map/ppermute | solution.py:120
  158.6 0.8 collective-permute-done.6
  159.8 1.2 copy-done.4
  161.3 1.8 %fusion = bf16[64,2048]{1,0:T(8,128)(2,1)S(1)} fusion(f32[64,2048]{1,0:T(8,128)S(1)} %fusion.21, bf16[384,2048]{1,0:T(8,128)(2,1)} %collective-permute-done.3, bf16[64,768]{1,0:T(8,128)(2,1)S(1)} %fusion.13), kind=kOutput, calls=%fused_computation.1 | convolution fusion | flops 100925440 | bytes 2408448 | tf_op jit(solution)/shard_map/dot_general | solution.py:213
  163.2 9.8 %all_to_all.32 = bf16[4,16,2048]{2,1,0:T(8,128)(2,1)S(1)} all-to-all(bf16[4,16,2048]{2,1,0:T(8,128)(2,1)S(1)} %bitcast.63), channel_id=1, replica_groups=mesh['z'=12,'q'=4,'m'=2,'g'=2,'xp'=2,'c'=2] {'g','xp'}, dimensions={0} | all-to-all | bytes 524288 | tf_op jit(solution)/shard_map/all_to_all | solution.py:106
  173.2 0.7 multiply_convert_fusion
  (67 shorter events, 3.0 us)
Async XLA Ops:
  6.5 1.7 copy-start
  6.5 3.1 %copy-start.5 = (bf16[32,2048]{1,0:T(8,128)(2,1)S(1)}, bf16[32,2048]{1,0:T(8,128)(2,1)}, u32[]{:S(2)}) copy-start(bf16[32,2048]{1,0:T(8,128)(2,1)} %param.16) | copy-start | bytes 393220
  6.5 3.1 %copy-start.7 = (f32[2048]{0:T(1024)S(1)}, f32[2048]{0:T(1024)}, u32[]{:S(2)}) copy-start(f32[2048]{0:T(1024)} %param.18) | copy-start | bytes 24580
  6.5 90.3 %all-gather.2.cloned.1.call-start = ((), (), s32[]{:S(2)}) async-start(), calls=%async_computation.6 | async-start | bytes 3407872 | tf_op jit(solution)/shard_map/all_gather | solution.py:166
  6.5 3.1 %copy-start.1 = (bf16[2048,512]{1,0:T(8,128)(2,1)S(1)}, bf16[2048,512]{1,0:T(8,128)(2,1)}, u32[]{:S(2)}) copy-start(bf16[2048,512]{1,0:T(8,128)(2,1)} %param.21) | copy-start | bytes 6291460
  9.6 29.2 %copy-start.6 = (bf16[128,2048]{1,0:T(8,128)(2,1)S(1)}, bf16[128,2048]{1,0:T(8,128)(2,1)}, u32[]{:S(2)}) copy-start(bf16[128,2048]{1,0:T(8,128)(2,1)} %param.15) | copy-start | bytes 1572868
  9.7 29.4 %copy-start.12 = (f32[2048]{0:T(1024)S(1)}, f32[2048]{0:T(1024)}, u32[]{:S(2)}) copy-start(f32[2048]{0:T(1024)} %param.17) | copy-start | bytes 24580
  30.2 25.3 %collective-permute-start.1 = (bf16[2048,384]{1,0:T(8,128)(2,1)}, bf16[2048,384]{1,0:T(8,128)(2,1)}, u32[]{:S(2)}, u32[]{:S(2)}) collective-permute-start(bf16[2048,384]{1,0:T(8,128)(2,1)} %param.24), channel_id=1, source_target_pairs={{0,1},{1,0},{2,3},{3,2},{4,5},{5,4},{6,7},{7,6},{8,9},{9,8},{10,11... | collective-permute-start | bytes 4718600 | tf_op jit(solution)/shard_map/ppermute | solution.py:120
  32.1 23.4 %collective-permute-start.2 = (bf16[2048,384]{1,0:T(8,128)(2,1)}, bf16[2048,384]{1,0:T(8,128)(2,1)}, u32[]{:S(2)}, u32[]{:S(2)}) collective-permute-start(bf16[2048,384]{1,0:T(8,128)(2,1)} %param.25), channel_id=1, source_target_pairs={{0,1},{1,0},{2,3},{3,2},{4,5},{5,4},{6,7},{7,6},{8,9},{9,8},{10,11... | collective-permute-start | bytes 4718600 | tf_op jit(solution)/shard_map/ppermute | solution.py:120
  34.5 21.0 %collective-permute-start.3 = (bf16[384,2048]{1,0:T(8,128)(2,1)}, bf16[384,2048]{1,0:T(8,128)(2,1)}, u32[]{:S(2)}, u32[]{:S(2)}) collective-permute-start(bf16[384,2048]{1,0:T(8,128)(2,1)} %param.28), channel_id=1, source_target_pairs={{0,1},{1,0},{2,3},{3,2},{4,5},{5,4},{6,7},{7,6},{8,9},{9,8},{10,11... | collective-permute-start | bytes 4718600 | tf_op jit(solution)/shard_map/ppermute | solution.py:120
  36.5 19.0 %collective-permute-start = (bf16[256,2048]{1,0:T(8,128)(2,1)}, bf16[256,2048]{1,0:T(8,128)(2,1)}, u32[]{:S(2)}, u32[]{:S(2)}) collective-permute-start(bf16[256,2048]{1,0:T(8,128)(2,1)} %own_ref), channel_id=1, source_target_pairs={{0,1},{1,0},{2,3},{3,2},{4,5},{5,4},{6,7},{7,6},{8,9},{9,8},{10,11... | collective-permute-start | bytes 3145736 | tf_op jit(solution)/shard_map/ppermute | solution.py:120
  39.1 8.1 %copy-start.8 = (bf16[3,384]{1,0:T(4,128)(2,1)S(1)}, bf16[3,384]{1,0:T(4,128)(2,1)}, u32[]{:S(2)}) copy-start(bf16[3,384]{1,0:T(4,128)(2,1)} %param.27) | copy-start | bytes 6916
  39.1 8.1 %copy-start.9 = (bf16[3,384]{1,0:T(4,128)(2,1)S(1)}, bf16[3,384]{1,0:T(4,128)(2,1)}, u32[]{:S(2)}) copy-start(bf16[3,384]{1,0:T(4,128)(2,1)} %param.26) | copy-start | bytes 6916
  41.6 13.9 %all-to-all-start.1 = ((bf16[8,128,256]{2,1,0:T(8,128)(2,1)}), bf16[8,128,256]{2,1,0:T(8,128)(2,1)S(1)}, u32[]{:S(2)}, u32[]{:S(2)}) async-start(bf16[8,128,256]{2,1,0:T(8,128)(2,1)} %broadcast_in_dim.7), calls=%async_computation.1 | async-start | bytes 1048576 | tf_op jit(solution)/shard_map/all_to_all | solution.py:106
  47.2 3.1 %collective-permute-start.4 = (bf16[2,3,384]{2,1,0:T(4,128)(2,1)S(1)}, bf16[2,3,384]{2,1,0:T(4,128)(2,1)S(1)}, u32[]{:S(2)}, u32[]{:S(2)}) collective-permute-start(bf16[2,3,384]{2,1,0:T(4,128)(2,1)S(1)} %pad_maximum_fusion.5), channel_id=1, source_target_pairs={{0,1},{1,0},{2,3},{3,2},{4,5},{5,4},{6,7},{7,6},{8,9},{9,8},{10,11... | collective-permute-start | bytes 13832 | tf_op jit(solution)/shard_map/ppermute | solution.py:120
  55.5 41.3 %copy-start.2 = (bf16[8,128,256]{2,1,0:T(8,128)(2,1)}, bf16[8,128,256]{2,1,0:T(8,128)(2,1)S(1)}, u32[]{:S(2)}) copy-start(bf16[8,128,256]{2,1,0:T(8,128)(2,1)S(1)} %all-to-all-done.1.q_ref) | copy-start | bytes 1572868
  119.8 14.5 %copy-start.10 = (f32[2048]{0:T(1024)S(1)}, f32[2048]{0:T(1024)}, u32[]{:S(2)}) copy-start(f32[2048]{0:T(1024)} %param.23) | copy-start | bytes 24580
  123.0 11.1 %all-to-all-start.3 = ((bf16[4,16,2048]{2,1,0:T(8,128)(2,1)}), bf16[4,16,2048]{2,1,0:T(8,128)(2,1)S(1)}, u32[]{:S(2)}, u32[]{:S(2)}) async-start(bf16[4,16,2048]{2,1,0:T(8,128)(2,1)} %bitcast.62), calls=%async_computation.3 | async-start | bytes 524288 | tf_op jit(solution)/shard_map/all_to_all | solution.py:106
  135.1 10.1 %all-to-all-start.4 = ((bf16[4,16,2048]{2,1,0:T(8,128)(2,1)}), bf16[4,16,2048]{2,1,0:T(8,128)(2,1)S(1)}, u32[]{:S(2)}, u32[]{:S(2)}) async-start(bf16[4,16,2048]{2,1,0:T(8,128)(2,1)} %broadcast_in_dim.8), calls=%async_computation.4 | async-start | bytes 524288 | tf_op jit(solution)/shard_map/all_to_all | solution.py:106
  145.2 1.9 %copy-start.3 = (bf16[2048,384]{1,0:T(8,128)(2,1)S(1)}, bf16[2048,384]{1,0:T(8,128)(2,1)}, u32[]{:S(2)}) copy-start(bf16[2048,384]{1,0:T(8,128)(2,1)} %param.25) | copy-start | bytes 4718596
  151.1 8.3 %collective-permute-start.5 = (bf16[2,1,2,768]{3,2,1,0:T(2,128)(2,1)S(1)}, bf16[2,1,2,768]{3,2,1,0:T(2,128)(2,1)S(1)}, u32[]{:S(2)}, u32[]{:S(2)}) collective-permute-start(bf16[2,1,2,768]{3,2,1,0:T(2,128)(2,1)S(1)} %pad_maximum_fusion.4), channel_id=1, source_target_pairs={{1,8},{9,16},{17,24},{25,32},{33,40},{41,48},{49,56},{57,64},{65,7... | collective-permute-start | bytes 18440 | tf_op jit(solution)/shard_map/ppermute | solution.py:126
  152.4 6.9 %collective-permute-start.6 = (bf16[2,4,2,768]{3,2,1,0:T(2,128)(2,1)S(1)}, bf16[2,4,2,768]{3,2,1,0:T(2,128)(2,1)S(1)}, u32[]{:S(2)}, u32[]{:S(2)}) collective-permute-start(bf16[2,4,2,768]{3,2,1,0:T(2,128)(2,1)S(1)} %pad_maximum_fusion.3), channel_id=1, source_target_pairs={{0,1},{1,0},{2,3},{3,2},{4,5},{5,4},{6,7},{7,6},{8,9},{9,8},{10,11... | collective-permute-start | bytes 73736 | tf_op jit(solution)/shard_map/ppermute | solution.py:120
  159.5 1.4 copy-start.4
  161.3 11.9 %copy-start.11 = (f32[2048]{0:T(1024)S(1)}, f32[2048]{0:T(1024)}, u32[]{:S(2)}) copy-start(f32[2048]{0:T(1024)} %param.29) | copy-start | bytes 24580
Sparse Core Ops, SparseCore 0:
  30.3 66.4 all-gather.1

commit v2 on v1

v2 whole, which is shorter than its diff:
```python
import jax
import jax.numpy as jnp
from jax import lax
from jax.experimental import pallas as pl
from jax.experimental.pallas import tpu as pltpu
from jax.sharding import Mesh
from jax.sharding import PartitionSpec as P

D = 2048
HEAD = 256
KV_HEADS = 2
CONV = 3
TGT_DEV = 128
PAD = 16
EPS = 1e-06

M = 4
SP = ("q", "m", "y")
TP = ("g", "xp", "c")
CHIPS = ("g", "xp")
SLICES = ("m", "xp")
BLOCK = 16
HALF = TGT_DEV // 2
bf16 = jnp.bfloat16
f32 = jnp.float32


def normalize(values, gain):
    widened = values.astype(f32)
    scaled = widened * lax.rsqrt(jnp.mean(widened * widened, axis=-1, keepdims=True) + EPS)
    return (scaled * gain).astype(bf16)


def attend_body(q_ref, own_ref, other_ref, o_ref):
    sources = (own_ref, other_ref)
    row = lax.broadcasted_iota(jnp.int32, (PAD, HEAD), 0)
    for at in range(0, q_ref.shape[0], 4):
        q = q_ref[at : at + 4].reshape(4 * HALF, HEAD)
        scores = [
            lax.dot_general(
                q, kv[:, :HEAD], (((1,), (1,)), ((), ())), preferred_element_type=f32
            )
            for kv in sources
        ]
        tops = [jnp.max(s, axis=1, keepdims=True) for s in scores]
        top = jnp.maximum(tops[0], tops[1])
        probs = [jnp.exp(s - top) for s in scores]
        total = sum(jnp.sum(p, axis=1, keepdims=True) for p in probs)
        o = sum(
            jnp.dot(p.astype(bf16), kv[:, HEAD:], preferred_element_type=f32)
            for p, kv in zip(probs, sources)
        )
        o = (o / total).astype(bf16)
        lse = top + jnp.log(total)
        for b in range(2):
            o_ref[at // 2 + b, :TGT_DEV, :] = o[b * TGT_DEV : (b + 1) * TGT_DEV]
            column = lse[b * TGT_DEV : (b + 1) * TGT_DEV]
            line = jnp.broadcast_to(column, (TGT_DEV, TGT_DEV)).T[:1]
            hi = line.astype(bf16).astype(f32)
            mid = (line - hi).astype(bf16).astype(f32)
            lo = line - hi - mid
            first = jnp.concatenate([hi, mid], axis=1)
            second = jnp.concatenate([lo, jnp.zeros_like(lo)], axis=1)
            tile = jnp.where(row == 0, first, jnp.where(row == 1, second, 0.0))
            o_ref[at // 2 + b, TGT_DEV:, :] = tile.astype(bf16)


def attend(queries, own, other, step=8):
    blocks = queries.shape[0]
    return pl.pallas_call(
        attend_body,
        grid=(blocks // step,),
        in_specs=[
            pl.BlockSpec((step, HALF, HEAD), lambda i: (i, 0, 0)),
            pl.BlockSpec(own.shape, lambda i: (0, 0)),
            pl.BlockSpec(other.shape, lambda i: (0, 0)),
        ],
        out_specs=pl.BlockSpec((step // 2, TGT_DEV + PAD, HEAD), lambda i: (i, 0, 0)),
        out_shape=jax.ShapeDtypeStruct((blocks // 2, TGT_DEV + PAD, HEAD), bf16),
    )(queries, own, other)


def merge_body(parts_ref, own_ref, other_ref, o_ref):
    count = parts_ref.shape[0]
    tail = parts_ref[:, TGT_DEV:, :].astype(f32)
    lse = tail[:, 0, :TGT_DEV] + tail[:, 0, TGT_DEV:] + tail[:, 1, :TGT_DEV]
    weight = jnp.exp(lse - jnp.max(lse, axis=0, keepdims=True))
    weight = (weight / jnp.sum(weight, axis=0, keepdims=True)).T
    merged = parts_ref[0, :TGT_DEV, :].astype(f32) * weight[:, :1]
    for t in range(1, count):
        merged = merged + parts_ref[t, :TGT_DEV, :].astype(f32) * weight[:, t : t + 1]
    merged = merged.astype(bf16)
    projected = jnp.dot(merged[:HALF], own_ref[...], preferred_element_type=f32)
    projected += jnp.dot(merged[HALF:], other_ref[...], preferred_element_type=f32)
    o_ref[...] = projected.astype(bf16)


def merge_project(parts, own, other):
    return pl.pallas_call(
        merge_body,
        out_shape=jax.ShapeDtypeStruct((HALF, D), bf16),
    )(parts, own, other)


def mixer_in_body(tiles_ref, target_ref, gain_ref, *refs):
    weights, (res_ref, gu_ref, tails_ref), held, sem = refs[:4], refs[4:7], refs[7], refs[8]
    copies = [pltpu.make_async_copy(w, held.at[k], sem.at[k]) for k, w in enumerate(weights)]
    for copy in copies:
        copy.start()
    projected = tiles_ref[0].astype(f32)
    for t in range(1, tiles_ref.shape[0]):
        projected = projected + tiles_ref[t].astype(f32)
    residual = (target_ref[...].astype(f32) + projected).astype(bf16)
    res_ref[...] = residual
    rows = normalize(residual, gain_ref[...])
    width = held.shape[2]
    for k, copy in enumerate(copies):
        copy.wait()
        part = jnp.dot(rows, held[k], preferred_element_type=f32).astype(bf16)
        gu_ref[:, k * width : (k + 1) * width] = part
        last = [part[b + BLOCK - (CONV - 1) : b + BLOCK] for b in range(0, HALF, BLOCK)]
        tails_ref[:, k * width : (k + 1) * width] = jnp.concatenate(last, axis=0)


def mixer_in(tiles, target, gain, weights):
    vmem = pl.BlockSpec(memory_space=pltpu.VMEM)
    hbm = pl.BlockSpec(memory_space=pl.ANY)
    width = weights[0].shape[1]
    count = len(weights)
    return pl.pallas_call(
        mixer_in_body,
        in_specs=[vmem, vmem, vmem] + [hbm] * count,
        out_shape=[
            jax.ShapeDtypeStruct((HALF, D), bf16),
            jax.ShapeDtypeStruct((HALF, count * width), bf16),
            jax.ShapeDtypeStruct((HALF // BLOCK * (CONV - 1), count * width), bf16),
        ],
        scratch_shapes=[
            pltpu.VMEM((count, D, width), bf16),
            pltpu.SemaphoreType.DMA((count,)),
        ],
    )(tiles, target, gain.reshape(1, D), *weights)


def mixer_out_body(core_ref, gu_ref, across_ref, before_ref, taps_ref, down_ref, other_ref, o_ref, held, sem):
    copies = [
        pltpu.make_async_copy(w, held.at[k], sem.at[k]) for k, w in enumerate((down_ref, other_ref))
    ]
    for copy in copies:
        copy.start()
    width = held.shape[1]
    halo = CONV - 1
    first = core_ref[0] == 0
    across = across_ref[...].astype(f32)
    before = before_ref[...].astype(f32)
    shifted = jnp.concatenate([before, across[:-halo]], axis=0)
    earlier = jnp.where(first, shifted, across)

    def convolved(at, from_at, tap_row, tap_at):
        blocks = []
        for b in range(HALF // BLOCK):
            ahead = earlier[b * halo : (b + 1) * halo, from_at : from_at + width]
            here = gu_ref[b * BLOCK : (b + 1) * BLOCK, at : at + width].astype(f32)
            padded = jnp.concatenate([ahead, here], axis=0)
            mixed = 0.0
            for tap in range(CONV):
                scale = taps_ref[tap_row + tap : tap_row + tap + 1, tap_at : tap_at + width]
                mixed = mixed + scale * padded[tap : tap + BLOCK]
            blocks.append(mixed)
        return jnp.concatenate(blocks, axis=0)

    total = 0.0
    for k, copy in enumerate(copies):
        gate = convolved(k * width, (1 - k) * width, 0, k * width)
        up = convolved((2 + k) * width, (3 - k) * width, CONV, k * width)
        hidden = (gate / (1.0 + jnp.exp(-gate)) * up).astype(bf16)
        copy.wait()
        total = total + jnp.dot(hidden, held[k], preferred_element_type=f32)
    o_ref[...] = total.astype(bf16)


def mixer_out(core, gate_up, across, before, taps, down, other):
    vmem = pl.BlockSpec(memory_space=pltpu.VMEM)
    hbm = pl.BlockSpec(memory_space=pl.ANY)
    return pl.pallas_call(
        mixer_out_body,
        in_specs=[pl.BlockSpec(memory_space=pltpu.SMEM), vmem, vmem, vmem, vmem, hbm, hbm],
        out_shape=jax.ShapeDtypeStruct((HALF, D), bf16),
        scratch_shapes=[pltpu.VMEM((2, *down.shape), bf16), pltpu.SemaphoreType.DMA((2,))],
    )(core, gate_up, across, before, taps, down, other)


def exchanged(array, axes):
    return lax.all_to_all(array, axes, 0, 0, tiled=True)


def sent_to_all(shard, axes):
    count = lax.axis_size(axes)
    return exchanged(jnp.broadcast_to(shard, (count, *shard.shape)), axes)


def other_core(array):
    return lax.ppermute(array, "c", [(0, 1), (1, 0)])


def from_last_line(array):
    lines = lax.axis_size(SP)
    axes = (*SP, "c")
    return lax.ppermute(array, axes, [(2 * i + 1, 2 * i + 2) for i in range(lines - 1)])


def shards(
    target,
    source,
    query_gain,
    source_gain,
    query_weight,
    key_weight,
    value_weight,
    out_weight,
    mixer_gain,
    gate_weight,
    up_weight,
    gate_taps,
    up_taps,
    down_weight,
    final_gain,
):
    core = lax.axis_index("c")
    chip = lax.axis_index(CHIPS)
    source_normed = normalize(source, source_gain)
    key_rows = jnp.dot(source_normed, key_weight, preferred_element_type=f32).astype(bf16)
    value_rows = jnp.dot(source_normed, value_weight, preferred_element_type=f32).astype(bf16)
    rows = source.shape[0]
    by_head = jnp.stack(
        [
            jnp.concatenate([key_rows[:, :HEAD], value_rows[:, :HEAD]], axis=1),
            jnp.concatenate([key_rows[:, HEAD:], value_rows[:, HEAD:]], axis=1),
        ]
    )
    quads = lax.axis_size("q")
    to_send = jnp.broadcast_to(by_head[:, None], (KV_HEADS, quads, rows, 2 * HEAD))
    near = exchanged(to_send.reshape(KV_HEADS * quads, rows, 2 * HEAD), ("g", "q"))
    near = near.reshape(KV_HEADS * quads * rows, 2 * HEAD)
    near, target, out_weight, gate_weight, up_weight, gate_taps, up_taps, down_weight = (
        lax.optimization_barrier(
            (near, target, out_weight, gate_weight, up_weight, gate_taps, up_taps, down_weight)
        )
    )
    kv = sent_to_all(near, "y").reshape(-1, 2 * HEAD)

    normed = normalize(target, query_gain)
    own_query = jnp.dot(normed, query_weight, preferred_element_type=f32).astype(bf16)
    own_query = own_query * jnp.asarray(HEAD ** (-0.5), bf16)
    by_core = own_query.reshape(4, 2, BLOCK, HEAD)
    kept = lax.dynamic_index_in_dim(by_core, core, 1, False).reshape(HALF, HEAD)
    given = lax.dynamic_index_in_dim(by_core, 1 - core, 1, False).reshape(HALF, HEAD)
    both = jnp.stack([kept, other_core(given)])
    queries = lax.all_gather(both, "xp", axis=0, tiled=True)
    queries = lax.all_gather(queries, "m", axis=0, tiled=True)
    target_half = lax.dynamic_index_in_dim(target.reshape(4, 2, BLOCK, D), core, 1, False)
    target_half = target_half.reshape(HALF, D)
    out_other = other_core(out_weight)
    gate_other = other_core(gate_weight)
    up_other = other_core(up_weight)
    down_other = other_core(down_weight)
    taps = jnp.concatenate([gate_taps, up_taps], axis=0)
    taps = jnp.concatenate([taps, other_core(taps)], axis=1).astype(f32)
    queries, target_half, out_other, gate_other, up_other, down_other, taps = (
        lax.optimization_barrier(
            (queries, target_half, out_other, gate_other, up_other, down_other, taps)
        )
    )
    parts = exchanged(attend(queries, kv, other_core(kv)), SLICES)
    core_at = core.astype(jnp.int32).reshape(1)
    partial = merge_project(parts, out_weight, out_other)
    residual, gate_up, tails = mixer_in(
        sent_to_all(partial, CHIPS),
        target_half,
        mixer_gain,
        (gate_weight, gate_other, up_weight, up_other),
    )
    before = from_last_line(tails[-(CONV - 1) :])
    across = other_core(tails)
    partial = mixer_out(core_at, gate_up, across, before, taps, down_weight, down_other)
    tiles = exchanged(partial.reshape(HALF // BLOCK, BLOCK, D), CHIPS)
    mixer = jnp.sum(tiles.astype(f32), axis=0)
    own_rows = lax.dynamic_slice_in_dim(residual, chip * BLOCK, BLOCK, 0)
    return normalize(own_rows.astype(f32) + mixer, final_gain)


def solution(mesh):
    lines = mesh.shape["sp"]
    devices = mesh.devices.reshape(lines // 8 // M, M, 8, 2, 2, 2)
    split = Mesh(devices, SP + TP)
    whole = SP + TP
    return jax.shard_map(
        shards,
        mesh=split,
        in_specs=(
            P(SP, None),
            P(whole, None),
            P(),
            P(),
            P(None, TP),
            P(),
            P(),
            P(TP, None),
            P(),
            P(None, TP),
            P(None, TP),
            P(None, TP),
            P(None, TP),
            P(TP, None),
            P(),
        ),
        out_specs=P(whole, None),
        check_vma=False,
    )
```

time: 182 us -> 195 us (1.071)
  the two profiles are of different devices: /device:TPU:24 before, /device:TPU:64 now
where the time goes in v2:
time: 195 us; the launch traced here: 194 us
  blocking collectives  86 us (44%)
  waiting for transfers between devices  45.4 us (23%)
  starting transfers between devices  28.5 us (15%)
  Pallas kernels  21.6 us (11%)
  local copies, waits for them, and re-layouts  6 us (3%)
  matrix products  3.49 us (2%)
  other arithmetic  2.94 us (2%)
    all_to_all x3, blocking collectives, exchanged(): return lax.all_to_all(array, axes, 0, 0, tiled=True)  60 us
    all_to_all x2, waiting for transfers between devices, exchanged(): return lax.all_to_all(array, axes, 0, 0, tiled=True)  38.5 us
    all_gather x1, blocking collectives, shards(): queries = lax.all_gather(queries, 'm', axis=0, tiled=True)  21 us
    ppermute x8, starting transfers between devices, other_core(): return lax.ppermute(array, 'c', [(0, 1), (1, 0)])  16.6 us
    all_to_all x2, starting transfers between devices, exchanged(): return lax.all_to_all(array, axes, 0, 0, tiled=True)  10.7 us
    pallas_call x1, Pallas kernels, attend(): pl.pallas_call(attend_body, grid=(blocks // step,), in_specs=[pl.BlockSpe...  8.84 us
    ppermute x1, waiting for transfers between devices, from_last_line(): lax.ppermute(array, axes, [(2 * i + 1, 2 * i + 2) for i in range(lines -...  5.76 us
    pallas_call x1, Pallas kernels, mixer_in(): pl.pallas_call(mixer_in_body, in_specs=[vmem, vmem, vmem] + [hbm] * count...  5.31 us
  transfers between devices with their start and end apart: 11, of which 4 were waited for; matrix products, arithmetic and copies ran while one was open for 2% of the time, Pallas kernels for 0%

profile of v2, /device:TPU:64, one launch (start us, length us, event | category | flops | bytes accessed | tf_op | source)
XLA Modules:
  0.0 194.3 jit_solution(67910063863984421)
XLA Ops:
  0.0 1.2 fusion.7
  1.7 1.4 convolution_convert_fusion.1
  3.7 27.3 %all_to_all.25 = bf16[6,32,512]{2,1,0:T(8,128)(2,1)S(1)} all-to-all(bf16[6,32,512]{2,1,0:T(8,128)(2,1)S(1)} %bitcast.25), channel_id=1, replica_groups=mesh['q'=3,'m'=4,'y'=8,'g'=2,'xp'=2,'c'=2] {'g','q'}, dimensions={0} | all-to-all | bytes 393216 | tf_op jit(solution)/shard_map/all_to_all | solution.py:194
  31.0 1.3 broadcast_in_dim.7
  32.3 7.2 %all-to-all-start.1 = ((bf16[8,192,512]{2,1,0:T(8,128)(2,1)}), bf16[8,192,512]{2,1,0:T(8,128)(2,1)}, u32[]{:S(2)}, u32[]{:S(2)}) async-start(bf16[8,192,512]{2,1,0:T(8,128)(2,1)} %broadcast_in_dim.7), calls=%async_computation.1 | async-start | bytes 3145728 | tf_op jit(solution)/shard_map/all_to_all | solution.py:194
  39.5 1.9 collective-permute-start.2
  41.4 2.4 %collective-permute-start.3 = (bf16[2048,384]{1,0:T(8,128)(2,1)}, bf16[2048,384]{1,0:T(8,128)(2,1)}, u32[]{:S(2)}, u32[]{:S(2)}) collective-permute-start(bf16[2048,384]{1,0:T(8,128)(2,1)} %refs_2_), channel_id=1, source_target_pairs={{0,1},{1,0},{2,3},{3,2},{4,5},{5,4},{6,7},{7,6},{8,9},{9,8},{10,11... | collective-permute-start | bytes 4718600 | tf_op jit(solution)/shard_map/ppermute | solution.py:203
  43.9 1.9 collective-permute-start.4
  46.0 31.8 %all-to-all-done.1 = bf16[8,192,512]{2,1,0:T(8,128)(2,1)} async-done(((bf16[8,192,512]{2,1,0:T(8,128)(2,1)}), bf16[8,192,512]{2,1,0:T(8,128)(2,1)}, u32[]{:S(2)}, u32[]{:S(2)}) %all-to-all-start.1) | async-done | bytes 1572896 | tf_op jit(solution)/shard_map/all_to_all | solution.py:194
  77.8 2.0 %collective-permute-start.6 = (bf16[1536,512]{1,0:T(8,128)(2,1)}, bf16[1536,512]{1,0:T(8,128)(2,1)}, u32[]{:S(2)}, u32[]{:S(2)}) collective-permute-start(bf16[1536,512]{1,0:T(8,128)(2,1)} %bitcast.10.own_ref), channel_id=1, source_target_pairs={{0,1},{1,0},{2,3},{3,2},{4,5},{5,4},{6,7},{7,6},{8,9},{9,8},{10,11... | collective-permute-start | bytes 4718600 | tf_op jit(solution)/shard_map/ppermute | solution.py:203
  79.9 2.4 %collective-permute-start.5 = (bf16[6,384]{1,0:T(8,128)(2,1)S(1)}, bf16[6,384]{1,0:T(8,128)(2,1)S(1)}, u32[]{:S(2)}, u32[]{:S(2)}) collective-permute-start(bf16[6,384]{1,0:T(8,128)(2,1)S(1)} %pad_maximum_fusion.2), channel_id=1, source_target_pairs={{0,1},{1,0},{2,3},{3,2},{4,5},{5,4},{6,7},{7,6},{8,9},{9,8},{10,11... | collective-permute-start | bytes 13832 | tf_op jit(solution)/shard_map/ppermute | solution.py:203
  82.3 1.6 fusion
  84.0 1.9 collective-permute-start
  85.9 1.2 collective-permute-done
  87.1 2.1 %collective-permute-start.1 = (bf16[256,2048]{1,0:T(8,128)(2,1)S(1)}, bf16[256,2048]{1,0:T(8,128)(2,1)S(1)}, u32[]{:S(2)}, u32[]{:S(2)}) collective-permute-start(bf16[256,2048]{1,0:T(8,128)(2,1)S(1)} %copy-done.4), channel_id=1, source_target_pairs={{0,1},{1,0},{2,3},{3,2},{4,5},{5,4},{6,7},{7,6},{8,9},{9,8},{10,11... | collective-permute-start | bytes 3145736 | tf_op jit(solution)/shard_map/ppermute | solution.py:203
  89.1 0.7 constant_dynamic-slice_fusion
  90.5 5.0 %all_gather.6 = bf16[4,64,256]{2,1,0:T(8,128)(2,1)S(1)} all-gather(bf16[2,64,256]{2,1,0:T(8,128)(2,1)S(1)} %pad_maximum_fusion.1), channel_id=1, replica_groups=mesh['q'=3,'m'=4,'y'=8,'g'=2,'xp'=2,'c'=2] {'xp'}, dimensions={0}, use_global_device_ids=true | all-gather | bytes 196608 | tf_op jit(solution)/shard_map/all_gather | solution.py:259
  95.5 21.0 %all_gather.7.q_ref = bf16[16,64,256]{2,1,0:T(8,128)(2,1)} all-gather(bf16[4,64,256]{2,1,0:T(8,128)(2,1)S(1)} %all_gather.6), channel_id=1, replica_groups=mesh['q'=3,'m'=4,'y'=8,'g'=2,'xp'=2,'c'=2] {'m'}, dimensions={0}, use_global_device_ids=true | all-gather | bytes 655360 | tf_op jit(solution)/shard_map/all_gather | solution.py:260
  116.5 1.0 copy-done.5
  117.6 8.8 %shard_map.145 = bf16[8,144,256]{2,1,0:T(8,128)(2,1)} custom-call(bf16[16,64,256]{2,1,0:T(8,128)(2,1)} %all_gather.7.q_ref, bf16[1536,512]{1,0:T(8,128)(2,1)} %bitcast.10.own_ref, bf16[1536,512]{1,0:T(8,128)(2,1)} %collective-permute-done.6.other_ref), custom_call_target="tpu_custom_call" | custom-call | tf_op jit(solution)/shard_map/pallas_call | solution.py:70
  126.4 17.4 %all_to_all.26.parts_ref = bf16[8,144,256]{2,1,0:T(8,128)(2,1)} all-to-all(bf16[8,144,256]{2,1,0:T(8,128)(2,1)} %shard_map.145), channel_id=1, replica_groups=mesh['q'=3,'m'=4,'y'=8,'g'=2,'xp'=2,'c'=2] {'m','xp'}, dimensions={0} | all-to-all | bytes 1179648 | tf_op jit(solution)/shard_map/all_to_all | solution.py:194
  143.8 3.2 %shard_map.146 = bf16[64,2048]{1,0:T(8,128)(2,1)} custom-call(bf16[8,144,256]{2,1,0:T(8,128)(2,1)} %all_to_all.26.parts_ref, bf16[256,2048]{1,0:T(8,128)(2,1)} %own_ref, bf16[256,2048]{1,0:T(8,128)(2,1)} %copy-done.5), custom_call_target="tpu_custom_call" | custom-call | tf_op jit(solution)/shard_map/pallas_call | solution.py:99
  147.0 1.1 broadcast_in_dim.8
  148.0 15.4 %all_to_all.27.tiles_ref = bf16[4,64,2048]{2,1,0:T(8,128)(2,1)} all-to-all(bf16[4,64,2048]{2,1,0:T(8,128)(2,1)S(1)} %broadcast_in_dim.8), channel_id=1, replica_groups=mesh['q'=3,'m'=4,'y'=8,'g'=2,'xp'=2,'c'=2] {'g','xp'}, dimensions={0} | all-to-all | bytes 2097152 | tf_op jit(solution)/shard_map/all_to_all | solution.py:194
  163.4 5.3 %shard_map.147 = (bf16[64,2048]{1,0:T(8,128)(2,1)}, bf16[64,1536]{1,0:T(8,128)(2,1)}, bf16[8,1536]{1,0:T(8,128)(2,1)}) custom-call(bf16[4,64,2048]{2,1,0:T(8,128)(2,1)} %all_to_all.27.tiles_ref, bf16[64,2048]{1,0:T(8,128)(2,1)} %bitcast.22, f32[1,2048]{1,0:T(1,128)} %bitcast.30, bf16[2048,384]{1,0:T(8,128)(2,1)} %refs_0_, ...), custom_call_target="tpu_custom_call" | custom-call | tf_op jit(solution)/shard_map/pallas_call | solution.py:130
  168.7 1.9 collective-permute-start.7
  170.6 0.7 slice.19
  171.4 1.3 collective-permute-start.8
  172.7 5.8 %collective-permute-done.8.before_ref = bf16[2,1536]{1,0:T(2,128)(2,1)S(1)} collective-permute-done((bf16[2,1536]{1,0:T(2,128)(2,1)S(1)}, bf16[2,1536]{1,0:T(2,128)(2,1)S(1)}, u32[]{:S(2)}, u32[]{:S(2)}) %collective-permute-start.8) | collective-permute-done | bytes 6176 | tf_op jit(solution)/shard_map/ppermute | solution.py:209
  179.1 4.3 %shard_map.148 = bf16[64,2048]{1,0:T(8,128)(2,1)} custom-call(s32[1]{0:T(128)} %bitcast.12.core_ref, bf16[64,1536]{1,0:T(8,128)(2,1)} %get-tuple-element.37.gu_ref, bf16[8,1536]{1,0:T(8,128)(2,1)} %copy-done.8, bf16[2,1536]{1,0:T(2,128)(2,1)} %copy-done.12, f32[6,768]{1,0:T(8,128)} %maximum_convert_fusion.taps_ref, bf16[384,2048]{1,0:T(8,128)(2,1)} %down_ref, ...), custom_call_target="tpu_custom_call" | custom-call | tf_op jit(solution)/shard_map/pallas_call | solution.py:185
  183.3 3.4 %all-to-all-start.4 = ((bf16[4,16,2048]{2,1,0:T(8,128)(2,1)}), bf16[4,16,2048]{2,1,0:T(8,128)(2,1)S(1)}, u32[]{:S(2)}, u32[]{:S(2)}) async-start(bf16[4,16,2048]{2,1,0:T(8,128)(2,1)} %bitcast.23), calls=%async_computation.4 | async-start | bytes 524288 | tf_op jit(solution)/shard_map/all_to_all | solution.py:194
  186.8 6.6 %all-to-all-done.4 = bf16[4,16,2048]{2,1,0:T(8,128)(2,1)S(1)} async-done(((bf16[4,16,2048]{2,1,0:T(8,128)(2,1)}), bf16[4,16,2048]{2,1,0:T(8,128)(2,1)S(1)}, u32[]{:S(2)}, u32[]{:S(2)}) %all-to-all-start.4) | async-done | bytes 262176 | tf_op jit(solution)/shard_map/all_to_all | solution.py:194
  (51 shorter events, 3.4 us)
Async XLA Ops:
  0.0 1.7 copy-start
  0.0 3.1 %copy-start.2 = (bf16[32,2048]{1,0:T(8,128)(2,1)S(1)}, bf16[32,2048]{1,0:T(8,128)(2,1)}, u32[]{:S(2)}) copy-start(bf16[32,2048]{1,0:T(8,128)(2,1)} %param.16) | copy-start | bytes 393220
  0.0 3.1 %copy-start.7 = (f32[2048]{0:T(1024)S(1)}, f32[2048]{0:T(1024)}, u32[]{:S(2)}) copy-start(f32[2048]{0:T(1024)} %param.18) | copy-start | bytes 24580
  0.0 3.1 %copy-start.1 = (bf16[2048,512]{1,0:T(8,128)(2,1)S(1)}, bf16[2048,512]{1,0:T(8,128)(2,1)}, u32[]{:S(2)}) copy-start(bf16[2048,512]{1,0:T(8,128)(2,1)} %param.20) | copy-start | bytes 6291460
  32.3 13.5 %copy-start.3 = (bf16[128,2048]{1,0:T(8,128)(2,1)S(1)}, bf16[128,2048]{1,0:T(8,128)(2,1)}, u32[]{:S(2)}) copy-start(bf16[128,2048]{1,0:T(8,128)(2,1)} %param.15) | copy-start | bytes 1572868
  32.3 47.6 %copy-start.9 = (bf16[3,384]{1,0:T(4,128)(2,1)S(1)}, bf16[3,384]{1,0:T(4,128)(2,1)}, u32[]{:S(2)}) copy-start(bf16[3,384]{1,0:T(4,128)(2,1)} %param.27) | copy-start | bytes 6916
  32.3 47.6 %copy-start.10 = (bf16[3,384]{1,0:T(4,128)(2,1)S(1)}, bf16[3,384]{1,0:T(4,128)(2,1)}, u32[]{:S(2)}) copy-start(bf16[3,384]{1,0:T(4,128)(2,1)} %param.26) | copy-start | bytes 6916
  32.3 50.1 %copy-start.13 = (f32[2048]{0:T(1024)S(1)}, f32[2048]{0:T(1024)}, u32[]{:S(2)}) copy-start(f32[2048]{0:T(1024)} %param.17) | copy-start | bytes 24580
  32.3 45.5 %all-to-all-start.1 = ((bf16[8,192,512]{2,1,0:T(8,128)(2,1)}), bf16[8,192,512]{2,1,0:T(8,128)(2,1)}, u32[]{:S(2)}, u32[]{:S(2)}) async-start(bf16[8,192,512]{2,1,0:T(8,128)(2,1)} %broadcast_in_dim.7), calls=%async_computation.1 | async-start | bytes 3145728 | tf_op jit(solution)/shard_map/all_to_all | solution.py:194
  39.5 78.0 %collective-permute-start.2 = (bf16[2048,384]{1,0:T(8,128)(2,1)}, bf16[2048,384]{1,0:T(8,128)(2,1)}, u32[]{:S(2)}, u32[]{:S(2)}) collective-permute-start(bf16[2048,384]{1,0:T(8,128)(2,1)} %refs_0_), channel_id=1, source_target_pairs={{0,1},{1,0},{2,3},{3,2},{4,5},{5,4},{6,7},{7,6},{8,9},{9,8},{10,11... | collective-permute-start | bytes 4718600 | tf_op jit(solution)/shard_map/ppermute | solution.py:203
  41.4 76.1 %collective-permute-start.3 = (bf16[2048,384]{1,0:T(8,128)(2,1)}, bf16[2048,384]{1,0:T(8,128)(2,1)}, u32[]{:S(2)}, u32[]{:S(2)}) collective-permute-start(bf16[2048,384]{1,0:T(8,128)(2,1)} %refs_2_), channel_id=1, source_target_pairs={{0,1},{1,0},{2,3},{3,2},{4,5},{5,4},{6,7},{7,6},{8,9},{9,8},{10,11... | collective-permute-start | bytes 4718600 | tf_op jit(solution)/shard_map/ppermute | solution.py:203
  43.9 73.7 %collective-permute-start.4 = (bf16[384,2048]{1,0:T(8,128)(2,1)}, bf16[384,2048]{1,0:T(8,128)(2,1)}, u32[]{:S(2)}, u32[]{:S(2)}) collective-permute-start(bf16[384,2048]{1,0:T(8,128)(2,1)} %down_ref), channel_id=1, source_target_pairs={{0,1},{1,0},{2,3},{3,2},{4,5},{5,4},{6,7},{7,6},{8,9},{9,8},{10,11... | collective-permute-start | bytes 4718600 | tf_op jit(solution)/shard_map/ppermute | solution.py:203
  77.8 9.2 %copy-start.4 = (bf16[256,2048]{1,0:T(8,128)(2,1)S(1)}, bf16[256,2048]{1,0:T(8,128)(2,1)}, u32[]{:S(2)}) copy-start(bf16[256,2048]{1,0:T(8,128)(2,1)} %own_ref) | copy-start | bytes 3145732
  77.8 39.7 %collective-permute-start.6 = (bf16[1536,512]{1,0:T(8,128)(2,1)}, bf16[1536,512]{1,0:T(8,128)(2,1)}, u32[]{:S(2)}, u32[]{:S(2)}) collective-permute-start(bf16[1536,512]{1,0:T(8,128)(2,1)} %bitcast.10.own_ref), channel_id=1, source_target_pairs={{0,1},{1,0},{2,3},{3,2},{4,5},{5,4},{6,7},{7,6},{8,9},{9,8},{10,11... | collective-permute-start | bytes 4718600 | tf_op jit(solution)/shard_map/ppermute | solution.py:203
  79.9 4.0 %collective-permute-start.5 = (bf16[6,384]{1,0:T(8,128)(2,1)S(1)}, bf16[6,384]{1,0:T(8,128)(2,1)S(1)}, u32[]{:S(2)}, u32[]{:S(2)}) collective-permute-start(bf16[6,384]{1,0:T(8,128)(2,1)S(1)} %pad_maximum_fusion.2), channel_id=1, source_target_pairs={{0,1},{1,0},{2,3},{3,2},{4,5},{5,4},{6,7},{7,6},{8,9},{9,8},{10,11... | collective-permute-start | bytes 13832 | tf_op jit(solution)/shard_map/ppermute | solution.py:203
  84.0 3.1 %collective-permute-start = (bf16[64,256]{1,0:T(8,128)(2,1)S(1)}, bf16[64,256]{1,0:T(8,128)(2,1)S(1)}, u32[]{:S(2)}, u32[]{:S(2)}) collective-permute-start(bf16[64,256]{1,0:T(8,128)(2,1)S(1)} %bitcast.29), channel_id=1, source_target_pairs={{0,1},{1,0},{2,3},{3,2},{4,5},{5,4},{6,7},{7,6},{8,9},{9,8},{10,11... | collective-permute-start | bytes 98312 | tf_op jit(solution)/shard_map/ppermute | solution.py:203
  87.1 29.4 %collective-permute-start.1 = (bf16[256,2048]{1,0:T(8,128)(2,1)S(1)}, bf16[256,2048]{1,0:T(8,128)(2,1)S(1)}, u32[]{:S(2)}, u32[]{:S(2)}) collective-permute-start(bf16[256,2048]{1,0:T(8,128)(2,1)S(1)} %copy-done.4), channel_id=1, source_target_pairs={{0,1},{1,0},{2,3},{3,2},{4,5},{5,4},{6,7},{7,6},{8,9},{9,8},{10,11... | collective-permute-start | bytes 3145736 | tf_op jit(solution)/shard_map/ppermute | solution.py:203
  116.5 1.0 copy-start.5
  168.7 9.7 %collective-permute-start.7 = (bf16[8,1536]{1,0:T(8,128)(2,1)}, bf16[8,1536]{1,0:T(8,128)(2,1)S(1)}, u32[]{:S(2)}, u32[]{:S(2)}) collective-permute-start(bf16[8,1536]{1,0:T(8,128)(2,1)} %get-tuple-element.38), channel_id=1, source_target_pairs={{0,1},{1,0},{2,3},{3,2},{4,5},{5,4},{6,7},{7,6},{8,9},{9,8},{10,11... | collective-permute-start | bytes 73736 | tf_op jit(solution)/shard_map/ppermute | solution.py:203
  171.4 7.1 %collective-permute-start.8 = (bf16[2,1536]{1,0:T(2,128)(2,1)S(1)}, bf16[2,1536]{1,0:T(2,128)(2,1)S(1)}, u32[]{:S(2)}, u32[]{:S(2)}) collective-permute-start(bf16[2,1536]{1,0:T(2,128)(2,1)S(1)} %slice.19), channel_id=1, source_target_pairs={{1,8},{9,16},{17,24},{25,32},{33,40},{41,48},{49,56},{57,64},{65,7... | collective-permute-start | bytes 18440 | tf_op jit(solution)/shard_map/ppermute | solution.py:209
  178.4 0.6 copy-start.12
  178.5 0.6 copy-start.8
  179.1 14.4 %copy-start.6 = (bf16[64,2048]{1,0:T(8,128)(2,1)S(1)}, bf16[64,2048]{1,0:T(8,128)(2,1)}, u32[]{:S(2)}) copy-start(bf16[64,2048]{1,0:T(8,128)(2,1)} %get-tuple-element.36) | copy-start | bytes 786436
  179.1 14.6 %copy-start.11 = (f32[2048]{0:T(1024)S(1)}, f32[2048]{0:T(1024)}, u32[]{:S(2)}) copy-start(f32[2048]{0:T(1024)} %param.29) | copy-start | bytes 24580
  183.3 10.1 %all-to-all-start.4 = ((bf16[4,16,2048]{2,1,0:T(8,128)(2,1)}), bf16[4,16,2048]{2,1,0:T(8,128)(2,1)S(1)}, u32[]{:S(2)}, u32[]{:S(2)}) async-start(bf16[4,16,2048]{2,1,0:T(8,128)(2,1)} %bitcast.23), calls=%async_computation.4 | async-start | bytes 524288 | tf_op jit(solution)/shard_map/all_to_all | solution.py:194

commit v3 on v2

--- a/solution.py
+++ b/solution.py
@@ -14,11 +14,11 @@
 PAD = 16
 EPS = 1e-06
 
-M = 4
-SP = ("q", "m", "y")
+SP = ("zq", "zm", "ym", "yq")
 TP = ("g", "xp", "c")
 CHIPS = ("g", "xp")
-SLICES = ("m", "xp")
+SLICES = ("ym", "zm")
+SAME_SLICE = ("yq", "zq")
 BLOCK = 16
 HALF = TGT_DEV // 2
 bf16 = jnp.bfloat16
@@ -80,7 +80,15 @@
     )(queries, own, other)
 
 
-def merge_body(parts_ref, own_ref, other_ref, o_ref):
+def merge_body(parts_hbm, own_hbm, other_hbm, o_ref, parts_ref, held, sem):
+    arrive = pltpu.make_async_copy(parts_hbm, parts_ref, sem.at[2])
+    arrive.start()
+    copies = [
+        pltpu.make_async_copy(w, held.at[k], sem.at[k]) for k, w in enumerate((own_hbm, other_hbm))
+    ]
+    for copy in copies:
+        copy.start()
+    arrive.wait()
     count = parts_ref.shape[0]
     tail = parts_ref[:, TGT_DEV:, :].astype(f32)
     lse = tail[:, 0, :TGT_DEV] + tail[:, 0, TGT_DEV:] + tail[:, 1, :TGT_DEV]
@@ -90,23 +98,41 @@
     for t in range(1, count):
         merged = merged + parts_ref[t, :TGT_DEV, :].astype(f32) * weight[:, t : t + 1]
     merged = merged.astype(bf16)
-    projected = jnp.dot(merged[:HALF], own_ref[...], preferred_element_type=f32)
-    projected += jnp.dot(merged[HALF:], other_ref[...], preferred_element_type=f32)
-    o_ref[...] = projected.astype(bf16)
-
-
-def merge_project(parts, own, other):
+    copies[0].wait()
+    projected = jnp.dot(merged[:HALF], held[0], preferred_element_type=f32)
+    copies[1].wait()
+    projected += jnp.dot(merged[HALF:], held[1], preferred_element_type=f32)
+    projected = projected.astype(bf16)
+    for t in range(o_ref.shape[0]):
+        o_ref[t] = projected
+
+
+def merge_project(parts, own, other, copies):
+    hbm = pl.BlockSpec(memory_space=pl.ANY)
     return pl.pallas_call(
         merge_body,
-        out_shape=jax.ShapeDtypeStruct((HALF, D), bf16),
+        in_specs=[hbm] * 3,
+        out_shape=jax.ShapeDtypeStruct((copies, HALF, D), bf16),
+        scratch_shapes=[
+            pltpu.VMEM(parts.shape, bf16),
+            pltpu.VMEM((2, *own.shape), bf16),
+            pltpu.SemaphoreType.DMA((3,)),
+        ],
     )(parts, own, other)
 
 
-def mixer_in_body(tiles_ref, target_ref, gain_ref, *refs):
-    weights, (res_ref, gu_ref, tails_ref), held, sem = refs[:4], refs[4:7], refs[7], refs[8]
+def mixer_in_body(tiles_hbm, target_hbm, gain_ref, *refs):
+    weights, (res_ref, gu_ref, tails_ref, last_ref) = refs[:4], refs[4:8]
+    tiles_ref, target_ref, held, sem = refs[8:]
+    arrive = [
+        pltpu.make_async_copy(tiles_hbm, tiles_ref, sem.at[4]),
+        pltpu.make_async_copy(target_hbm, target_ref, sem.at[5]),
+    ]
     copies = [pltpu.make_async_copy(w, held.at[k], sem.at[k]) for k, w in enumerate(weights)]
-    for copy in copies:
+    for copy in arrive + copies:
         copy.start()
+    for copy in arrive:
+        copy.wait()
     projected = tiles_ref[0].astype(f32)
     for t in range(1, tiles_ref.shape[0]):
         projected = projected + tiles_ref[t].astype(f32)
@@ -120,6 +146,7 @@
         gu_ref[:, k * width : (k + 1) * width] = part
         last = [part[b + BLOCK - (CONV - 1) : b + BLOCK] for b in range(0, HALF, BLOCK)]
         tails_ref[:, k * width : (k + 1) * width] = jnp.concatenate(last, axis=0)
+        last_ref[:, k * width : (k + 1) * width] = last[-1]
 
 
 def mixer_in(tiles, target, gain, weights):
@@ -129,15 +156,18 @@
     count = len(weights)
     return pl.pallas_call(
         mixer_in_body,
-        in_specs=[vmem, vmem, vmem] + [hbm] * count,
+        in_specs=[hbm, hbm, vmem] + [hbm] * count,
         out_shape=[
             jax.ShapeDtypeStruct((HALF, D), bf16),
             jax.ShapeDtypeStruct((HALF, count * width), bf16),
             jax.ShapeDtypeStruct((HALF // BLOCK * (CONV - 1), count * width), bf16),
+            jax.ShapeDtypeStruct((CONV - 1, count * width), bf16),
         ],
         scratch_shapes=[
+            pltpu.VMEM(tiles.shape, bf16),
+            pltpu.VMEM(target.shape, bf16),
             pltpu.VMEM((count, D, width), bf16),
-            pltpu.SemaphoreType.DMA((count,)),
+            pltpu.SemaphoreType.DMA((count + 2,)),
         ],
     )(tiles, target, gain.reshape(1, D), *weights)
 
@@ -156,18 +186,28 @@
     shifted = jnp.concatenate([before, across[:-halo]], axis=0)
     earlier = jnp.where(first, shifted, across)
 
+    place = lax.broadcasted_iota(jnp.int32, (HALF, width), 0) % BLOCK
+
+    def spread(row, from_at):
+        return jnp.concatenate(
+            [
+                jnp.broadcast_to(
+                    earlier[b * halo + row : b * halo + row + 1, from_at : from_at + width],
+                    (BLOCK, width),
+                )
+                for b in range(HALF // BLOCK)
+            ],
+            axis=0,
+        )
+
     def convolved(at, from_at, tap_row, tap_at):
-        blocks = []
-        for b in range(HALF // BLOCK):
-            ahead = earlier[b * halo : (b + 1) * halo, from_at : from_at + width]
-            here = gu_ref[b * BLOCK : (b + 1) * BLOCK, at : at + width].astype(f32)
-            padded = jnp.concatenate([ahead, here], axis=0)
-            mixed = 0.0
-            for tap in range(CONV):
-                scale = taps_ref[tap_row + tap : tap_row + tap + 1, tap_at : tap_at + width]
-                mixed = mixed + scale * padded[tap : tap + BLOCK]
-            blocks.append(mixed)
-        return jnp.concatenate(blocks, axis=0)
+        here = gu_ref[:, at : at + width].astype(f32)
+        last = spread(1, from_at)
+        one = jnp.where(place == 0, last, pltpu.roll(here, 1, 0))
+        two = jnp.where(place == 1, last, pltpu.roll(here, 2, 0))
+        two = jnp.where(place == 0, spread(0, from_at), two)
+        scale = taps_ref[tap_row : tap_row + CONV, tap_at : tap_at + width]
+        return scale[0:1] * two + scale[1:2] * one + scale[2:3] * here
 
     total = 0.0
     for k, copy in enumerate(copies):
@@ -238,16 +278,14 @@
             jnp.concatenate([key_rows[:, HEAD:], value_rows[:, HEAD:]], axis=1),
         ]
     )
-    quads = lax.axis_size("q")
-    to_send = jnp.broadcast_to(by_head[:, None], (KV_HEADS, quads, rows, 2 * HEAD))
-    near = exchanged(to_send.reshape(KV_HEADS * quads, rows, 2 * HEAD), ("g", "q"))
-    near = near.reshape(KV_HEADS * quads * rows, 2 * HEAD)
-    near, target, out_weight, gate_weight, up_weight, gate_taps, up_taps, down_weight = (
-        lax.optimization_barrier(
-            (near, target, out_weight, gate_weight, up_weight, gate_taps, up_taps, down_weight)
-        )
-    )
-    kv = sent_to_all(near, "y").reshape(-1, 2 * HEAD)
+    near_lines = lax.axis_size(SAME_SLICE)
+    by_head = by_head.reshape(KV_HEADS * rows, 2 * HEAD)
+    near = sent_to_all(by_head, SAME_SLICE)
+    near = near.reshape(near_lines, KV_HEADS, rows, 2 * HEAD).transpose(1, 0, 2, 3)
+    near = near.reshape(KV_HEADS, 1, near_lines * rows, 2 * HEAD)
+    chips = lax.axis_size(CHIPS)
+    near = jnp.broadcast_to(near, (KV_HEADS, chips // KV_HEADS, *near.shape[2:]))
+    kv = exchanged(near.reshape(chips, *near.shape[2:]), CHIPS).reshape(-1, 2 * HEAD)
 
     normed = normalize(target, query_gain)
     own_query = jnp.dot(normed, query_weight, preferred_element_type=f32).astype(bf16)
@@ -255,17 +293,20 @@
     by_core = own_query.reshape(4, 2, BLOCK, HEAD)
     kept = lax.dynamic_index_in_dim(by_core, core, 1, False).reshape(HALF, HEAD)
     given = lax.dynamic_index_in_dim(by_core, 1 - core, 1, False).reshape(HALF, HEAD)
-    both = jnp.stack([kept, other_core(given)])
-    queries = lax.all_gather(both, "xp", axis=0, tiled=True)
-    queries = lax.all_gather(queries, "m", axis=0, tiled=True)
+    given = other_core(given)
+    both = jnp.stack([kept, given])
+    queries = lax.all_gather(both[None], "zm", axis=0, tiled=True)
+    queries = lax.all_gather(queries[None], "ym", axis=0, tiled=True)
+    queries = queries.reshape(-1, HALF, HEAD)
     target_half = lax.dynamic_index_in_dim(target.reshape(4, 2, BLOCK, D), core, 1, False)
     target_half = target_half.reshape(HALF, D)
+    taps = jnp.concatenate([gate_taps, up_taps], axis=0)
     out_other = other_core(out_weight)
     gate_other = other_core(gate_weight)
     up_other = other_core(up_weight)
     down_other = other_core(down_weight)
-    taps = jnp.concatenate([gate_taps, up_taps], axis=0)
-    taps = jnp.concatenate([taps, other_core(taps)], axis=1).astype(f32)
+    taps_other = other_core(taps)
+    taps = jnp.concatenate([taps, taps_other], axis=1).astype(f32)
     queries, target_half, out_other, gate_other, up_other, down_other, taps = (
         lax.optimization_barrier(
             (queries, target_half, out_other, gate_other, up_other, down_other, taps)
@@ -273,14 +314,14 @@
     )
     parts = exchanged(attend(queries, kv, other_core(kv)), SLICES)
     core_at = core.astype(jnp.int32).reshape(1)
-    partial = merge_project(parts, out_weight, out_other)
-    residual, gate_up, tails = mixer_in(
-        sent_to_all(partial, CHIPS),
+    partial = merge_project(parts, out_weight, out_other, chips)
+    residual, gate_up, tails, last = mixer_in(
+        exchanged(partial, CHIPS),
         target_half,
         mixer_gain,
         (gate_weight, gate_other, up_weight, up_other),
     )
-    before = from_last_line(tails[-(CONV - 1) :])
+    before = from_last_line(last)
     across = other_core(tails)
     partial = mixer_out(core_at, gate_up, across, before, taps, down_weight, down_other)
     tiles = exchanged(partial.reshape(HALF // BLOCK, BLOCK, D), CHIPS)
@@ -291,7 +332,7 @@
 
 def solution(mesh):
     lines = mesh.shape["sp"]
-    devices = mesh.devices.reshape(lines // 8 // M, M, 8, 2, 2, 2)
+    devices = mesh.devices.reshape(lines // 32, 4, 2, 4, 2, 2, 2)
     split = Mesh(devices, SP + TP)
     whole = SP + TP
     return jax.shard_map(

time: 195 us -> 208 us (1.067)
  blocking collectives: 86 us -> 125 us
  waiting for transfers between devices: 45.4 us -> 23 us
  starting transfers between devices: 28.5 us -> 26.3 us
    all_to_all x3, blocking collectives: 60 us -> 85.4 us  [exchanged(): return lax.all_to_all(array, axes, 0, 0, tiled=True)]
    all_to_all x2, waiting for transfers between devices: 38.5 us -> 16.2 us  [exchanged(): return lax.all_to_all(array, axes, 0, 0, tiled=True)]
    all_gather x2, blocking collectives: 26 us -> 39.5 us  [the longest x1 24.4 us: shards(): queries = lax.all_gather(both[None], 'zm', axis=0, tiled=True)]
    all_to_all x2, starting transfers between devices: 10.7 us -> 7.9 us  [exchanged(): return lax.all_to_all(array, axes, 0, 0, tiled=True)]
    broadcast_in_dim x2 -> x1, local copies, waits for them, and re-layouts: 2.34 us -> 0.06 us  [sent_to_all(): return exchanged(jnp.broadcast_to(shard, (count, *shard.shape)), axes)]
where the time goes in v3:
time: 208 us; the launch traced here: 207 us
  blocking collectives  125 us (60%)
  starting transfers between devices  26.3 us (13%)
  waiting for transfers between devices  23 us (11%)
  Pallas kernels  21.4 us (10%)
  local copies, waits for them, and re-layouts  4.28 us (2%)
  matrix products  3.57 us (2%)
  other arithmetic  2.94 us (1%)
    all_to_all x3, blocking collectives, exchanged(): return lax.all_to_all(array, axes, 0, 0, tiled=True)  85.4 us
    all_gather x1, blocking collectives, shards(): queries = lax.all_gather(both[None], 'zm', axis=0, tiled=True)  24.4 us
    ppermute x8, starting transfers between devices, other_core(): return lax.ppermute(array, 'c', [(0, 1), (1, 0)])  17.1 us
    all_to_all x2, waiting for transfers between devices, exchanged(): return lax.all_to_all(array, axes, 0, 0, tiled=True)  16.2 us
    all_gather x1, blocking collectives, shards(): queries = lax.all_gather(queries[None], 'ym', axis=0, tiled=True)  15.2 us
    pallas_call x1, Pallas kernels, attend(): pl.pallas_call(attend_body, grid=(blocks // step,), in_specs=[pl.BlockSpe...  8.84 us
    all_to_all x2, starting transfers between devices, exchanged(): return lax.all_to_all(array, axes, 0, 0, tiled=True)  7.9 us
    ppermute x1, waiting for transfers between devices, from_last_line(): lax.ppermute(array, axes, [(2 * i + 1, 2 * i + 2) for i in range(lines -...  5.97 us
  transfers between devices with their start and end apart: 11, of which 4 were waited for; matrix products, arithmetic and copies ran while one was open for 2% of the time, Pallas kernels for 0%

profile of v3, /device:TPU:64, one launch (start us, length us, event | category | flops | bytes accessed | tf_op | source)
XLA Modules:
  0.0 206.9 jit_solution(15580920596531487454)
XLA Ops:
  0.0 1.2 fusion.7
  1.7 1.4 convolution_convert_fusion.1
  3.7 42.2 %all_to_all.25 = bf16[12,64,512]{2,1,0:T(8,128)(2,1)S(1)} all-to-all(bf16[12,64,512]{2,1,0:T(8,128)(2,1)S(1)} %broadcast_in_dim.24), channel_id=1, replica_groups=mesh['zq'=3,'zm'=4,'ym'=2,'yq'=4,'g'=2,'xp'=2,'c'=2] {'yq','zq'}, dimensions={0} | all-to-all | bytes 1572864 | tf_op jit(solution)/shard_map/all_to_all | solution.py:234
  46.0 1.3 broadcast_in_dim.26
  47.3 4.5 %all-to-all-start.1 = ((bf16[4,384,512]{2,1,0:T(8,128)(2,1)}), bf16[4,384,512]{2,1,0:T(8,128)(2,1)}, u32[]{:S(2)}, u32[]{:S(2)}) async-start(bf16[4,384,512]{2,1,0:T(8,128)(2,1)} %bitcast.27), calls=%async_computation.1 | async-start | bytes 3145728 | tf_op jit(solution)/shard_map/all_to_all | solution.py:234
  51.8 1.9 collective-permute-start.5
  53.7 2.4 %collective-permute-start.2 = (bf16[2048,384]{1,0:T(8,128)(2,1)}, bf16[2048,384]{1,0:T(8,128)(2,1)}, u32[]{:S(2)}, u32[]{:S(2)}) collective-permute-start(bf16[2048,384]{1,0:T(8,128)(2,1)} %refs_0_.1), channel_id=1, source_target_pairs={{0,1},{1,0},{2,3},{3,2},{4,5},{5,4},{6,7},{7,6},{8,9},{9,8},{10,11... | collective-permute-start | bytes 4718600 | tf_op jit(solution)/shard_map/ppermute | solution.py:243
  56.1 1.9 collective-permute-start.3
  58.1 2.4 %collective-permute-start.4 = (bf16[384,2048]{1,0:T(8,128)(2,1)}, bf16[384,2048]{1,0:T(8,128)(2,1)}, u32[]{:S(2)}, u32[]{:S(2)}) collective-permute-start(bf16[384,2048]{1,0:T(8,128)(2,1)} %down_ref.1), channel_id=1, source_target_pairs={{0,1},{1,0},{2,3},{3,2},{4,5},{5,4},{6,7},{7,6},{8,9},{9,8},{10,11... | collective-permute-start | bytes 4718600 | tf_op jit(solution)/shard_map/ppermute | solution.py:243
  60.7 9.6 %all-to-all-done.1 = bf16[4,384,512]{2,1,0:T(8,128)(2,1)} async-done(((bf16[4,384,512]{2,1,0:T(8,128)(2,1)}), bf16[4,384,512]{2,1,0:T(8,128)(2,1)}, u32[]{:S(2)}, u32[]{:S(2)}) %all-to-all-start.1) | async-done | bytes 1572896 | tf_op jit(solution)/shard_map/all_to_all | solution.py:234
  70.3 1.9 collective-permute-start.6
  72.2 1.7 fusion
  73.9 2.4 %collective-permute-start = (bf16[64,256]{1,0:T(8,128)(2,1)S(1)}, bf16[64,256]{1,0:T(8,128)(2,1)S(1)}, u32[]{:S(2)}, u32[]{:S(2)}) collective-permute-start(bf16[64,256]{1,0:T(8,128)(2,1)S(1)} %bitcast.39), channel_id=1, source_target_pairs={{0,1},{1,0},{2,3},{3,2},{4,5},{5,4},{6,7},{7,6},{8,9},{9,8},{10,11... | collective-permute-start | bytes 98312 | tf_op jit(solution)/shard_map/ppermute | solution.py:243
  76.3 0.8 collective-permute-done
  77.2 2.2 %collective-permute-start.1 = (bf16[256,2048]{1,0:T(8,128)(2,1)S(1)}, bf16[256,2048]{1,0:T(8,128)(2,1)S(1)}, u32[]{:S(2)}, u32[]{:S(2)}) collective-permute-start(bf16[256,2048]{1,0:T(8,128)(2,1)S(1)} %copy-done.4), channel_id=1, source_target_pairs={{0,1},{1,0},{2,3},{3,2},{4,5},{5,4},{6,7},{7,6},{8,9},{9,8},{10,11... | collective-permute-start | bytes 3145736 | tf_op jit(solution)/shard_map/ppermute | solution.py:243
  79.4 0.7 constant_dynamic-slice_fusion
  80.2 0.6 maximum_convert_fusion.taps_ref
  80.8 24.4 %all-gather = bf16[8,64,256]{2,1,0:T(8,128)(2,1)S(1)} all-gather(bf16[2,64,256]{2,1,0:T(8,128)(2,1)S(1)} %pad_maximum_fusion), channel_id=2, replica_groups=mesh['zq'=3,'zm'=4,'ym'=2,'yq'=4,'g'=2,'xp'=2,'c'=2] {'zm'}, dimensions={0}, use_global_device_ids=true | all-gather | bytes 327680 | tf_op jit(solution)/shard_map/all_gather | solution.py:298
  105.1 15.2 %all-gather.1 = bf16[8,2,64,256]{3,2,1,0:T(8,128)(2,1)} all-gather(bf16[4,2,64,256]{3,2,1,0:T(8,128)(2,1)S(1)} %bitcast.33), channel_id=3, replica_groups=mesh['zq'=3,'zm'=4,'ym'=2,'yq'=4,'g'=2,'xp'=2,'c'=2] {'ym'}, dimensions={0}, use_global_device_ids=true | all-gather | bytes 786432 | tf_op jit(solution)/shard_map/all_gather | solution.py:299
  120.3 1.0 copy-done.5
  121.4 8.8 %shard_map.145 = bf16[8,144,256]{2,1,0:T(8,128)(2,1)} custom-call(bf16[16,64,256]{2,1,0:T(8,128)(2,1)} %bitcast.30, bf16[1536,512]{1,0:T(8,128)(2,1)} %bitcast.15.own_ref, bf16[1536,512]{1,0:T(8,128)(2,1)} %collective-permute-done.6.other_ref), custom_call_target="tpu_custom_call" | custom-call | tf_op jit(solution)/shard_map/pallas_call | solution.py:70
  130.2 25.3 %all_to_all.26.parts_hbm = bf16[8,144,256]{2,1,0:T(8,128)(2,1)} all-to-all(bf16[8,144,256]{2,1,0:T(8,128)(2,1)} %shard_map.145), channel_id=1, replica_groups=mesh['zq'=3,'zm'=4,'ym'=2,'yq'=4,'g'=2,'xp'=2,'c'=2] {'ym','zm'}, dimensions={0} | all-to-all | bytes 1179648 | tf_op jit(solution)/shard_map/all_to_all | solution.py:234
  155.6 3.2 %shard_map.146 = bf16[4,64,2048]{2,1,0:T(8,128)(2,1)} custom-call(bf16[8,144,256]{2,1,0:T(8,128)(2,1)} %all_to_all.26.parts_hbm, bf16[256,2048]{1,0:T(8,128)(2,1)} %own_hbm.1, bf16[256,2048]{1,0:T(8,128)(2,1)} %copy-done.5), custom_call_target="tpu_custom_call" | custom-call | tf_op jit(solution)/shard_map/pallas_call | solution.py:112
  158.8 17.9 %all_to_all.27.tiles_hbm = bf16[4,64,2048]{2,1,0:T(8,128)(2,1)} all-to-all(bf16[4,64,2048]{2,1,0:T(8,128)(2,1)} %shard_map.146), channel_id=1, replica_groups=mesh['zq'=3,'zm'=4,'ym'=2,'yq'=4,'g'=2,'xp'=2,'c'=2] {'g','xp'}, dimensions={0} | all-to-all | bytes 2097152 | tf_op jit(solution)/shard_map/all_to_all | solution.py:234
  176.7 5.1 %shard_map.147 = (bf16[64,2048]{1,0:T(8,128)(2,1)}, bf16[64,1536]{1,0:T(8,128)(2,1)}, bf16[8,1536]{1,0:T(8,128)(2,1)}, bf16[2,1536]{1,0:T(2,128)(2,1)}) custom-call(bf16[4,64,2048]{2,1,0:T(8,128)(2,1)} %all_to_all.27.tiles_hbm, bf16[64,2048]{1,0:T(8,128)(2,1)} %bitcast.32, f32[1,2048]{1,0:T(1,128)} %bitcast.40, bf16[2048,384]{1,0:T(8,128)(2,1)} %refs_0_.1, ...), custom_call_target="tpu_custom_call" | custom-call | tf_op jit(solution)/shard_map/pallas_call | solution.py:157
  181.8 1.9 collective-permute-start.7
  183.7 1.3 collective-permute-start.8
  185.0 6.0 %collective-permute-done.8.before_ref = bf16[2,1536]{1,0:T(2,128)(2,1)S(1)} collective-permute-done((bf16[2,1536]{1,0:T(2,128)(2,1)}, bf16[2,1536]{1,0:T(2,128)(2,1)S(1)}, u32[]{:S(2)}, u32[]{:S(2)}) %collective-permute-start.8) | collective-permute-done | bytes 6176 | tf_op jit(solution)/shard_map/ppermute | solution.py:249
  191.6 4.3 %shard_map.148 = bf16[64,2048]{1,0:T(8,128)(2,1)} custom-call(s32[1]{0:T(128)} %bitcast.17.core_ref, bf16[64,1536]{1,0:T(8,128)(2,1)} %get-tuple-element.22.gu_ref, bf16[8,1536]{1,0:T(8,128)(2,1)} %copy-done.8, bf16[2,1536]{1,0:T(2,128)(2,1)} %copy-done.12, f32[6,768]{1,0:T(8,128)} %maximum_convert_fusion.taps_ref, bf16[384,2048]{1,0:T(8,128)(2,1)} %down_ref.1, ...), custom_call_target="tpu_custom_call" | custom-call | tf_op jit(solution)/shard_map/pallas_call | solution.py:225
  195.9 3.4 %all-to-all-start.4 = ((bf16[4,16,2048]{2,1,0:T(8,128)(2,1)}), bf16[4,16,2048]{2,1,0:T(8,128)(2,1)S(1)}, u32[]{:S(2)}, u32[]{:S(2)}) async-start(bf16[4,16,2048]{2,1,0:T(8,128)(2,1)} %bitcast.34), calls=%async_computation.4 | async-start | bytes 524288 | tf_op jit(solution)/shard_map/all_to_all | solution.py:234
  199.3 6.6 %all-to-all-done.4 = bf16[4,16,2048]{2,1,0:T(8,128)(2,1)S(1)} async-done(((bf16[4,16,2048]{2,1,0:T(8,128)(2,1)}), bf16[4,16,2048]{2,1,0:T(8,128)(2,1)S(1)}, u32[]{:S(2)}, u32[]{:S(2)}) %all-to-all-start.4) | async-done | bytes 262176 | tf_op jit(solution)/shard_map/all_to_all | solution.py:234
  206.1 0.7 multiply_convert_fusion
  (50 shorter events, 2.2 us)
Async XLA Ops:
  0.0 1.7 copy-start
  0.0 3.1 %copy-start.2 = (bf16[32,2048]{1,0:T(8,128)(2,1)S(1)}, bf16[32,2048]{1,0:T(8,128)(2,1)}, u32[]{:S(2)}) copy-start(bf16[32,2048]{1,0:T(8,128)(2,1)} %param.16) | copy-start | bytes 393220
  0.0 3.1 %copy-start.7 = (f32[2048]{0:T(1024)S(1)}, f32[2048]{0:T(1024)}, u32[]{:S(2)}) copy-start(f32[2048]{0:T(1024)} %param.18) | copy-start | bytes 24580
  0.0 3.1 %copy-start.1 = (bf16[2048,512]{1,0:T(8,128)(2,1)S(1)}, bf16[2048,512]{1,0:T(8,128)(2,1)}, u32[]{:S(2)}) copy-start(bf16[2048,512]{1,0:T(8,128)(2,1)} %param.20) | copy-start | bytes 6291460
  47.3 4.5 %copy-start.9 = (bf16[3,384]{1,0:T(4,128)(2,1)S(1)}, bf16[3,384]{1,0:T(4,128)(2,1)}, u32[]{:S(2)}) copy-start(bf16[3,384]{1,0:T(4,128)(2,1)} %param.27) | copy-start | bytes 6916
  47.3 4.5 %copy-start.10 = (bf16[3,384]{1,0:T(4,128)(2,1)S(1)}, bf16[3,384]{1,0:T(4,128)(2,1)}, u32[]{:S(2)}) copy-start(bf16[3,384]{1,0:T(4,128)(2,1)} %param.26) | copy-start | bytes 6916
  47.3 13.2 %copy-start.3 = (bf16[128,2048]{1,0:T(8,128)(2,1)S(1)}, bf16[128,2048]{1,0:T(8,128)(2,1)}, u32[]{:S(2)}) copy-start(bf16[128,2048]{1,0:T(8,128)(2,1)} %param.15) | copy-start | bytes 1572868
  47.3 24.9 %copy-start.13 = (f32[2048]{0:T(1024)S(1)}, f32[2048]{0:T(1024)}, u32[]{:S(2)}) copy-start(f32[2048]{0:T(1024)} %param.17) | copy-start | bytes 24580
  47.3 23.0 %all-to-all-start.1 = ((bf16[4,384,512]{2,1,0:T(8,128)(2,1)}), bf16[4,384,512]{2,1,0:T(8,128)(2,1)}, u32[]{:S(2)}, u32[]{:S(2)}) async-start(bf16[4,384,512]{2,1,0:T(8,128)(2,1)} %bitcast.27), calls=%async_computation.1 | async-start | bytes 3145728 | tf_op jit(solution)/shard_map/all_to_all | solution.py:234
  51.8 22.1 %collective-permute-start.5 = (bf16[6,384]{1,0:T(8,128)(2,1)S(1)}, bf16[6,384]{1,0:T(8,128)(2,1)S(1)}, u32[]{:S(2)}, u32[]{:S(2)}) collective-permute-start(bf16[6,384]{1,0:T(8,128)(2,1)S(1)} %pad_maximum_fusion.2), channel_id=1, source_target_pairs={{0,1},{1,0},{2,3},{3,2},{4,5},{5,4},{6,7},{7,6},{8,9},{9,8},{10,11... | collective-permute-start | bytes 13832 | tf_op jit(solution)/shard_map/ppermute | solution.py:243
  53.7 67.6 %collective-permute-start.2 = (bf16[2048,384]{1,0:T(8,128)(2,1)}, bf16[2048,384]{1,0:T(8,128)(2,1)}, u32[]{:S(2)}, u32[]{:S(2)}) collective-permute-start(bf16[2048,384]{1,0:T(8,128)(2,1)} %refs_0_.1), channel_id=1, source_target_pairs={{0,1},{1,0},{2,3},{3,2},{4,5},{5,4},{6,7},{7,6},{8,9},{9,8},{10,11... | collective-permute-start | bytes 4718600 | tf_op jit(solution)/shard_map/ppermute | solution.py:243
  56.1 65.2 %collective-permute-start.3 = (bf16[2048,384]{1,0:T(8,128)(2,1)}, bf16[2048,384]{1,0:T(8,128)(2,1)}, u32[]{:S(2)}, u32[]{:S(2)}) collective-permute-start(bf16[2048,384]{1,0:T(8,128)(2,1)} %refs_2_.1), channel_id=1, source_target_pairs={{0,1},{1,0},{2,3},{3,2},{4,5},{5,4},{6,7},{7,6},{8,9},{9,8},{10,11... | collective-permute-start | bytes 4718600 | tf_op jit(solution)/shard_map/ppermute | solution.py:243
  58.1 63.3 %collective-permute-start.4 = (bf16[384,2048]{1,0:T(8,128)(2,1)}, bf16[384,2048]{1,0:T(8,128)(2,1)}, u32[]{:S(2)}, u32[]{:S(2)}) collective-permute-start(bf16[384,2048]{1,0:T(8,128)(2,1)} %down_ref.1), channel_id=1, source_target_pairs={{0,1},{1,0},{2,3},{3,2},{4,5},{5,4},{6,7},{7,6},{8,9},{9,8},{10,11... | collective-permute-start | bytes 4718600 | tf_op jit(solution)/shard_map/ppermute | solution.py:243
  70.3 51.1 %collective-permute-start.6 = (bf16[1536,512]{1,0:T(8,128)(2,1)}, bf16[1536,512]{1,0:T(8,128)(2,1)}, u32[]{:S(2)}, u32[]{:S(2)}) collective-permute-start(bf16[1536,512]{1,0:T(8,128)(2,1)} %bitcast.15.own_ref), channel_id=1, source_target_pairs={{0,1},{1,0},{2,3},{3,2},{4,5},{5,4},{6,7},{7,6},{8,9},{9,8},{10,11... | collective-permute-start | bytes 4718600 | tf_op jit(solution)/shard_map/ppermute | solution.py:243
  72.2 5.0 %copy-start.4 = (bf16[256,2048]{1,0:T(8,128)(2,1)S(1)}, bf16[256,2048]{1,0:T(8,128)(2,1)}, u32[]{:S(2)}) copy-start(bf16[256,2048]{1,0:T(8,128)(2,1)} %own_hbm.1) | copy-start | bytes 3145732
  73.9 3.3 %collective-permute-start = (bf16[64,256]{1,0:T(8,128)(2,1)S(1)}, bf16[64,256]{1,0:T(8,128)(2,1)S(1)}, u32[]{:S(2)}, u32[]{:S(2)}) collective-permute-start(bf16[64,256]{1,0:T(8,128)(2,1)S(1)} %bitcast.39), channel_id=1, source_target_pairs={{0,1},{1,0},{2,3},{3,2},{4,5},{5,4},{6,7},{7,6},{8,9},{9,8},{10,11... | collective-permute-start | bytes 98312 | tf_op jit(solution)/shard_map/ppermute | solution.py:243
  77.2 43.2 %collective-permute-start.1 = (bf16[256,2048]{1,0:T(8,128)(2,1)S(1)}, bf16[256,2048]{1,0:T(8,128)(2,1)S(1)}, u32[]{:S(2)}, u32[]{:S(2)}) collective-permute-start(bf16[256,2048]{1,0:T(8,128)(2,1)S(1)} %copy-done.4), channel_id=1, source_target_pairs={{0,1},{1,0},{2,3},{3,2},{4,5},{5,4},{6,7},{7,6},{8,9},{9,8},{10,11... | collective-permute-start | bytes 3145736 | tf_op jit(solution)/shard_map/ppermute | solution.py:243
  120.3 1.0 copy-start.5
  181.8 9.2 %collective-permute-start.7 = (bf16[8,1536]{1,0:T(8,128)(2,1)}, bf16[8,1536]{1,0:T(8,128)(2,1)S(1)}, u32[]{:S(2)}, u32[]{:S(2)}) collective-permute-start(bf16[8,1536]{1,0:T(8,128)(2,1)} %get-tuple-element.23), channel_id=1, source_target_pairs={{0,1},{1,0},{2,3},{3,2},{4,5},{5,4},{6,7},{7,6},{8,9},{9,8},{10,11... | collective-permute-start | bytes 73736 | tf_op jit(solution)/shard_map/ppermute | solution.py:243
  183.7 7.3 %collective-permute-start.8 = (bf16[2,1536]{1,0:T(2,128)(2,1)}, bf16[2,1536]{1,0:T(2,128)(2,1)S(1)}, u32[]{:S(2)}, u32[]{:S(2)}) collective-permute-start(bf16[2,1536]{1,0:T(2,128)(2,1)} %get-tuple-element.24), channel_id=1, source_target_pairs={{1,8},{9,16},{17,24},{25,32},{33,40},{41,48},{49,56},{57,64},{65,7... | collective-permute-start | bytes 18440 | tf_op jit(solution)/shard_map/ppermute | solution.py:249
  191.0 0.6 copy-start.12
  191.0 0.6 copy-start.8
  191.6 14.4 %copy-start.6 = (bf16[64,2048]{1,0:T(8,128)(2,1)S(1)}, bf16[64,2048]{1,0:T(8,128)(2,1)}, u32[]{:S(2)}) copy-start(bf16[64,2048]{1,0:T(8,128)(2,1)} %get-tuple-element.21) | copy-start | bytes 786436
  191.6 14.5 %copy-start.11 = (f32[2048]{0:T(1024)S(1)}, f32[2048]{0:T(1024)}, u32[]{:S(2)}) copy-start(f32[2048]{0:T(1024)} %param.29) | copy-start | bytes 24580
  195.9 10.1 %all-to-all-start.4 = ((bf16[4,16,2048]{2,1,0:T(8,128)(2,1)}), bf16[4,16,2048]{2,1,0:T(8,128)(2,1)S(1)}, u32[]{:S(2)}, u32[]{:S(2)}) async-start(bf16[4,16,2048]{2,1,0:T(8,128)(2,1)} %bitcast.34), calls=%async_computation.4 | async-start | bytes 524288 | tf_op jit(solution)/shard_map/all_to_all | solution.py:234

commit v4 on v3

--- a/solution.py
+++ b/solution.py
@@ -17,7 +17,7 @@
 SP = ("zq", "zm", "ym", "yq")
 TP = ("g", "xp", "c")
 CHIPS = ("g", "xp")
-SLICES = ("ym", "zm")
+SLICES = ("zm", "ym")
 SAME_SLICE = ("yq", "zq")
 BLOCK = 16
 HALF = TGT_DEV // 2
@@ -31,11 +31,17 @@
     return (scaled * gain).astype(bf16)
 
 
-def attend_body(q_ref, own_ref, other_ref, o_ref):
+def attend_body(line_ref, q_ref, own_ref, other_ref, o_ref):
     sources = (own_ref, other_ref)
     row = lax.broadcasted_iota(jnp.int32, (PAD, HEAD), 0)
-    for at in range(0, q_ref.shape[0], 4):
-        q = q_ref[at : at + 4].reshape(4 * HALF, HEAD)
+    lines = q_ref.shape[0] // 2
+    base = pl.program_id(0) * o_ref.shape[0]
+    for at in range(0, o_ref.shape[0] * 2, 4):
+        pieces = [
+            q_ref[pl.ds(2 * ((line_ref[0] + lines - (base + at // 2 + b)) % lines), 2)]
+            for b in range(2)
+        ]
+        q = jnp.concatenate(pieces, axis=0).reshape(4 * HALF, HEAD)
         scores = [
             lax.dot_general(
                 q, kv[:, :HEAD], (((1,), (1,)), ((), ())), preferred_element_type=f32
@@ -65,30 +71,29 @@
             o_ref[at // 2 + b, TGT_DEV:, :] = tile.astype(bf16)
 
 
-def attend(queries, own, other, step=8):
-    blocks = queries.shape[0]
+def attend(line, queries, own, other, step=4):
+    blocks = queries.shape[0] // 2
+    whole = pl.BlockSpec(queries.shape, lambda i: (0, 0, 0))
     return pl.pallas_call(
         attend_body,
         grid=(blocks // step,),
         in_specs=[
-            pl.BlockSpec((step, HALF, HEAD), lambda i: (i, 0, 0)),
+            pl.BlockSpec(memory_space=pltpu.SMEM),
+            whole,
             pl.BlockSpec(own.shape, lambda i: (0, 0)),
             pl.BlockSpec(other.shape, lambda i: (0, 0)),
         ],
-        out_specs=pl.BlockSpec((step // 2, TGT_DEV + PAD, HEAD), lambda i: (i, 0, 0)),
-        out_shape=jax.ShapeDtypeStruct((blocks // 2, TGT_DEV + PAD, HEAD), bf16),
-    )(queries, own, other)
-
-
-def merge_body(parts_hbm, own_hbm, other_hbm, o_ref, parts_ref, held, sem):
-    arrive = pltpu.make_async_copy(parts_hbm, parts_ref, sem.at[2])
-    arrive.start()
+        out_specs=pl.BlockSpec((step, TGT_DEV + PAD, HEAD), lambda i: (i, 0, 0)),
+        out_shape=pltpu.VMEM((blocks, TGT_DEV + PAD, HEAD), bf16),
+    )(line, queries, own, other)
+
+
+def merge_body(parts_ref, own_hbm, other_hbm, o_ref, held, sem):
     copies = [
         pltpu.make_async_copy(w, held.at[k], sem.at[k]) for k, w in enumerate((own_hbm, other_hbm))
     ]
     for copy in copies:
         copy.start()
-    arrive.wait()
     count = parts_ref.shape[0]
     tail = parts_ref[:, TGT_DEV:, :].astype(f32)
     lse = tail[:, 0, :TGT_DEV] + tail[:, 0, TGT_DEV:] + tail[:, 1, :TGT_DEV]
@@ -107,32 +112,29 @@
         o_ref[t] = projected
 
 
+def in_vmem(array):
+    return pltpu.with_memory_space_constraint(array, pltpu.VMEM)
+
+
 def merge_project(parts, own, other, copies):
     hbm = pl.BlockSpec(memory_space=pl.ANY)
     return pl.pallas_call(
         merge_body,
-        in_specs=[hbm] * 3,
+        in_specs=[pl.BlockSpec(memory_space=pltpu.VMEM), hbm, hbm],
         out_shape=jax.ShapeDtypeStruct((copies, HALF, D), bf16),
-        scratch_shapes=[
-            pltpu.VMEM(parts.shape, bf16),
-            pltpu.VMEM((2, *own.shape), bf16),
-            pltpu.SemaphoreType.DMA((3,)),
-        ],
-    )(parts, own, other)
-
-
-def mixer_in_body(tiles_hbm, target_hbm, gain_ref, *refs):
+        scratch_shapes=[pltpu.VMEM((2, *own.shape), bf16), pltpu.SemaphoreType.DMA((2,))],
+    )(in_vmem(parts), own, other)
+
+
+def mixer_in_body(tiles_ref, target_hbm, gain_ref, *refs):
     weights, (res_ref, gu_ref, tails_ref, last_ref) = refs[:4], refs[4:8]
-    tiles_ref, target_ref, held, sem = refs[8:]
-    arrive = [
-        pltpu.make_async_copy(tiles_hbm, tiles_ref, sem.at[4]),
-        pltpu.make_async_copy(target_hbm, target_ref, sem.at[5]),
-    ]
+    target_ref, held, sem = refs[8:]
+    arrive = pltpu.make_async_copy(target_hbm, target_ref, sem.at[4])
+    arrive.start()
     copies = [pltpu.make_async_copy(w, held.at[k], sem.at[k]) for k, w in enumerate(weights)]
-    for copy in arrive + copies:
+    for copy in copies:
         copy.start()
-    for copy in arrive:
-        copy.wait()
+    arrive.wait()
     projected = tiles_ref[0].astype(f32)
     for t in range(1, tiles_ref.shape[0]):
         projected = projected + tiles_ref[t].astype(f32)
@@ -156,20 +158,19 @@
     count = len(weights)
     return pl.pallas_call(
         mixer_in_body,
-        in_specs=[hbm, hbm, vmem] + [hbm] * count,
+        in_specs=[vmem, hbm, vmem] + [hbm] * count,
         out_shape=[
-            jax.ShapeDtypeStruct((HALF, D), bf16),
-            jax.ShapeDtypeStruct((HALF, count * width), bf16),
-            jax.ShapeDtypeStruct((HALF // BLOCK * (CONV - 1), count * width), bf16),
-            jax.ShapeDtypeStruct((CONV - 1, count * width), bf16),
+            pltpu.VMEM((HALF, D), bf16),
+            pltpu.VMEM((HALF, count * width), bf16),
+            pltpu.VMEM((HALF // BLOCK * (CONV - 1), count * width), bf16),
+            pltpu.VMEM((CONV - 1, count * width), bf16),
         ],
         scratch_shapes=[
-            pltpu.VMEM(tiles.shape, bf16),
             pltpu.VMEM(target.shape, bf16),
             pltpu.VMEM((count, D, width), bf16),
-            pltpu.SemaphoreType.DMA((count + 2,)),
+            pltpu.SemaphoreType.DMA((count + 1,)),
         ],
-    )(tiles, target, gain.reshape(1, D), *weights)
+    )(in_vmem(tiles), target, gain.reshape(1, D), *weights)
 
 
 def mixer_out_body(core_ref, gu_ref, across_ref, before_ref, taps_ref, down_ref, other_ref, o_ref, held, sem):
@@ -225,9 +226,9 @@
     return pl.pallas_call(
         mixer_out_body,
         in_specs=[pl.BlockSpec(memory_space=pltpu.SMEM), vmem, vmem, vmem, vmem, hbm, hbm],
-        out_shape=jax.ShapeDtypeStruct((HALF, D), bf16),
+        out_shape=pltpu.VMEM((HALF, D), bf16),
         scratch_shapes=[pltpu.VMEM((2, *down.shape), bf16), pltpu.SemaphoreType.DMA((2,))],
-    )(core, gate_up, across, before, taps, down, other)
+    )(core, in_vmem(gate_up), in_vmem(across), in_vmem(before), taps, down, other)
 
 
 def exchanged(array, axes):
@@ -295,9 +296,12 @@
     given = lax.dynamic_index_in_dim(by_core, 1 - core, 1, False).reshape(HALF, HEAD)
     given = other_core(given)
     both = jnp.stack([kept, given])
-    queries = lax.all_gather(both[None], "zm", axis=0, tiled=True)
-    queries = lax.all_gather(queries[None], "ym", axis=0, tiled=True)
-    queries = queries.reshape(-1, HALF, HEAD)
+    lines = lax.axis_size(SLICES)
+    queries = [both]
+    for by in range(1, lines):
+        pairs = [(i, (i + by) % lines) for i in range(lines)]
+        queries.append(lax.ppermute(both, SLICES, pairs))
+    queries = jnp.concatenate(queries, axis=0)
     target_half = lax.dynamic_index_in_dim(target.reshape(4, 2, BLOCK, D), core, 1, False)
     target_half = target_half.reshape(HALF, D)
     taps = jnp.concatenate([gate_taps, up_taps], axis=0)
@@ -312,7 +316,8 @@
             (queries, target_half, out_other, gate_other, up_other, down_other, taps)
         )
     )
-    parts = exchanged(attend(queries, kv, other_core(kv)), SLICES)
+    line_at = lax.axis_index(SLICES).astype(jnp.int32).reshape(1)
+    parts = exchanged(attend(line_at, queries, kv, other_core(kv)), SLICES)
     core_at = core.astype(jnp.int32).reshape(1)
     partial = merge_project(parts, out_weight, out_other, chips)
     residual, gate_up, tails, last = mixer_in(

time: 208 us -> 217 us (1.043)
  starting transfers between devices: 26.3 us -> 65.3 us
  blocking collectives: 125 us -> 88.9 us
  waiting for transfers between devices: 23 us -> 30.3 us
    all_gather x2 -> x0, blocking collectives: 39.5 us -> none  [the longest x1 24.4 us: shards(): queries = lax.all_gather(both[None], 'zm', axis=0, tiled=True)]
    ppermute x0 -> x7, starting transfers between devices: none -> 39.5 us  [shards(): queries.append(lax.ppermute(both, SLICES, pairs))]
    ppermute x0 -> x7, waiting for transfers between devices: none -> 15.2 us  [shards(): queries.append(lax.ppermute(both, SLICES, pairs))]
    all_to_all x2, waiting for transfers between devices: 16.2 us -> 6.64 us  [exchanged(): return lax.all_to_all(array, axes, 0, 0, tiled=True)]
    all_to_all x3, blocking collectives: 85.4 us -> 88.9 us  [exchanged(): return lax.all_to_all(array, axes, 0, 0, tiled=True)]
  transfers between devices with their start and end apart: 11 -> 18, of which waited for: 4 -> 8; matrix products, arithmetic and copies ran while one was open for 2% -> 2% of each run, Pallas kernels for 0% -> 0%
where the time goes in v4:
time: 217 us; the launch traced here: 216 us
  blocking collectives  88.9 us (41%)
  starting transfers between devices  65.3 us (30%)
  waiting for transfers between devices  30.3 us (14%)
  Pallas kernels  19.4 us (9%)
  local copies, waits for them, and re-layouts  5.57 us (3%)
  matrix products  3.06 us (1%)
  other arithmetic  2.95 us (1%)
    all_to_all x3, blocking collectives, exchanged(): return lax.all_to_all(array, axes, 0, 0, tiled=True)  88.9 us
    ppermute x7, starting transfers between devices, shards(): queries.append(lax.ppermute(both, SLICES, pairs))  39.5 us
    ppermute x8, starting transfers between devices, other_core(): return lax.ppermute(array, 'c', [(0, 1), (1, 0)])  16.3 us
    ppermute x7, waiting for transfers between devices, shards(): queries.append(lax.ppermute(both, SLICES, pairs))  15.2 us
    pallas_call x1, Pallas kernels, attend(): pl.pallas_call(attend_body, grid=(blocks // step,), in_specs=[pl.BlockSpe...  8.19 us
    all_to_all x2, starting transfers between devices, exchanged(): return lax.all_to_all(array, axes, 0, 0, tiled=True)  8.15 us
    all_to_all x2, waiting for transfers between devices, exchanged(): return lax.all_to_all(array, axes, 0, 0, tiled=True)  6.64 us
    ppermute x1, waiting for transfers between devices, from_last_line(): lax.ppermute(array, axes, [(2 * i + 1, 2 * i + 2) for i in range(lines -...  5.76 us
  transfers between devices with their start and end apart: 18, of which 8 were waited for; matrix products, arithmetic and copies ran while one was open for 2% of the time, Pallas kernels for 0%

profile of v4, /device:TPU:64, one launch (start us, length us, event | category | flops | bytes accessed | tf_op | source)
XLA Modules:
  0.0 215.9 jit_solution(11162051587324566241)
XLA Ops:
  1.2 2.2 %convolution_convert_fusion.1 = bf16[32,512]{1,0:T(8,128)(2,1)S(1)} fusion(bf16[2048,512]{1,0:T(8,128)(2,1)} %param.21, bf16[32,2048]{1,0:T(8,128)(2,1)} %param.16, f32[2048]{0:T(1024)} %param.18, f32[32]{0:T(128)S(1)} %add_rsqrt_fusion.1), kind=kOutput, calls=%fused_computation.4 | convolution fusion | flops 67387392 | bytes 2269312 | tf_op jit(solution)/shard_map/dot_general | solution.py:274
  4.1 42.2 %all_to_all.25 = bf16[12,64,512]{2,1,0:T(8,128)(2,1)S(1)} all-to-all(bf16[12,64,512]{2,1,0:T(8,128)(2,1)S(1)} %broadcast_in_dim.6), channel_id=1, replica_groups=mesh['zq'=3,'zm'=4,'ym'=2,'yq'=4,'g'=2,'xp'=2,'c'=2] {'yq','zq'}, dimensions={0} | all-to-all | bytes 1572864 | tf_op jit(solution)/shard_map/all_to_all | solution.py:235
  46.3 1.3 broadcast_in_dim.8
  47.6 4.7 %all-to-all-start.1 = ((bf16[4,384,512]{2,1,0:T(8,128)(2,1)}), bf16[4,384,512]{2,1,0:T(8,128)(2,1)}, u32[]{:S(2)}, u32[]{:S(2)}) async-start(bf16[4,384,512]{2,1,0:T(8,128)(2,1)} %bitcast.13), calls=%async_computation.1 | async-start | bytes 3145728 | tf_op jit(solution)/shard_map/all_to_all | solution.py:235
  53.0 1.9 collective-permute-start
  56.1 6.0 %collective-permute-start.7 = (bf16[2,64,256]{2,1,0:T(8,128)(2,1)S(1)}, bf16[2,64,256]{2,1,0:T(8,128)(2,1)S(1)}, u32[]{:S(2)}, u32[]{:S(2)}) collective-permute-start(bf16[2,64,256]{2,1,0:T(8,128)(2,1)S(1)} %pad_maximum_fusion), channel_id=1, source_target_pairs={{0,224},{32,0},{64,32},{96,64},{128,96},{160,128},{192,160},{224,1... | collective-permute-start | bytes 196616 | tf_op jit(solution)/shard_map/ppermute | solution.py:303
  62.1 11.7 %collective-permute-start.6 = (bf16[2,64,256]{2,1,0:T(8,128)(2,1)S(1)}, bf16[2,64,256]{2,1,0:T(8,128)(2,1)S(1)}, u32[]{:S(2)}, u32[]{:S(2)}) collective-permute-start(bf16[2,64,256]{2,1,0:T(8,128)(2,1)S(1)} %pad_maximum_fusion), channel_id=1, source_target_pairs={{0,192},{32,224},{64,0},{96,32},{128,64},{160,96},{192,128},{224,1... | collective-permute-start | bytes 196616 | tf_op jit(solution)/shard_map/ppermute | solution.py:303
  73.8 3.3 %collective-permute-start.5 = (bf16[2,64,256]{2,1,0:T(8,128)(2,1)S(1)}, bf16[2,64,256]{2,1,0:T(8,128)(2,1)S(1)}, u32[]{:S(2)}, u32[]{:S(2)}) collective-permute-start(bf16[2,64,256]{2,1,0:T(8,128)(2,1)S(1)} %pad_maximum_fusion), channel_id=1, source_target_pairs={{0,160},{32,192},{64,224},{96,0},{128,32},{160,64},{192,96},{224,1... | collective-permute-start | bytes 196616 | tf_op jit(solution)/shard_map/ppermute | solution.py:303
  77.1 1.9 collective-permute-start.4
  79.0 1.9 collective-permute-start.12
  82.1 2.1 collective-permute-start.9
  84.2 2.3 %collective-permute-start.10 = (bf16[2048,384]{1,0:T(8,128)(2,1)}, bf16[2048,384]{1,0:T(8,128)(2,1)}, u32[]{:S(2)}, u32[]{:S(2)}) collective-permute-start(bf16[2048,384]{1,0:T(8,128)(2,1)} %refs_2_.1), channel_id=1, source_target_pairs={{0,1},{1,0},{2,3},{3,2},{4,5},{5,4},{6,7},{7,6},{8,9},{9,8},{10,11... | collective-permute-start | bytes 4718600 | tf_op jit(solution)/shard_map/ppermute | solution.py:244
  86.5 2.1 collective-permute-start.11
  88.6 2.3 %collective-permute-start.13 = (bf16[1536,512]{1,0:T(8,128)(2,1)}, bf16[1536,512]{1,0:T(8,128)(2,1)}, u32[]{:S(2)}, u32[]{:S(2)}) collective-permute-start(bf16[1536,512]{1,0:T(8,128)(2,1)} %bitcast.14.own_ref), channel_id=1, source_target_pairs={{0,1},{1,0},{2,3},{3,2},{4,5},{5,4},{6,7},{7,6},{8,9},{9,8},{10,11... | collective-permute-start | bytes 4718600 | tf_op jit(solution)/shard_map/ppermute | solution.py:244
  90.8 7.4 %collective-permute-start.3 = (bf16[2,64,256]{2,1,0:T(8,128)(2,1)S(1)}, bf16[2,64,256]{2,1,0:T(8,128)(2,1)S(1)}, u32[]{:S(2)}, u32[]{:S(2)}) collective-permute-start(bf16[2,64,256]{2,1,0:T(8,128)(2,1)S(1)} %pad_maximum_fusion), channel_id=1, source_target_pairs={{0,96},{32,128},{64,160},{96,192},{128,224},{160,0},{192,32},{224,... | collective-permute-start | bytes 196616 | tf_op jit(solution)/shard_map/ppermute | solution.py:303
  98.2 5.4 %collective-permute-done.3 = bf16[2,64,256]{2,1,0:T(8,128)(2,1)S(1)} collective-permute-done((bf16[2,64,256]{2,1,0:T(8,128)(2,1)S(1)}, bf16[2,64,256]{2,1,0:T(8,128)(2,1)S(1)}, u32[]{:S(2)}, u32[]{:S(2)}) %collective-permute-start.3) | collective-permute-done | bytes 65568 | tf_op jit(solution)/shard_map/ppermute | solution.py:303
  104.3 4.0 %collective-permute-start.2 = (bf16[2,64,256]{2,1,0:T(8,128)(2,1)S(1)}, bf16[2,64,256]{2,1,0:T(8,128)(2,1)}, u32[]{:S(2)}, u32[]{:S(2)}) collective-permute-start(bf16[2,64,256]{2,1,0:T(8,128)(2,1)S(1)} %pad_maximum_fusion), channel_id=1, source_target_pairs={{0,64},{32,96},{64,128},{96,160},{128,192},{160,224},{192,0},{224,... | collective-permute-start | bytes 196616 | tf_op jit(solution)/shard_map/ppermute | solution.py:303
  109.1 3.6 %collective-permute-done.2 = bf16[2,64,256]{2,1,0:T(8,128)(2,1)} collective-permute-done((bf16[2,64,256]{2,1,0:T(8,128)(2,1)S(1)}, bf16[2,64,256]{2,1,0:T(8,128)(2,1)}, u32[]{:S(2)}, u32[]{:S(2)}) %collective-permute-start.2) | collective-permute-done | bytes 65568 | tf_op jit(solution)/shard_map/ppermute | solution.py:303
  112.7 5.2 %collective-permute-start.1 = (bf16[2,64,256]{2,1,0:T(8,128)(2,1)S(1)}, bf16[2,64,256]{2,1,0:T(8,128)(2,1)S(1)}, u32[]{:S(2)}, u32[]{:S(2)}) collective-permute-start(bf16[2,64,256]{2,1,0:T(8,128)(2,1)S(1)} %pad_maximum_fusion), channel_id=1, source_target_pairs={{0,32},{32,64},{64,96},{96,128},{128,160},{160,192},{192,224},{224... | collective-permute-start | bytes 196616 | tf_op jit(solution)/shard_map/ppermute | solution.py:303
  117.9 6.1 %collective-permute-done.1 = bf16[2,64,256]{2,1,0:T(8,128)(2,1)S(1)} collective-permute-done((bf16[2,64,256]{2,1,0:T(8,128)(2,1)S(1)}, bf16[2,64,256]{2,1,0:T(8,128)(2,1)S(1)}, u32[]{:S(2)}, u32[]{:S(2)}) %collective-permute-start.1) | collective-permute-done | bytes 65568 | tf_op jit(solution)/shard_map/ppermute | solution.py:303
  124.0 1.9 collective-permute-start.8
  129.8 8.2 %shard_map.145 = bf16[8,144,256]{2,1,0:T(8,128)(2,1)S(1)} custom-call(s32[1]{0:T(128)} %bitcast.line_ref, bf16[16,64,256]{2,1,0:T(8,128)(2,1)} %copy-done.6, bf16[1536,512]{1,0:T(8,128)(2,1)} %bitcast.14.own_ref, bf16[1536,512]{1,0:T(8,128)(2,1)} %collective-permute-done.13.other_ref), custom_call_target="tpu_custom_call" | custom-call | tf_op jit(solution)/shard_map/pallas_call | solution.py:77
  138.0 27.5 %all_to_all.26.parts_ref = bf16[8,144,256]{2,1,0:T(8,128)(2,1)S(1)} all-to-all(bf16[8,144,256]{2,1,0:T(8,128)(2,1)S(1)} %shard_map.145), channel_id=1, replica_groups=mesh['zq'=3,'zm'=4,'ym'=2,'yq'=4,'g'=2,'xp'=2,'c'=2] {'zm','ym'}, dimensions={0} | all-to-all | bytes 1179648 | tf_op jit(solution)/shard_map/all_to_all | solution.py:235
  165.5 3.0 %shard_map.146 = bf16[4,64,2048]{2,1,0:T(8,128)(2,1)} custom-call(bf16[8,144,256]{2,1,0:T(8,128)(2,1)S(1)} %all_to_all.26.parts_ref, bf16[256,2048]{1,0:T(8,128)(2,1)} %own_hbm.1, bf16[256,2048]{1,0:T(8,128)(2,1)} %copy-done.5), custom_call_target="tpu_custom_call" | custom-call | tf_op jit(solution)/shard_map/pallas_call | solution.py:121
  168.5 19.3 %all_to_all.27.tiles_ref = bf16[4,64,2048]{2,1,0:T(8,128)(2,1)S(1)} all-to-all(bf16[4,64,2048]{2,1,0:T(8,128)(2,1)} %shard_map.146), channel_id=1, replica_groups=mesh['zq'=3,'zm'=4,'ym'=2,'yq'=4,'g'=2,'xp'=2,'c'=2] {'g','xp'}, dimensions={0} | all-to-all | bytes 2097152 | tf_op jit(solution)/shard_map/all_to_all | solution.py:235
  187.8 4.1 %shard_map.147 = (bf16[64,2048]{1,0:T(8,128)(2,1)S(1)}, bf16[64,1536]{1,0:T(8,128)(2,1)S(1)}, bf16[8,1536]{1,0:T(8,128)(2,1)S(1)}, bf16[2,1536]{1,0:T(2,128)(2,1)S(1)}) custom-call(bf16[4,64,2048]{2,1,0:T(8,128)(2,1)S(1)} %all_to_all.27.tiles_ref, bf16[64,2048]{1,0:T(8,128)(2,1)} %bitcast.34, f32[1,2048]{1,0:T(1,128)} %bitcast.41, ...), custom_call_target="tpu_custom_call" | custom-call | tf_op jit(solution)/shard_map/pallas_call | solution.py:159
  191.9 1.9 collective-permute-start.14
  193.8 1.3 collective-permute-start.15
  195.1 5.8 %collective-permute-done.15.before_ref = bf16[2,1536]{1,0:T(2,128)(2,1)S(1)} collective-permute-done((bf16[2,1536]{1,0:T(2,128)(2,1)S(1)}, bf16[2,1536]{1,0:T(2,128)(2,1)S(1)}, u32[]{:S(2)}, u32[]{:S(2)}) %collective-permute-start.15) | collective-permute-done | bytes 6176 | tf_op jit(solution)/shard_map/ppermute | solution.py:250
  200.9 4.0 %shard_map.148 = bf16[64,2048]{1,0:T(8,128)(2,1)} custom-call(s32[1]{0:T(128)} %bitcast.16.core_ref, bf16[64,1536]{1,0:T(8,128)(2,1)S(1)} %get-tuple-element.22.gu_ref, bf16[8,1536]{1,0:T(8,128)(2,1)S(1)} %collective-permute-done.14.across_ref, bf16[2,1536]{1,0:T(2,128)(2,1)S(1)} %collective-permute-done.15.before_ref, ...), custom_call_target="tpu_custom_call" | custom-call | tf_op jit(solution)/shard_map/pallas_call | solution.py:226
  205.0 3.4 %all-to-all-start.4 = ((bf16[4,16,2048]{2,1,0:T(8,128)(2,1)}), bf16[4,16,2048]{2,1,0:T(8,128)(2,1)S(1)}, u32[]{:S(2)}, u32[]{:S(2)}) async-start(bf16[4,16,2048]{2,1,0:T(8,128)(2,1)} %bitcast.17), calls=%async_computation.4 | async-start | bytes 524288 | tf_op jit(solution)/shard_map/all_to_all | solution.py:235
  208.4 6.6 %all-to-all-done.4 = bf16[4,16,2048]{2,1,0:T(8,128)(2,1)S(1)} async-done(((bf16[4,16,2048]{2,1,0:T(8,128)(2,1)}), bf16[4,16,2048]{2,1,0:T(8,128)(2,1)S(1)}, u32[]{:S(2)}, u32[]{:S(2)}) %all-to-all-start.4) | async-done | bytes 262176 | tf_op jit(solution)/shard_map/all_to_all | solution.py:235
  (69 shorter events, 10.9 us)
Async XLA Ops:
  0.0 52.6 %copy-start = (bf16[2048,256]{1,0:T(8,128)(2,1)S(1)}, bf16[2048,256]{1,0:T(8,128)(2,1)}, u32[]{:S(2)}) copy-start(bf16[2048,256]{1,0:T(8,128)(2,1)} %param.19) | copy-start | bytes 3145732
  0.0 3.4 %copy-start.3 = (bf16[32,2048]{1,0:T(8,128)(2,1)S(1)}, bf16[32,2048]{1,0:T(8,128)(2,1)}, u32[]{:S(2)}) copy-start(bf16[32,2048]{1,0:T(8,128)(2,1)} %param.16) | copy-start | bytes 393220
  0.0 3.4 %copy-start.8 = (f32[2048]{0:T(1024)S(1)}, f32[2048]{0:T(1024)}, u32[]{:S(2)}) copy-start(f32[2048]{0:T(1024)} %param.18) | copy-start | bytes 24580
  0.0 3.4 %copy-start.1 = (bf16[2048,512]{1,0:T(8,128)(2,1)S(1)}, bf16[2048,512]{1,0:T(8,128)(2,1)}, u32[]{:S(2)}) copy-start(bf16[2048,512]{1,0:T(8,128)(2,1)} %param.20) | copy-start | bytes 6291460
  47.6 4.8 %copy-start.4 = (bf16[128,2048]{1,0:T(8,128)(2,1)S(1)}, bf16[128,2048]{1,0:T(8,128)(2,1)}, u32[]{:S(2)}) copy-start(bf16[128,2048]{1,0:T(8,128)(2,1)} %param.15) | copy-start | bytes 1572868
  47.6 5.0 %copy-start.12 = (f32[2048]{0:T(1024)S(1)}, f32[2048]{0:T(1024)}, u32[]{:S(2)}) copy-start(f32[2048]{0:T(1024)} %param.17) | copy-start | bytes 24580
  47.6 41.0 %all-to-all-start.1 = ((bf16[4,384,512]{2,1,0:T(8,128)(2,1)}), bf16[4,384,512]{2,1,0:T(8,128)(2,1)}, u32[]{:S(2)}, u32[]{:S(2)}) async-start(bf16[4,384,512]{2,1,0:T(8,128)(2,1)} %bitcast.13), calls=%async_computation.1 | async-start | bytes 3145728 | tf_op jit(solution)/shard_map/all_to_all | solution.py:235
  52.3 26.7 %copy-start.9 = (bf16[3,384]{1,0:T(4,128)(2,1)S(1)}, bf16[3,384]{1,0:T(4,128)(2,1)}, u32[]{:S(2)}) copy-start(bf16[3,384]{1,0:T(4,128)(2,1)} %param.27) | copy-start | bytes 6916
  52.3 26.7 %copy-start.10 = (bf16[3,384]{1,0:T(4,128)(2,1)S(1)}, bf16[3,384]{1,0:T(4,128)(2,1)}, u32[]{:S(2)}) copy-start(bf16[3,384]{1,0:T(4,128)(2,1)} %param.26) | copy-start | bytes 6916
  52.3 34.1 %copy-start.2 = (bf16[384,2048]{1,0:T(8,128)(2,1)S(1)}, bf16[384,2048]{1,0:T(8,128)(2,1)}, u32[]{:S(2)}) copy-start(bf16[384,2048]{1,0:T(8,128)(2,1)} %down_ref.1) | copy-start | bytes 4718596
  53.0 3.1 %collective-permute-start = (bf16[64,256]{1,0:T(8,128)(2,1)S(1)}, bf16[64,256]{1,0:T(8,128)(2,1)S(1)}, u32[]{:S(2)}, u32[]{:S(2)}) collective-permute-start(bf16[64,256]{1,0:T(8,128)(2,1)S(1)} %bitcast.40), channel_id=1, source_target_pairs={{0,1},{1,0},{2,3},{3,2},{4,5},{5,4},{6,7},{7,6},{8,9},{9,8},{10,11... | collective-permute-start | bytes 98312 | tf_op jit(solution)/shard_map/ppermute | solution.py:244
  56.1 28.1 %collective-permute-start.7 = (bf16[2,64,256]{2,1,0:T(8,128)(2,1)S(1)}, bf16[2,64,256]{2,1,0:T(8,128)(2,1)S(1)}, u32[]{:S(2)}, u32[]{:S(2)}) collective-permute-start(bf16[2,64,256]{2,1,0:T(8,128)(2,1)S(1)} %pad_maximum_fusion), channel_id=1, source_target_pairs={{0,224},{32,0},{64,32},{96,64},{128,96},{160,128},{192,160},{224,1... | collective-permute-start | bytes 196616 | tf_op jit(solution)/shard_map/ppermute | solution.py:303
  62.1 24.3 %collective-permute-start.6 = (bf16[2,64,256]{2,1,0:T(8,128)(2,1)S(1)}, bf16[2,64,256]{2,1,0:T(8,128)(2,1)S(1)}, u32[]{:S(2)}, u32[]{:S(2)}) collective-permute-start(bf16[2,64,256]{2,1,0:T(8,128)(2,1)S(1)} %pad_maximum_fusion), channel_id=1, source_target_pairs={{0,192},{32,224},{64,0},{96,32},{128,64},{160,96},{192,128},{224,1... | collective-permute-start | bytes 196616 | tf_op jit(solution)/shard_map/ppermute | solution.py:303
  73.8 14.7 %collective-permute-start.5 = (bf16[2,64,256]{2,1,0:T(8,128)(2,1)S(1)}, bf16[2,64,256]{2,1,0:T(8,128)(2,1)S(1)}, u32[]{:S(2)}, u32[]{:S(2)}) collective-permute-start(bf16[2,64,256]{2,1,0:T(8,128)(2,1)S(1)} %pad_maximum_fusion), channel_id=1, source_target_pairs={{0,160},{32,192},{64,224},{96,0},{128,32},{160,64},{192,96},{224,1... | collective-permute-start | bytes 196616 | tf_op jit(solution)/shard_map/ppermute | solution.py:303
  77.1 13.8 %collective-permute-start.4 = (bf16[2,64,256]{2,1,0:T(8,128)(2,1)S(1)}, bf16[2,64,256]{2,1,0:T(8,128)(2,1)S(1)}, u32[]{:S(2)}, u32[]{:S(2)}) collective-permute-start(bf16[2,64,256]{2,1,0:T(8,128)(2,1)S(1)} %pad_maximum_fusion), channel_id=1, source_target_pairs={{0,128},{32,160},{64,192},{96,224},{128,0},{160,32},{192,64},{224,... | collective-permute-start | bytes 196616 | tf_op jit(solution)/shard_map/ppermute | solution.py:303
  79.0 3.1 %collective-permute-start.12 = (bf16[6,384]{1,0:T(8,128)(2,1)S(1)}, bf16[6,384]{1,0:T(8,128)(2,1)S(1)}, u32[]{:S(2)}, u32[]{:S(2)}) collective-permute-start(bf16[6,384]{1,0:T(8,128)(2,1)S(1)} %pad_maximum_fusion.2), channel_id=1, source_target_pairs={{0,1},{1,0},{2,3},{3,2},{4,5},{5,4},{6,7},{7,6},{8,9},{9,8},{10,11... | collective-permute-start | bytes 13832 | tf_op jit(solution)/shard_map/ppermute | solution.py:244
  82.1 46.7 %collective-permute-start.9 = (bf16[2048,384]{1,0:T(8,128)(2,1)}, bf16[2048,384]{1,0:T(8,128)(2,1)}, u32[]{:S(2)}, u32[]{:S(2)}) collective-permute-start(bf16[2048,384]{1,0:T(8,128)(2,1)} %refs_0_.1), channel_id=1, source_target_pairs={{0,1},{1,0},{2,3},{3,2},{4,5},{5,4},{6,7},{7,6},{8,9},{9,8},{10,11... | collective-permute-start | bytes 4718600 | tf_op jit(solution)/shard_map/ppermute | solution.py:244
  84.2 44.6 %collective-permute-start.10 = (bf16[2048,384]{1,0:T(8,128)(2,1)}, bf16[2048,384]{1,0:T(8,128)(2,1)}, u32[]{:S(2)}, u32[]{:S(2)}) collective-permute-start(bf16[2048,384]{1,0:T(8,128)(2,1)} %refs_2_.1), channel_id=1, source_target_pairs={{0,1},{1,0},{2,3},{3,2},{4,5},{5,4},{6,7},{7,6},{8,9},{9,8},{10,11... | collective-permute-start | bytes 4718600 | tf_op jit(solution)/shard_map/ppermute | solution.py:244
  86.5 42.3 %collective-permute-start.11 = (bf16[384,2048]{1,0:T(8,128)(2,1)S(1)}, bf16[384,2048]{1,0:T(8,128)(2,1)}, u32[]{:S(2)}, u32[]{:S(2)}) collective-permute-start(bf16[384,2048]{1,0:T(8,128)(2,1)S(1)} %copy-done.2), channel_id=1, source_target_pairs={{0,1},{1,0},{2,3},{3,2},{4,5},{5,4},{6,7},{7,6},{8,9},{9,8},{10,11... | collective-permute-start | bytes 4718600 | tf_op jit(solution)/shard_map/ppermute | solution.py:244
  88.6 40.2 %collective-permute-start.13 = (bf16[1536,512]{1,0:T(8,128)(2,1)}, bf16[1536,512]{1,0:T(8,128)(2,1)}, u32[]{:S(2)}, u32[]{:S(2)}) collective-permute-start(bf16[1536,512]{1,0:T(8,128)(2,1)} %bitcast.14.own_ref), channel_id=1, source_target_pairs={{0,1},{1,0},{2,3},{3,2},{4,5},{5,4},{6,7},{7,6},{8,9},{9,8},{10,11... | collective-permute-start | bytes 4718600 | tf_op jit(solution)/shard_map/ppermute | solution.py:244
  90.8 12.8 %collective-permute-start.3 = (bf16[2,64,256]{2,1,0:T(8,128)(2,1)S(1)}, bf16[2,64,256]{2,1,0:T(8,128)(2,1)S(1)}, u32[]{:S(2)}, u32[]{:S(2)}) collective-permute-start(bf16[2,64,256]{2,1,0:T(8,128)(2,1)S(1)} %pad_maximum_fusion), channel_id=1, source_target_pairs={{0,96},{32,128},{64,160},{96,192},{128,224},{160,0},{192,32},{224,... | collective-permute-start | bytes 196616 | tf_op jit(solution)/shard_map/ppermute | solution.py:303
  103.7 0.6 copy-start.7
  104.3 8.4 %collective-permute-start.2 = (bf16[2,64,256]{2,1,0:T(8,128)(2,1)S(1)}, bf16[2,64,256]{2,1,0:T(8,128)(2,1)}, u32[]{:S(2)}, u32[]{:S(2)}) collective-permute-start(bf16[2,64,256]{2,1,0:T(8,128)(2,1)S(1)} %pad_maximum_fusion), channel_id=1, source_target_pairs={{0,64},{32,96},{64,128},{96,160},{128,192},{160,224},{192,0},{224,... | collective-permute-start | bytes 196616 | tf_op jit(solution)/shard_map/ppermute | solution.py:303
  112.7 11.3 %collective-permute-start.1 = (bf16[2,64,256]{2,1,0:T(8,128)(2,1)S(1)}, bf16[2,64,256]{2,1,0:T(8,128)(2,1)S(1)}, u32[]{:S(2)}, u32[]{:S(2)}) collective-permute-start(bf16[2,64,256]{2,1,0:T(8,128)(2,1)S(1)} %pad_maximum_fusion), channel_id=1, source_target_pairs={{0,32},{32,64},{64,96},{96,128},{128,160},{160,192},{192,224},{224... | collective-permute-start | bytes 196616 | tf_op jit(solution)/shard_map/ppermute | solution.py:303
  124.0 4.8 %collective-permute-start.8 = (bf16[256,2048]{1,0:T(8,128)(2,1)}, bf16[256,2048]{1,0:T(8,128)(2,1)S(1)}, u32[]{:S(2)}, u32[]{:S(2)}) collective-permute-start(bf16[256,2048]{1,0:T(8,128)(2,1)} %own_hbm.1), channel_id=1, source_target_pairs={{0,1},{1,0},{2,3},{3,2},{4,5},{5,4},{6,7},{7,6},{8,9},{9,8},{10,11... | collective-permute-start | bytes 3145736 | tf_op jit(solution)/shard_map/ppermute | solution.py:244
  128.3 1.5 copy-start.6
  128.8 1.0 copy-start.5
  191.9 9.0 %collective-permute-start.14 = (bf16[8,1536]{1,0:T(8,128)(2,1)S(1)}, bf16[8,1536]{1,0:T(8,128)(2,1)S(1)}, u32[]{:S(2)}, u32[]{:S(2)}) collective-permute-start(bf16[8,1536]{1,0:T(8,128)(2,1)S(1)} %get-tuple-element.23), channel_id=1, source_target_pairs={{0,1},{1,0},{2,3},{3,2},{4,5},{5,4},{6,7},{7,6},{8,9},{9,8},{10,11... | collective-permute-start | bytes 73736 | tf_op jit(solution)/shard_map/ppermute | solution.py:244
  193.8 7.1 %collective-permute-start.15 = (bf16[2,1536]{1,0:T(2,128)(2,1)S(1)}, bf16[2,1536]{1,0:T(2,128)(2,1)S(1)}, u32[]{:S(2)}, u32[]{:S(2)}) collective-permute-start(bf16[2,1536]{1,0:T(2,128)(2,1)S(1)} %get-tuple-element.24), channel_id=1, source_target_pairs={{1,8},{9,16},{17,24},{25,32},{33,40},{41,48},{49,56},{57,64},{65,7... | collective-permute-start | bytes 18440 | tf_op jit(solution)/shard_map/ppermute | solution.py:250
  200.9 14.3 %copy-start.11 = (f32[2048]{0:T(1024)S(1)}, f32[2048]{0:T(1024)}, u32[]{:S(2)}) copy-start(f32[2048]{0:T(1024)} %param.29) | copy-start | bytes 24580
  205.0 10.1 %all-to-all-start.4 = ((bf16[4,16,2048]{2,1,0:T(8,128)(2,1)}), bf16[4,16,2048]{2,1,0:T(8,128)(2,1)S(1)}, u32[]{:S(2)}, u32[]{:S(2)}) async-start(bf16[4,16,2048]{2,1,0:T(8,128)(2,1)} %bitcast.17), calls=%async_computation.4 | async-start | bytes 524288 | tf_op jit(solution)/shard_map/all_to_all | solution.py:235

commit v5 on v4

--- a/solution.py
+++ b/solution.py
@@ -31,17 +31,11 @@
     return (scaled * gain).astype(bf16)
 
 
-def attend_body(line_ref, q_ref, own_ref, other_ref, o_ref):
+def attend_body(q_ref, own_ref, other_ref, o_ref):
     sources = (own_ref, other_ref)
     row = lax.broadcasted_iota(jnp.int32, (PAD, HEAD), 0)
-    lines = q_ref.shape[0] // 2
-    base = pl.program_id(0) * o_ref.shape[0]
-    for at in range(0, o_ref.shape[0] * 2, 4):
-        pieces = [
-            q_ref[pl.ds(2 * ((line_ref[0] + lines - (base + at // 2 + b)) % lines), 2)]
-            for b in range(2)
-        ]
-        q = jnp.concatenate(pieces, axis=0).reshape(4 * HALF, HEAD)
+    for at in range(0, q_ref.shape[0], 4):
+        q = q_ref[at : at + 4].reshape(4 * HALF, HEAD)
         scores = [
             lax.dot_general(
                 q, kv[:, :HEAD], (((1,), (1,)), ((), ())), preferred_element_type=f32
@@ -71,21 +65,19 @@
             o_ref[at // 2 + b, TGT_DEV:, :] = tile.astype(bf16)
 
 
-def attend(line, queries, own, other, step=4):
-    blocks = queries.shape[0] // 2
-    whole = pl.BlockSpec(queries.shape, lambda i: (0, 0, 0))
+def attend(queries, own, other, step=8):
+    blocks = queries.shape[0]
     return pl.pallas_call(
         attend_body,
         grid=(blocks // step,),
         in_specs=[
-            pl.BlockSpec(memory_space=pltpu.SMEM),
-            whole,
+            pl.BlockSpec((step, HALF, HEAD), lambda i: (i, 0, 0)),
             pl.BlockSpec(own.shape, lambda i: (0, 0)),
-            pl.BlockSpec(other.shape, lambda i: (0, 0)),
+            pl.BlockSpec(memory_space=pltpu.VMEM),
         ],
-        out_specs=pl.BlockSpec((step, TGT_DEV + PAD, HEAD), lambda i: (i, 0, 0)),
-        out_shape=pltpu.VMEM((blocks, TGT_DEV + PAD, HEAD), bf16),
-    )(line, queries, own, other)
+        out_specs=pl.BlockSpec((step // 2, TGT_DEV + PAD, HEAD), lambda i: (i, 0, 0)),
+        out_shape=pltpu.VMEM((blocks // 2, TGT_DEV + PAD, HEAD), bf16),
+    )(queries, own, in_vmem(other))
 
 
 def merge_body(parts_ref, own_hbm, other_hbm, o_ref, held, sem):
@@ -296,28 +288,21 @@
     given = lax.dynamic_index_in_dim(by_core, 1 - core, 1, False).reshape(HALF, HEAD)
     given = other_core(given)
     both = jnp.stack([kept, given])
-    lines = lax.axis_size(SLICES)
-    queries = [both]
-    for by in range(1, lines):
-        pairs = [(i, (i + by) % lines) for i in range(lines)]
-        queries.append(lax.ppermute(both, SLICES, pairs))
-    queries = jnp.concatenate(queries, axis=0)
+    queries = lax.all_gather(both[None], "ym", axis=0, tiled=True)
+    queries = lax.all_gather(queries[None], "zm", axis=0, tiled=True)
+    queries = queries.reshape(-1, HALF, HEAD)
     target_half = lax.dynamic_index_in_dim(target.reshape(4, 2, BLOCK, D), core, 1, False)
     target_half = target_half.reshape(HALF, D)
-    taps = jnp.concatenate([gate_taps, up_taps], axis=0)
+    queries, target_half = lax.optimization_barrier((queries, target_half))
+    attended = attend(queries, kv, other_core(kv))
+    parts = exchanged(attended, SLICES)
     out_other = other_core(out_weight)
     gate_other = other_core(gate_weight)
     up_other = other_core(up_weight)
     down_other = other_core(down_weight)
+    taps = jnp.concatenate([gate_taps, up_taps], axis=0)
     taps_other = other_core(taps)
     taps = jnp.concatenate([taps, taps_other], axis=1).astype(f32)
-    queries, target_half, out_other, gate_other, up_other, down_other, taps = (
-        lax.optimization_barrier(
-            (queries, target_half, out_other, gate_other, up_other, down_other, taps)
-        )
-    )
-    line_at = lax.axis_index(SLICES).astype(jnp.int32).reshape(1)
-    parts = exchanged(attend(line_at, queries, kv, other_core(kv)), SLICES)
     core_at = core.astype(jnp.int32).reshape(1)
     partial = merge_project(parts, out_weight, out_other, chips)
     residual, gate_up, tails, last = mixer_in(

time: 217 us -> 189 us (0.87)
  the two profiles are of different devices: /device:TPU:64 before, /device:TPU:128 now
where the time goes in v5:
time: 189 us; the launch traced here: 188 us
  blocking collectives  98.5 us (52%)
  starting transfers between devices  35 us (19%)
  waiting for transfers between devices  28 us (15%)
  Pallas kernels  19.5 us (10%)
  matrix products  3.05 us (2%)
  other arithmetic  2.95 us (2%)
    all_to_all x2, blocking collectives, exchanged(): return lax.all_to_all(array, axes, 0, 0, tiled=True)  67.9 us
    all_to_all x3, waiting for transfers between devices, exchanged(): return lax.all_to_all(array, axes, 0, 0, tiled=True)  22.8 us
    all_gather x1, blocking collectives, shards(): queries = lax.all_gather(queries[None], 'zm', axis=0, tiled=True)  20.2 us
    all_to_all x3, starting transfers between devices, exchanged(): return lax.all_to_all(array, axes, 0, 0, tiled=True)  16.8 us
    ppermute x8, starting transfers between devices, other_core(): return lax.ppermute(array, 'c', [(0, 1), (1, 0)])  16.8 us
    all_gather x1, blocking collectives, shards(): queries = lax.all_gather(both[None], 'ym', axis=0, tiled=True)  10.3 us
    pallas_call x1, Pallas kernels, attend(): pl.pallas_call(attend_body, grid=(blocks // step,), in_specs=[pl.BlockSpe...  8.37 us
    ppermute x1, waiting for transfers between devices, from_last_line(): lax.ppermute(array, axes, [(2 * i + 1, 2 * i + 2) for i in range(lines -...  5.13 us
  transfers between devices with their start and end apart: 12, of which 5 were waited for; matrix products, arithmetic and copies ran while one was open for 1% of the time, Pallas kernels for 4%

profile of v5, /device:TPU:128, one launch (start us, length us, event | category | flops | bytes accessed | tf_op | source)
XLA Modules:
  0.0 188.4 jit_solution(5521682017810062810)
XLA Ops:
  0.0 1.2 fusion.7
  1.2 2.2 %convolution_convert_fusion.2 = bf16[32,512]{1,0:T(8,128)(2,1)S(1)} fusion(bf16[2048,512]{1,0:T(8,128)(2,1)} %param.20, bf16[32,2048]{1,0:T(8,128)(2,1)} %param.16, f32[2048]{0:T(1024)} %param.18, f32[32]{0:T(128)S(1)} %add_rsqrt_fusion.1), kind=kOutput, calls=%fused_computation.5 | convolution fusion | flops 67387392 | bytes 2269312 | tf_op jit(solution)/shard_map/dot_general | solution.py:265
  3.5 0.5 convolution_convert_fusion.1
  4.1 46.0 %all_to_all.25 = bf16[12,64,512]{2,1,0:T(8,128)(2,1)S(1)} all-to-all(bf16[12,64,512]{2,1,0:T(8,128)(2,1)S(1)} %broadcast_in_dim.24), channel_id=1, replica_groups=mesh['zq'=3,'zm'=4,'ym'=2,'yq'=4,'g'=2,'xp'=2,'c'=2] {'yq','zq'}, dimensions={0} | all-to-all | bytes 1572864 | tf_op jit(solution)/shard_map/all_to_all | solution.py:227
  50.3 21.8 %all_to_all.26 = bf16[4,384,512]{2,1,0:T(8,128)(2,1)} all-to-all(bf16[4,384,512]{2,1,0:T(8,128)(2,1)S(1)} %bitcast.27), channel_id=1, replica_groups=mesh['zq'=3,'zm'=4,'ym'=2,'yq'=4,'g'=2,'xp'=2,'c'=2] {'g','xp'}, dimensions={0} | all-to-all | bytes 3145728 | tf_op jit(solution)/shard_map/all_to_all | solution.py:227
  72.2 1.9 %collective-permute-start.1 = (bf16[1536,512]{1,0:T(8,128)(2,1)}, bf16[1536,512]{1,0:T(8,128)(2,1)S(1)}, u32[]{:S(2)}, u32[]{:S(2)}) collective-permute-start(bf16[1536,512]{1,0:T(8,128)(2,1)} %bitcast.15.own_ref), channel_id=1, source_target_pairs={{0,1},{1,0},{2,3},{3,2},{4,5},{5,4},{6,7},{7,6},{8,9},{9,8},{10,11... | collective-permute-start | bytes 4718600 | tf_op jit(solution)/shard_map/ppermute | solution.py:236
  74.1 0.2 fusion.1
  74.3 0.4 fusion
  74.7 2.4 %collective-permute-start = (bf16[64,256]{1,0:T(8,128)(2,1)S(1)}, bf16[64,256]{1,0:T(8,128)(2,1)S(1)}, u32[]{:S(2)}, u32[]{:S(2)}) collective-permute-start(bf16[64,256]{1,0:T(8,128)(2,1)S(1)} %bitcast.37), channel_id=1, source_target_pairs={{0,1},{1,0},{2,3},{3,2},{4,5},{5,4},{6,7},{7,6},{8,9},{9,8},{10,11... | collective-permute-start | bytes 98312 | tf_op jit(solution)/shard_map/ppermute | solution.py:236
  77.1 0.7 constant_dynamic-slice_fusion
  78.0 10.3 %all-gather = bf16[4,64,256]{2,1,0:T(8,128)(2,1)S(1)} all-gather(bf16[2,64,256]{2,1,0:T(8,128)(2,1)S(1)} %pad_maximum_fusion), channel_id=2, replica_groups=mesh['zq'=3,'zm'=4,'ym'=2,'yq'=4,'g'=2,'xp'=2,'c'=2] {'ym'}, dimensions={0}, use_global_device_ids=true | all-gather | bytes 196608 | tf_op jit(solution)/shard_map/all_gather | solution.py:291
  88.3 20.2 %all-gather.1 = bf16[8,2,64,256]{3,2,1,0:T(8,128)(2,1)} all-gather(bf16[2,2,64,256]{3,2,1,0:T(8,128)(2,1)S(1)} %bitcast.33), channel_id=3, replica_groups=mesh['zq'=3,'zm'=4,'ym'=2,'yq'=4,'g'=2,'xp'=2,'c'=2] {'zm'}, dimensions={0}, use_global_device_ids=true | all-gather | bytes 655360 | tf_op jit(solution)/shard_map/all_gather | solution.py:292
  108.6 8.4 %shard_map.145 = bf16[8,144,256]{2,1,0:T(8,128)(2,1)} custom-call(bf16[16,64,256]{2,1,0:T(8,128)(2,1)} %bitcast.30, bf16[1536,512]{1,0:T(8,128)(2,1)} %bitcast.15.own_ref, bf16[1536,512]{1,0:T(8,128)(2,1)S(1)} %collective-permute-done.1.other_ref), custom_call_target="tpu_custom_call" | custom-call | tf_op jit(solution)/shard_map/pallas_call | solution.py:70
  116.9 9.9 %all-to-all-start.2 = ((bf16[8,144,256]{2,1,0:T(8,128)(2,1)}), bf16[8,144,256]{2,1,0:T(8,128)(2,1)S(1)}, u32[]{:S(2)}, u32[]{:S(2)}) async-start(bf16[8,144,256]{2,1,0:T(8,128)(2,1)} %shard_map.145), calls=%async_computation.2 | async-start | bytes 1179648 | tf_op jit(solution)/shard_map/all_to_all | solution.py:227
  126.8 1.9 %collective-permute-start.2 = (bf16[256,2048]{1,0:T(8,128)(2,1)}, bf16[256,2048]{1,0:T(8,128)(2,1)S(1)}, u32[]{:S(2)}, u32[]{:S(2)}) collective-permute-start(bf16[256,2048]{1,0:T(8,128)(2,1)} %own_hbm.1), channel_id=1, source_target_pairs={{0,1},{1,0},{2,3},{3,2},{4,5},{5,4},{6,7},{7,6},{8,9},{9,8},{10,11... | collective-permute-start | bytes 3145736 | tf_op jit(solution)/shard_map/ppermute | solution.py:236
  128.8 2.4 %collective-permute-start.3 = (bf16[2048,384]{1,0:T(8,128)(2,1)}, bf16[2048,384]{1,0:T(8,128)(2,1)}, u32[]{:S(2)}, u32[]{:S(2)}) collective-permute-start(bf16[2048,384]{1,0:T(8,128)(2,1)} %refs_0_.1), channel_id=1, source_target_pairs={{0,1},{1,0},{2,3},{3,2},{4,5},{5,4},{6,7},{7,6},{8,9},{9,8},{10,11... | collective-permute-start | bytes 4718600 | tf_op jit(solution)/shard_map/ppermute | solution.py:236
  131.2 1.9 %collective-permute-start.4 = (bf16[2048,384]{1,0:T(8,128)(2,1)}, bf16[2048,384]{1,0:T(8,128)(2,1)}, u32[]{:S(2)}, u32[]{:S(2)}) collective-permute-start(bf16[2048,384]{1,0:T(8,128)(2,1)} %refs_2_.1), channel_id=1, source_target_pairs={{0,1},{1,0},{2,3},{3,2},{4,5},{5,4},{6,7},{7,6},{8,9},{9,8},{10,11... | collective-permute-start | bytes 4718600 | tf_op jit(solution)/shard_map/ppermute | solution.py:236
  133.1 2.4 %collective-permute-start.8 = (bf16[384,2048]{1,0:T(8,128)(2,1)}, bf16[384,2048]{1,0:T(8,128)(2,1)}, u32[]{:S(2)}, u32[]{:S(2)}) collective-permute-start(bf16[384,2048]{1,0:T(8,128)(2,1)} %down_ref.1), channel_id=1, source_target_pairs={{0,1},{1,0},{2,3},{3,2},{4,5},{5,4},{6,7},{7,6},{8,9},{9,8},{10,11... | collective-permute-start | bytes 4718600 | tf_op jit(solution)/shard_map/ppermute | solution.py:236
  135.5 5.8 %all-to-all-done.2.parts_ref = bf16[8,144,256]{2,1,0:T(8,128)(2,1)S(1)} async-done(((bf16[8,144,256]{2,1,0:T(8,128)(2,1)}), bf16[8,144,256]{2,1,0:T(8,128)(2,1)S(1)}, u32[]{:S(2)}, u32[]{:S(2)}) %all-to-all-start.2) | async-done | bytes 589856 | tf_op jit(solution)/shard_map/all_to_all | solution.py:227
  141.4 3.0 %shard_map.146 = bf16[4,64,2048]{2,1,0:T(8,128)(2,1)} custom-call(bf16[8,144,256]{2,1,0:T(8,128)(2,1)S(1)} %all-to-all-done.2.parts_ref, bf16[256,2048]{1,0:T(8,128)(2,1)} %own_hbm.1, bf16[256,2048]{1,0:T(8,128)(2,1)} %copy-done.4), custom_call_target="tpu_custom_call" | custom-call | tf_op jit(solution)/shard_map/pallas_call | solution.py:113
  144.4 3.5 %all-to-all-start.3 = ((bf16[4,64,2048]{2,1,0:T(8,128)(2,1)}), bf16[4,64,2048]{2,1,0:T(8,128)(2,1)S(1)}, u32[]{:S(2)}, u32[]{:S(2)}) async-start(bf16[4,64,2048]{2,1,0:T(8,128)(2,1)} %shard_map.146), calls=%async_computation.3 | async-start | bytes 2097152 | tf_op jit(solution)/shard_map/all_to_all | solution.py:227
  148.0 1.9 %collective-permute-start.7 = (bf16[6,384]{1,0:T(8,128)(2,1)S(1)}, bf16[6,384]{1,0:T(8,128)(2,1)S(1)}, u32[]{:S(2)}, u32[]{:S(2)}) collective-permute-start(bf16[6,384]{1,0:T(8,128)(2,1)S(1)} %pad_maximum_fusion.2), channel_id=1, source_target_pairs={{0,1},{1,0},{2,3},{3,2},{4,5},{5,4},{6,7},{7,6},{8,9},{9,8},{10,11... | collective-permute-start | bytes 13832 | tf_op jit(solution)/shard_map/ppermute | solution.py:236
  150.0 10.3 %all-to-all-done.3.tiles_ref = bf16[4,64,2048]{2,1,0:T(8,128)(2,1)S(1)} async-done(((bf16[4,64,2048]{2,1,0:T(8,128)(2,1)}), bf16[4,64,2048]{2,1,0:T(8,128)(2,1)S(1)}, u32[]{:S(2)}, u32[]{:S(2)}) %all-to-all-start.3) | async-done | bytes 1048608 | tf_op jit(solution)/shard_map/all_to_all | solution.py:227
  160.3 4.1 %shard_map.147 = (bf16[64,2048]{1,0:T(8,128)(2,1)S(1)}, bf16[64,1536]{1,0:T(8,128)(2,1)S(1)}, bf16[8,1536]{1,0:T(8,128)(2,1)S(1)}, bf16[2,1536]{1,0:T(2,128)(2,1)S(1)}) custom-call(bf16[4,64,2048]{2,1,0:T(8,128)(2,1)S(1)} %all-to-all-done.3.tiles_ref, bf16[64,2048]{1,0:T(8,128)(2,1)} %bitcast.32, f32[1,2048]{1,0:T(1,128)} %bitcast.39, ...), custom_call_target="tpu_custom_call" | custom-call | tf_op jit(solution)/shard_map/pallas_call | solution.py:151
  164.4 1.9 %collective-permute-start.5 = (bf16[8,1536]{1,0:T(8,128)(2,1)S(1)}, bf16[8,1536]{1,0:T(8,128)(2,1)S(1)}, u32[]{:S(2)}, u32[]{:S(2)}) collective-permute-start(bf16[8,1536]{1,0:T(8,128)(2,1)S(1)} %get-tuple-element.15), channel_id=1, source_target_pairs={{0,1},{1,0},{2,3},{3,2},{4,5},{5,4},{6,7},{7,6},{8,9},{9,8},{10,11... | collective-permute-start | bytes 73736 | tf_op jit(solution)/shard_map/ppermute | solution.py:236
  166.3 1.3 collective-permute-start.6
  167.6 0.6 maximum_convert_fusion.taps_ref
  168.3 5.1 %collective-permute-done.6.before_ref = bf16[2,1536]{1,0:T(2,128)(2,1)S(1)} collective-permute-done((bf16[2,1536]{1,0:T(2,128)(2,1)S(1)}, bf16[2,1536]{1,0:T(2,128)(2,1)S(1)}, u32[]{:S(2)}, u32[]{:S(2)}) %collective-permute-start.6) | collective-permute-done | bytes 6176 | tf_op jit(solution)/shard_map/ppermute | solution.py:242
  173.4 4.0 %shard_map.148 = bf16[64,2048]{1,0:T(8,128)(2,1)} custom-call(s32[1]{0:T(128)} %bitcast.17.core_ref, bf16[64,1536]{1,0:T(8,128)(2,1)S(1)} %get-tuple-element.14.gu_ref, bf16[8,1536]{1,0:T(8,128)(2,1)S(1)} %collective-permute-done.5.across_ref, bf16[2,1536]{1,0:T(2,128)(2,1)S(1)} %collective-permute-done.6.before_ref, f32[6,768]{1,0:T(8,128)} %maximum_convert_fusion.taps_ref, ...), custom_call_target="tpu_custom_call" | custom-call | tf_op jit(solution)/shard_map/pallas_call | solution.py:218
  177.4 3.4 %all-to-all-start.4 = ((bf16[4,16,2048]{2,1,0:T(8,128)(2,1)}), bf16[4,16,2048]{2,1,0:T(8,128)(2,1)S(1)}, u32[]{:S(2)}, u32[]{:S(2)}) async-start(bf16[4,16,2048]{2,1,0:T(8,128)(2,1)} %bitcast.18), calls=%async_computation.4 | async-start | bytes 524288 | tf_op jit(solution)/shard_map/all_to_all | solution.py:227
  180.9 6.6 %all-to-all-done.4 = bf16[4,16,2048]{2,1,0:T(8,128)(2,1)S(1)} async-done(((bf16[4,16,2048]{2,1,0:T(8,128)(2,1)}), bf16[4,16,2048]{2,1,0:T(8,128)(2,1)S(1)}, u32[]{:S(2)}, u32[]{:S(2)}) %all-to-all-start.4) | async-done | bytes 262176 | tf_op jit(solution)/shard_map/all_to_all | solution.py:227
  187.7 0.7 multiply_convert_fusion
  (43 shorter events, 0.7 us)
Async XLA Ops:
  0.0 74.3 %copy-start = (bf16[2048,256]{1,0:T(8,128)(2,1)S(1)}, bf16[2048,256]{1,0:T(8,128)(2,1)}, u32[]{:S(2)}) copy-start(bf16[2048,256]{1,0:T(8,128)(2,1)} %param.19) | copy-start | bytes 3145732
  0.0 3.4 %copy-start.2 = (bf16[32,2048]{1,0:T(8,128)(2,1)S(1)}, bf16[32,2048]{1,0:T(8,128)(2,1)}, u32[]{:S(2)}) copy-start(bf16[32,2048]{1,0:T(8,128)(2,1)} %param.16) | copy-start | bytes 393220
  0.0 3.4 %copy-start.5 = (f32[2048]{0:T(1024)S(1)}, f32[2048]{0:T(1024)}, u32[]{:S(2)}) copy-start(f32[2048]{0:T(1024)} %param.18) | copy-start | bytes 24580
  0.0 3.4 %copy-start.1 = (bf16[2048,512]{1,0:T(8,128)(2,1)S(1)}, bf16[2048,512]{1,0:T(8,128)(2,1)}, u32[]{:S(2)}) copy-start(bf16[2048,512]{1,0:T(8,128)(2,1)} %param.21) | copy-start | bytes 6291460
  50.3 23.8 %copy-start.3 = (bf16[128,2048]{1,0:T(8,128)(2,1)S(1)}, bf16[128,2048]{1,0:T(8,128)(2,1)}, u32[]{:S(2)}) copy-start(bf16[128,2048]{1,0:T(8,128)(2,1)} %param.15) | copy-start | bytes 1572868
  50.3 24.0 %copy-start.9 = (f32[2048]{0:T(1024)S(1)}, f32[2048]{0:T(1024)}, u32[]{:S(2)}) copy-start(f32[2048]{0:T(1024)} %param.17) | copy-start | bytes 24580
  72.2 36.4 %collective-permute-start.1 = (bf16[1536,512]{1,0:T(8,128)(2,1)}, bf16[1536,512]{1,0:T(8,128)(2,1)S(1)}, u32[]{:S(2)}, u32[]{:S(2)}) collective-permute-start(bf16[1536,512]{1,0:T(8,128)(2,1)} %bitcast.15.own_ref), channel_id=1, source_target_pairs={{0,1},{1,0},{2,3},{3,2},{4,5},{5,4},{6,7},{7,6},{8,9},{9,8},{10,11... | collective-permute-start | bytes 4718600 | tf_op jit(solution)/shard_map/ppermute | solution.py:236
  74.7 3.3 %collective-permute-start = (bf16[64,256]{1,0:T(8,128)(2,1)S(1)}, bf16[64,256]{1,0:T(8,128)(2,1)S(1)}, u32[]{:S(2)}, u32[]{:S(2)}) collective-permute-start(bf16[64,256]{1,0:T(8,128)(2,1)S(1)} %bitcast.37), channel_id=1, source_target_pairs={{0,1},{1,0},{2,3},{3,2},{4,5},{5,4},{6,7},{7,6},{8,9},{9,8},{10,11... | collective-permute-start | bytes 98312 | tf_op jit(solution)/shard_map/ppermute | solution.py:236
  116.9 24.4 %all-to-all-start.2 = ((bf16[8,144,256]{2,1,0:T(8,128)(2,1)}), bf16[8,144,256]{2,1,0:T(8,128)(2,1)S(1)}, u32[]{:S(2)}, u32[]{:S(2)}) async-start(bf16[8,144,256]{2,1,0:T(8,128)(2,1)} %shard_map.145), calls=%async_computation.2 | async-start | bytes 1179648 | tf_op jit(solution)/shard_map/all_to_all | solution.py:227
  126.8 8.7 %collective-permute-start.2 = (bf16[256,2048]{1,0:T(8,128)(2,1)}, bf16[256,2048]{1,0:T(8,128)(2,1)S(1)}, u32[]{:S(2)}, u32[]{:S(2)}) collective-permute-start(bf16[256,2048]{1,0:T(8,128)(2,1)} %own_hbm.1), channel_id=1, source_target_pairs={{0,1},{1,0},{2,3},{3,2},{4,5},{5,4},{6,7},{7,6},{8,9},{9,8},{10,11... | collective-permute-start | bytes 3145736 | tf_op jit(solution)/shard_map/ppermute | solution.py:236
  128.8 21.2 %collective-permute-start.3 = (bf16[2048,384]{1,0:T(8,128)(2,1)}, bf16[2048,384]{1,0:T(8,128)(2,1)}, u32[]{:S(2)}, u32[]{:S(2)}) collective-permute-start(bf16[2048,384]{1,0:T(8,128)(2,1)} %refs_0_.1), channel_id=1, source_target_pairs={{0,1},{1,0},{2,3},{3,2},{4,5},{5,4},{6,7},{7,6},{8,9},{9,8},{10,11... | collective-permute-start | bytes 4718600 | tf_op jit(solution)/shard_map/ppermute | solution.py:236
  131.2 18.8 %collective-permute-start.4 = (bf16[2048,384]{1,0:T(8,128)(2,1)}, bf16[2048,384]{1,0:T(8,128)(2,1)}, u32[]{:S(2)}, u32[]{:S(2)}) collective-permute-start(bf16[2048,384]{1,0:T(8,128)(2,1)} %refs_2_.1), channel_id=1, source_target_pairs={{0,1},{1,0},{2,3},{3,2},{4,5},{5,4},{6,7},{7,6},{8,9},{9,8},{10,11... | collective-permute-start | bytes 4718600 | tf_op jit(solution)/shard_map/ppermute | solution.py:236
  133.1 35.2 %collective-permute-start.8 = (bf16[384,2048]{1,0:T(8,128)(2,1)}, bf16[384,2048]{1,0:T(8,128)(2,1)}, u32[]{:S(2)}, u32[]{:S(2)}) collective-permute-start(bf16[384,2048]{1,0:T(8,128)(2,1)} %down_ref.1), channel_id=1, source_target_pairs={{0,1},{1,0},{2,3},{3,2},{4,5},{5,4},{6,7},{7,6},{8,9},{9,8},{10,11... | collective-permute-start | bytes 4718600 | tf_op jit(solution)/shard_map/ppermute | solution.py:236
  135.5 5.8 %copy-start.4 = (bf16[256,2048]{1,0:T(8,128)(2,1)}, bf16[256,2048]{1,0:T(8,128)(2,1)S(1)}, u32[]{:S(2)}) copy-start(bf16[256,2048]{1,0:T(8,128)(2,1)S(1)} %collective-permute-done.2.other_hbm) | copy-start | bytes 3145732
  144.4 3.6 %copy-start.6 = (bf16[3,384]{1,0:T(4,128)(2,1)S(1)}, bf16[3,384]{1,0:T(4,128)(2,1)}, u32[]{:S(2)}) copy-start(bf16[3,384]{1,0:T(4,128)(2,1)} %param.27) | copy-start | bytes 6916
  144.4 3.6 %copy-start.7 = (bf16[3,384]{1,0:T(4,128)(2,1)S(1)}, bf16[3,384]{1,0:T(4,128)(2,1)}, u32[]{:S(2)}) copy-start(bf16[3,384]{1,0:T(4,128)(2,1)} %param.26) | copy-start | bytes 6916
  144.4 15.9 %all-to-all-start.3 = ((bf16[4,64,2048]{2,1,0:T(8,128)(2,1)}), bf16[4,64,2048]{2,1,0:T(8,128)(2,1)S(1)}, u32[]{:S(2)}, u32[]{:S(2)}) async-start(bf16[4,64,2048]{2,1,0:T(8,128)(2,1)} %shard_map.146), calls=%async_computation.3 | async-start | bytes 2097152 | tf_op jit(solution)/shard_map/all_to_all | solution.py:227
  148.0 19.6 %collective-permute-start.7 = (bf16[6,384]{1,0:T(8,128)(2,1)S(1)}, bf16[6,384]{1,0:T(8,128)(2,1)S(1)}, u32[]{:S(2)}, u32[]{:S(2)}) collective-permute-start(bf16[6,384]{1,0:T(8,128)(2,1)S(1)} %pad_maximum_fusion.2), channel_id=1, source_target_pairs={{0,1},{1,0},{2,3},{3,2},{4,5},{5,4},{6,7},{7,6},{8,9},{9,8},{10,11... | collective-permute-start | bytes 13832 | tf_op jit(solution)/shard_map/ppermute | solution.py:236
  164.4 9.0 %collective-permute-start.5 = (bf16[8,1536]{1,0:T(8,128)(2,1)S(1)}, bf16[8,1536]{1,0:T(8,128)(2,1)S(1)}, u32[]{:S(2)}, u32[]{:S(2)}) collective-permute-start(bf16[8,1536]{1,0:T(8,128)(2,1)S(1)} %get-tuple-element.15), channel_id=1, source_target_pairs={{0,1},{1,0},{2,3},{3,2},{4,5},{5,4},{6,7},{7,6},{8,9},{9,8},{10,11... | collective-permute-start | bytes 73736 | tf_op jit(solution)/shard_map/ppermute | solution.py:236
  166.3 7.1 %collective-permute-start.6 = (bf16[2,1536]{1,0:T(2,128)(2,1)S(1)}, bf16[2,1536]{1,0:T(2,128)(2,1)S(1)}, u32[]{:S(2)}, u32[]{:S(2)}) collective-permute-start(bf16[2,1536]{1,0:T(2,128)(2,1)S(1)} %get-tuple-element.16), channel_id=1, source_target_pairs={{1,8},{9,16},{17,24},{25,32},{33,40},{41,48},{49,56},{57,64},{65,7... | collective-permute-start | bytes 18440 | tf_op jit(solution)/shard_map/ppermute | solution.py:242
  173.4 14.3 %copy-start.8 = (f32[2048]{0:T(1024)S(1)}, f32[2048]{0:T(1024)}, u32[]{:S(2)}) copy-start(f32[2048]{0:T(1024)} %param.29) | copy-start | bytes 24580
  177.4 10.1 %all-to-all-start.4 = ((bf16[4,16,2048]{2,1,0:T(8,128)(2,1)}), bf16[4,16,2048]{2,1,0:T(8,128)(2,1)S(1)}, u32[]{:S(2)}, u32[]{:S(2)}) async-start(bf16[4,16,2048]{2,1,0:T(8,128)(2,1)} %bitcast.18), calls=%async_computation.4 | async-start | bytes 524288 | tf_op jit(solution)/shard_map/all_to_all | solution.py:227
